TPU v7x, 128 devices: a whole 4x4x4 slice. The times are simulated.
128 devices in a mesh: sp: 16 (over z, y), dp: 8 (over x, core).
Axes of the slice: x: 4, y: 4, z: 4, core: 2. Of those that a mesh axis runs over, the one named last changes fastest.
Arguments:
- residual: bfloat16 [8, 2048, 2048], P('dp', 'sp'), may hold values from -6 to 6
- query_maps: bfloat16 [8, 2048, 2048], P('dp', 'sp'), may hold values from -200 to 200
- key_maps: bfloat16 [8, 2048, 2048], P('dp', 'sp'), may hold values from -200 to 200
- value_rows: bfloat16 [8, 2048, 2048], P('dp', 'sp'), may hold values from -6 to 6
- lambdas: float32 [16], replicated, may hold values from 0.3 to 0.8
- head_gain: float32 [2048], replicated, may hold values from 0.1 to 1.9
- out_weight: bfloat16 [2048, 2048], replicated, may hold values from -0.125 to 0.125
- ffn_gain: float32 [2048], replicated, may hold values from 0.1 to 1.9
- routes: int32 [8, 2048, 2], P('dp', 'sp'), may hold values from 0 to 127, all different within a row; in each aligned block of 128 rows (0 to 127, 128 to 255, ..., all dimensions but the last counted through in order) at most 4 rows name the same one
- route_weights: float32 [8, 2048, 2], P('dp', 'sp'), may hold values from 0.2 to 1
- expert_gate: bfloat16 [128, 2048, 1024], P(('sp', 'dp')), may hold values from -0.125 to 0.125
- expert_up: bfloat16 [128, 2048, 1024], P(('sp', 'dp')), may hold values from -0.125 to 0.125
- expert_down: bfloat16 [128, 1024, 2048], P(('sp', 'dp')), may hold values from -0.1875 to 0.1875
Outputs:
- layer_out: bfloat16 [8, 2048, 2048], P('dp', 'sp')
Inputs may be any that keep to these rules, and one draw needn't show every extreme that they name: `routes`: A token's 2 experts differ; among the 128 rows of one device no expert is named more than 4 times, and in every draw some expert is named exactly 4 times by one device's rows.
All inputs are finite; a program needn't handle non-finite values.
Results may differ from a plain program's by a relative error of at most 0.012.
Values may be sent and summed in bfloat16 or wider, within the bound.
No kernel may reach another device: no remote copies, remote signals or barrier semaphores. Data moves between devices by JAX's collectives and lax.ppermute only.
A program may use at most 128 MiB of HBM per device.

v0:
```python
import jax
import jax.numpy as jnp
from jax import lax
from jax.sharding import Mesh
from jax.sharding import PartitionSpec as P

D = 2048
HEADS = 16
HD = 64
VD = 128
SP = ("sp_0", "sp_1")
SP_DP = ("sp_0", "sp_1", "dp")


eps = 1e-06


def side_by_side(arrays, axis, split_dim, concat_dim, along):
    both = jnp.concatenate(arrays, axis=along)
    whole, at, finished = (
        lax.all_to_all(both, axis, split_axis=split_dim, concat_axis=concat_dim, tiled=True),
        0,
        [],
    )
    for a in arrays:
        finished.append(lax.slice_in_dim(whole, at, at + a.shape[along], axis=along))
        at += a.shape[along]
    return tuple(finished)


def in_blocks(value, dim, size):
    lengths = value.shape
    blocks = value.reshape(*lengths[:dim], size, lengths[dim] // size, *lengths[dim + 1 :])
    return jnp.moveaxis(blocks, dim, 0)


def laid_out(blocks, dim):
    blocks = jnp.moveaxis(blocks, 0, dim)
    lengths = blocks.shape
    return blocks.reshape(*lengths[:dim], lengths[dim] * lengths[dim + 1], *lengths[dim + 2 :])


def exchange_in_order(blocks, axes, sequence):
    lengths = [lax.axis_size(a) for a in axes]
    blocks = blocks.reshape(*lengths, *blocks.shape[1:])
    for k in sequence:
        blocks = lax.all_to_all(blocks, axes[k], split_axis=k, concat_axis=k, tiled=True)
    return blocks.reshape(-1, *blocks.shape[len(axes) :])


def one_axis_at_a_time(value, axes, sequence, split_dim, concat_dim):
    blocks = in_blocks(value, split_dim, lax.axis_size(axes))
    return laid_out(exchange_in_order(blocks, axes, sequence), concat_dim)


def exchange_both(value, axis, axes, splits, concats):
    sizes = [lax.axis_size(a) for a in axes]
    blocks = in_blocks(value, splits[0], sizes[0])
    blocks = jnp.moveaxis(in_blocks(blocks, splits[1] + 1, sizes[1]), 0, 1)
    inside = blocks.shape[2:]
    blocks = blocks.reshape(-1, *inside)
    blocks = lax.all_to_all(blocks, axis, split_axis=0, concat_axis=0, tiled=True)
    blocks = laid_out(blocks.reshape(*sizes, *inside), concats[0] + 1)
    return laid_out(blocks, concats[1])


def attend_head(query_head, key_head, value_head, lam_head, gain_head):
    length = query_head.shape[0]
    block_rows = min(512, length)
    count_blocks = length // block_rows
    scaling = query_head.shape[-1] ** (-0.5)
    query_blocks = query_head.reshape(count_blocks, block_rows, 2, query_head.shape[-1])

    def one_block(query_block):
        scores = (
            jnp.einsum("qmd,kmd->mqk", query_block, key_head, preferred_element_type=jnp.float32)
            * scaling
        )
        probabilities = jax.nn.softmax(scores, axis=-1)
        mixed_map = (probabilities[0] - lam_head * probabilities[1]).astype(jnp.bfloat16)
        head_out = jnp.dot(mixed_map, value_head, preferred_element_type=jnp.float32)
        normed = head_out * lax.rsqrt(jnp.mean(head_out * head_out, axis=-1, keepdims=True) + eps)
        return (normed * gain_head * 0.8).astype(jnp.bfloat16)

    return lax.map(one_block, query_blocks).reshape(length, value_head.shape[-1])


def on_device(
    residual,
    query_maps,
    key_maps,
    value_rows,
    lambdas,
    head_gain,
    out_weight,
    ffn_gain,
    routes,
    route_weights,
    expert_gate,
    expert_up,
    expert_down,
):
    count_sp = lax.axis_size(SP)
    count_dp = lax.axis_size("dp")
    heads_here = HEADS // count_sp
    queries, keys_all, values_all = side_by_side((query_maps, key_maps, value_rows), SP, 2, 1, 0)
    first_head = lax.axis_index(SP) * heads_here
    lam_here = lax.dynamic_slice_in_dim(lambdas, first_head, heads_here)
    gain_here = lax.dynamic_slice_in_dim(head_gain, first_head * VD, heads_here * VD)
    query_head = queries[0, :, 0 : 2 * HD].reshape(-1, 2, HD)
    key_head = keys_all[0, :, 0 : 2 * HD].reshape(-1, 2, HD)
    value_head = values_all[0, :, 0:VD]
    outputs = attend_head(query_head, key_head, value_head, lam_here[0], gain_here)
    attended = outputs[None]
    returned_heads = one_axis_at_a_time(attended, SP, (0, 1), 1, 2)
    projected = jnp.dot(returned_heads[0], out_weight, preferred_element_type=jnp.float32)
    residual_mid = (residual[0].astype(jnp.float32) + projected).astype(jnp.bfloat16)
    middle = residual_mid.astype(jnp.float32)
    expert_input = (
        middle * lax.rsqrt(jnp.mean(middle * middle, axis=-1, keepdims=True) + eps) * ffn_gain
    ).astype(jnp.bfloat16)
    tok_rows = residual.shape[1]
    experts_all = count_sp * count_dp
    capacity = max(2, 4 * tok_rows // experts_all)
    flat_routes = routes[0].reshape(-1)
    flat_weights = route_weights[0].reshape(-1)
    onehot = (flat_routes[:, None] == jnp.arange(experts_all, dtype=jnp.int32)[None, :]).astype(
        jnp.int32
    )
    before = jnp.cumsum(onehot, axis=0) - onehot
    rank_of = jnp.sum(before * onehot, axis=1)
    slot = flat_routes * capacity + rank_of
    token_of = jnp.arange(flat_routes.shape[0], dtype=jnp.int32) // routes.shape[2]
    slot_token = jnp.full((experts_all * capacity,), tok_rows, jnp.int32).at[slot].set(token_of)
    padded_input = jnp.concatenate([expert_input, jnp.zeros((1, D), jnp.bfloat16)], axis=0)
    buffer = padded_input[slot_token].reshape(experts_all, capacity, D)
    shaped = buffer.reshape(count_sp, count_dp, capacity, D)
    received = exchange_both(shaped, SP_DP, (SP, "dp"), (0, 1), (0, 1))
    row_block = received.reshape(-1, D)
    gate_part = jnp.dot(row_block, expert_gate[0], preferred_element_type=jnp.float32)
    up_part = jnp.dot(row_block, expert_up[0], preferred_element_type=jnp.float32)
    hidden = (jax.nn.silu(gate_part) * up_part).astype(jnp.bfloat16)
    expert_out = jnp.dot(hidden, expert_down[0], preferred_element_type=jnp.float32).astype(
        jnp.bfloat16
    )
    returned = exchange_both(expert_out.reshape(received.shape), SP_DP, (SP, "dp"), (0, 1), (0, 1))
    picked = returned.reshape(experts_all * capacity, D)[slot]
    weighted = (picked.astype(jnp.float32) * flat_weights[:, None]).reshape(
        tok_rows, routes.shape[2], D
    )
    layer_out = (middle + jnp.sum(weighted, axis=1)).astype(jnp.bfloat16)
    return layer_out[None]


def solution(mesh):
    finer = Mesh(mesh.devices.reshape(4, 4, mesh.shape["dp"]), ("sp_0", "sp_1", "dp"))
    placed = (
        P("dp", SP, None),
        P("dp", SP, None),
        P("dp", SP, None),
        P("dp", SP, None),
        P(),
        P(),
        P(),
        P(),
        P("dp", SP, None),
        P("dp", SP, None),
        P(SP_DP, None, None),
        P(SP_DP, None, None),
        P(SP_DP, None, None),
    )
    return jax.shard_map(
        on_device, mesh=finer, in_specs=placed, out_specs=P("dp", SP, None), check_vma=False
    )
```

profile of v0, /device:TPU:1, one launch (start us, length us, event | category | flops | bytes accessed | tf_op | source)
XLA Modules:
  0.0 236.5 jit_solution(16447463761068725276)
XLA Ops:
  0.0 1.5 pad_maximum_fusion
  1.5 2.5 %copy.46 = bf16[3,128,2048]{1,0,2:T(4,128)(2,1)} copy(bf16[3,128,2048]{2,1,0:T(8,128)(2,1)S(1)} %pad_maximum_fusion) | data formatting | bytes 3145728 | tf_op jit(solution)/shard_map/concatenate | solution.py:19
  4.1 8.7 %all-to-all-start = ((bf16[3,128,2048]{1,0,2:T(4,128)(2,1)}), bf16[3,128,2048]{1,0,2:T(4,128)(2,1)S(1)}, u32[]{:S(2)}, u32[]{:S(2)}) async-start(bf16[3,128,2048]{1,0,2:T(4,128)(2,1)} %copy.46), calls=%async_computation | async-start | bytes 4194304 | tf_op jit(solution)/shard_map/all_to_all | solution.py:21
  12.8 0.1 copy.55
  12.9 0.1 eq.29
  13.1 0.1 copy.57
  13.2 0.2 fusion.45
  13.5 0.8 dynamic_slice.11
  14.2 0.6 dynamic_slice.10
  14.8 29.0 %all-to-all-done = bf16[3,128,2048]{1,0,2:T(4,128)(2,1)S(1)} async-done(((bf16[3,128,2048]{1,0,2:T(4,128)(2,1)}), bf16[3,128,2048]{1,0,2:T(4,128)(2,1)S(1)}, u32[]{:S(2)}, u32[]{:S(2)}) %all-to-all-start) | async-done | bytes 1572896 | tf_op jit(solution)/shard_map/all_to_all | solution.py:21
  43.8 1.3 copy.66
  45.1 0.3 fusion.58
  45.3 0.2 reshape_reshape_squeeze.3
  45.6 0.5 copy.48
  46.1 0.2 reshape_squeeze.4
  46.3 46.7 %while.10 = (s32[]{:T(128)}, bf16[4,512,128]{2,1,0:T(8,128)(2,1)}, bf16[4,512,2,64]{1,3,2,0:T(8,128)(2,1)S(1)}, bf16[2048,2,64]{0,2,1:T(8,128)(2,1)S(1)}, f32[]{...) while((s32[]{:T(128)}, bf16[4,512,128]{2,1,0:T(8,128)(2,1)}, ...), condition=%wide.region_4.5_spmd, body=%wide.region_0.4_spmd.sunk | while | flops 548801024 | bytes 35931228 | solution.py:85
  46.4 4.9 %fusion.74 = (f32[2,512]{1,0:T(2,128)S(1)}, f32[2,512,2048]{2,1,0:T(8,128)}) fusion(bf16[2048,2,64]{0,2,1:T(8,128)(2,1)S(1)} %get-tuple-element.157, bf16[4,512,2,64]{1,3,2,0:T(8,128)(2,1)S(1)} %get-tuple-element.156, s32[]{:T(128)} %get-tuple-element.146), kind=kOutput, calls=%fused_computation.69.clone.1 | convolution fusion | flops 274728960 | bytes 9048068 | tf_op jit(solution)/shard_map/while/body/eval_jaxpr/sub | solution.py:79
  51.3 4.4 %broadcast_divide_fusion.2 = f32[2,512,2048]{2,1,0:T(8,128)S(1)} fusion(f32[2,512,2048]{2,1,0:T(8,128)} %get-tuple-element.134, f32[2,512]{1,0:T(2,128)S(1)} %get-tuple-element.135), kind=kLoop, calls=%fused_computation.10.clone.1 | loop fusion | flops 2097152 | bytes 16781312 | tf_op jit(solution)/shard_map/while/body/eval_jaxpr/div | solution.py:79
  55.7 1.4 multiply_reduce_fusion.5
  57.3 0.1 copy.68
  57.4 0.7 constant_dynamic-update-slice_fusion.2
  58.0 4.9 %fusion.74 = (f32[2,512]{1,0:T(2,128)S(1)}, f32[2,512,2048]{2,1,0:T(8,128)}) fusion(bf16[2048,2,64]{0,2,1:T(8,128)(2,1)S(1)} %get-tuple-element.157, bf16[4,512,2,64]{1,3,2,0:T(8,128)(2,1)S(1)} %get-tuple-element.156, s32[]{:T(128)} %get-tuple-element.146), kind=kOutput, calls=%fused_computation.69.clone.1 | convolution fusion | flops 274728960 | bytes 9048068 | tf_op jit(solution)/shard_map/while/body/eval_jaxpr/sub | solution.py:79
  63.0 4.4 %broadcast_divide_fusion.2 = f32[2,512,2048]{2,1,0:T(8,128)S(1)} fusion(f32[2,512,2048]{2,1,0:T(8,128)} %get-tuple-element.134, f32[2,512]{1,0:T(2,128)S(1)} %get-tuple-element.135), kind=kLoop, calls=%fused_computation.10.clone.1 | loop fusion | flops 2097152 | bytes 16781312 | tf_op jit(solution)/shard_map/while/body/eval_jaxpr/div | solution.py:79
  67.4 1.4 multiply_reduce_fusion.5
  68.9 0.1 copy.68
  69.0 0.7 constant_dynamic-update-slice_fusion.2
  69.7 4.9 %fusion.74 = (f32[2,512]{1,0:T(2,128)S(1)}, f32[2,512,2048]{2,1,0:T(8,128)}) fusion(bf16[2048,2,64]{0,2,1:T(8,128)(2,1)S(1)} %get-tuple-element.157, bf16[4,512,2,64]{1,3,2,0:T(8,128)(2,1)S(1)} %get-tuple-element.156, s32[]{:T(128)} %get-tuple-element.146), kind=kOutput, calls=%fused_computation.69.clone.1 | convolution fusion | flops 274728960 | bytes 9048068 | tf_op jit(solution)/shard_map/while/body/eval_jaxpr/sub | solution.py:79
  74.6 4.4 %broadcast_divide_fusion.2 = f32[2,512,2048]{2,1,0:T(8,128)S(1)} fusion(f32[2,512,2048]{2,1,0:T(8,128)} %get-tuple-element.134, f32[2,512]{1,0:T(2,128)S(1)} %get-tuple-element.135), kind=kLoop, calls=%fused_computation.10.clone.1 | loop fusion | flops 2097152 | bytes 16781312 | tf_op jit(solution)/shard_map/while/body/eval_jaxpr/div | solution.py:79
  79.0 1.4 multiply_reduce_fusion.5
  80.6 0.1 copy.68
  80.7 0.7 constant_dynamic-update-slice_fusion.2
  81.4 4.9 %fusion.74 = (f32[2,512]{1,0:T(2,128)S(1)}, f32[2,512,2048]{2,1,0:T(8,128)}) fusion(bf16[2048,2,64]{0,2,1:T(8,128)(2,1)S(1)} %get-tuple-element.157, bf16[4,512,2,64]{1,3,2,0:T(8,128)(2,1)S(1)} %get-tuple-element.156, s32[]{:T(128)} %get-tuple-element.146), kind=kOutput, calls=%fused_computation.69.clone.1 | convolution fusion | flops 274728960 | bytes 9048068 | tf_op jit(solution)/shard_map/while/body/eval_jaxpr/sub | solution.py:79
  86.3 4.4 %broadcast_divide_fusion.2 = f32[2,512,2048]{2,1,0:T(8,128)S(1)} fusion(f32[2,512,2048]{2,1,0:T(8,128)} %get-tuple-element.134, f32[2,512]{1,0:T(2,128)S(1)} %get-tuple-element.135), kind=kLoop, calls=%fused_computation.10.clone.1 | loop fusion | flops 2097152 | bytes 16781312 | tf_op jit(solution)/shard_map/while/body/eval_jaxpr/div | solution.py:79
  90.7 1.4 multiply_reduce_fusion.5
  92.3 0.1 copy.68
  92.4 0.7 constant_dynamic-update-slice_fusion.2
  93.1 3.5 %all-to-all-start.1 = ((bf16[4,4,1,128,128]{4,3,1,2,0:T(8,128)(2,1)}), bf16[4,4,1,128,128]{4,3,1,2,0:T(8,128)(2,1)S(1)}, u32[]{:S(2)}, u32[]{:S(2)}) async-start(bf16[4,4,1,128,128]{4,3,1,2,0:T(8,128)(2,1)} %bitcast.8), calls=%async_computation.1 | async-start | bytes 1048576 | tf_op jit(solution)/shard_map/all_to_all | solution.py:47
  96.6 0.1 eq.25
  96.7 0.1 copy.54
  96.8 0.1 mul.103
  97.0 0.2 fusion.47
  97.2 6.8 %all-to-all-done.1 = bf16[4,4,1,128,128]{4,3,1,2,0:T(8,128)(2,1)S(1)} async-done(((bf16[4,4,1,128,128]{4,3,1,2,0:T(8,128)(2,1)}), bf16[4,4,1,128,128]{4,3,1,2,0:T(8,128)(2,1)S(1)}, u32[]{:S(2)}, u32[]{:S(2)}) %all-to-all-start.1) | async-done | bytes 524320 | tf_op jit(solution)/shard_map/all_to_all | solution.py:47
  104.0 0.8 copy.51
  104.8 3.5 %all-to-all-start.2 = ((bf16[4,4,1,128,128]{4,3,0,2,1:T(8,128)(2,1)}), bf16[4,4,1,128,128]{4,3,0,2,1:T(8,128)(2,1)S(1)}, u32[]{:S(2)}, u32[]{:S(2)}) async-start(bf16[4,4,1,128,128]{4,3,0,2,1:T(8,128)(2,1)} %copy.51), calls=%async_computation.2 | async-start | bytes 1048576 | tf_op jit(solution)/shard_map/all_to_all | solution.py:47
  108.3 1.4 scatter_custom_fusion
  109.8 5.5 %all-to-all-done.2 = bf16[4,4,1,128,128]{4,3,0,2,1:T(8,128)(2,1)S(1)} async-done(((bf16[4,4,1,128,128]{4,3,0,2,1:T(8,128)(2,1)}), bf16[4,4,1,128,128]{4,3,0,2,1:T(8,128)(2,1)S(1)}, u32[]{:S(2)}, u32[]{:S(2)}) %all-to-all-start.2) | async-done | bytes 524320 | tf_op jit(solution)/shard_map/all_to_all | solution.py:47
  115.3 0.3 copy.53
  115.6 4.7 %multiply_reduce_fusion.3 = (f32[128]{0:T(128)S(1)}, f32[128,2048]{1,0:T(8,128)S(1)}) fusion(bf16[128,2048]{0,1:T(8,128)(2,1)S(1)} %bitcast.118, bf16[2048,2048]{1,0:T(8,128)(2,1)} %param.21, bf16[1,128,2048]{2,1,0:T(8,128)(2,1)S(1)} %copy-done.1), kind=kOutput, calls=%fused_computation.44 | convolution fusion | flops 1075314560 | bytes 10486272 | tf_op jit(solution)/shard_map/dot_general | solution.py:116
  120.3 0.2 multiply_convert_fusion.2
  120.6 3.3 %gather_fusion = bf16[512,2048]{1,0:T(8,128)(2,1)} fusion(bf16[129,2048]{1,0:T(8,128)(2,1)S(1)} %concatenate.7, s32[1024]{0:T(1024)S(1)} %pad_clamp_fusion.1), kind=kCustom, calls=%fused_computation | custom fusion | bytes 4196352 | tf_op jit(solution)/shard_map/gather | solution.py:136
  123.9 2.7 %reshape_transpose_transpose_reshape_reshape_reshape_reshape.3 = bf16[128,1,1,4,2048]{4,3,0,2,1:T(4,128)(2,1)S(1)} reshape(bf16[512,2048]{1,0:T(8,128)(2,1)} %gather_fusion) | data formatting | bytes 4194304 | tf_op jit(solution)/shard_map/reshape;transpose;transpose;reshape;reshape;reshape;reshape | solution.py:61
  126.6 39.5 %all_to_all.35 = bf16[128,1,1,4,2048]{4,3,2,1,0:T(4,128)(2,1)} all-to-all(bf16[128,1,1,4,2048]{4,3,2,1,0:T(4,128)(2,1)S(1)} %bitcast.115), channel_id=1, replica_groups=mesh['sp_0'=4,'sp_1'=4,'dp'=8] {'sp_0','sp_1','dp'}, dimensions={0} | all-to-all | bytes 4194304 | tf_op jit(solution)/shard_map/all_to_all | solution.py:62
  166.2 2.5 %reshape_reshape.6 = bf16[512,2048]{1,0:T(8,128)(2,1)S(1)} reshape(bf16[16,8,1,4,2048]{4,3,1,0,2:T(4,128)(2,1)} %bitcast.116) | data formatting | bytes 4194304 | tf_op jit(solution)/shard_map/reshape;reshape | solution.py:139
  168.7 5.8 %fusion.33 = f32[512,1024]{1,0:T(8,128)} fusion(bf16[512,2048]{1,0:T(8,128)(2,1)S(1)} %reshape_reshape.6, bf16[1,2048,1024]{2,1,0:T(8,128)(2,1)} %param.25), kind=kOutput, calls=%fused_computation.32 | convolution fusion | flops 2147483648 | bytes 8388608 | tf_op jit(solution)/shard_map/dot_general | solution.py:140
  174.5 10.0 %fusion.35 = bf16[512,2048]{1,0:T(8,128)(2,1)} fusion(bf16[1,1024,2048]{2,1,0:T(8,128)(2,1)} %param.27, f32[512,1024]{1,0:T(8,128)} %fusion.33, bf16[512,2048]{1,0:T(8,128)(2,1)S(1)} %reshape_reshape.6, bf16[1,2048,1024]{2,1,0:T(8,128)(2,1)} %param.26), kind=kOutput, calls=%fused_computation.34 | convolution fusion | flops 4299161600 | bytes 14680064 | tf_op jit(solution)/shard_map/dot_general | solution.py:143
  184.5 4.1 %reshape_transpose_transpose_reshape_reshape_reshape.3 = bf16[128,1,1,4,2048]{4,3,0,2,1:T(4,128)(2,1)} reshape(bf16[512,2048]{1,0:T(8,128)(2,1)} %fusion.35) | data formatting | bytes 4194304 | tf_op jit(solution)/shard_map/reshape;transpose;transpose;reshape;reshape;reshape | solution.py:61
  188.6 4.5 %all-to-all-start.4 = ((bf16[128,1,1,4,2048]{4,3,2,1,0:T(4,128)(2,1)}), bf16[128,1,1,4,2048]{4,3,2,1,0:T(4,128)(2,1)S(1)}, u32[]{:S(2)}, u32[]{:S(2)}) async-start(bf16[128,1,1,4,2048]{4,3,2,1,0:T(4,128)(2,1)} %bitcast.114), calls=%async_computation.4 | async-start | bytes 4194304 | tf_op jit(solution)/shard_map/all_to_all | solution.py:62
  193.3 30.5 %all-to-all-done.4 = bf16[128,1,1,4,2048]{4,3,2,1,0:T(4,128)(2,1)S(1)} async-done(((bf16[128,1,1,4,2048]{4,3,2,1,0:T(4,128)(2,1)}), bf16[128,1,1,4,2048]{4,3,2,1,0:T(4,128)(2,1)S(1)}, u32[]{:S(2)}, u32[]{:S(2)}) %all-to-all-start.4) | async-done | bytes 2097184 | tf_op jit(solution)/shard_map/all_to_all | solution.py:62
  223.8 1.3 copy-done
  225.1 2.5 %reshape_reshape.7 = bf16[512,2048]{1,0:T(8,128)(2,1)S(1)} reshape(bf16[16,8,1,4,2048]{4,3,1,0,2:T(4,128)(2,1)} %bitcast.113) | data formatting | bytes 4194304 | tf_op jit(solution)/shard_map/reshape;reshape | solution.py:147
  227.7 2.3 gather_fusion.1
  230.0 2.4 %reshape.109 = f32[128,2,2048]{2,1,0:T(2,128)S(1)} reshape(bf16[256,2048]{1,0:T(8,128)(2,1)} %gather_fusion.1) | data formatting | bytes 3145728 | tf_op jit(solution)/shard_map/convert_element_type | solution.py:148
  232.4 3.2 %multiply_reduce_fusion.2 = f32[128,2048]{1,0:T(8,128)S(1)} fusion(f32[128,2,2048]{2,1,0:T(2,128)S(1)} %reshape.109, f32[128,2]{1,0:T(8,128)S(1)} %copy.61), kind=kLoop, calls=%fused_computation.38 | loop fusion | flops 786432 | bytes 3146752 | tf_op jit(solution)/shard_map/reduce_sum | solution.py:151
  235.6 0.9 fusion.44
  (37 shorter events, 0.8 us)
Async XLA Ops:
  4.1 8.8 %copy-start.3 = (s32[1,128,2]{1,2,0:T(2,128)S(1)}, s32[1,128,2]{1,2,0:T(2,128)}, u32[]{:S(2)}) copy-start(s32[1,128,2]{1,2,0:T(2,128)} %param.23) | copy-start | bytes 3076
  4.1 10.2 %copy-start.5 = (f32[16]{0:T(128)S(1)}, f32[16]{0:T(128)}, u32[]{:S(2)}) copy-start(f32[16]{0:T(128)} %param.19) | copy-start | bytes 196
  4.1 39.7 %all-to-all-start = ((bf16[3,128,2048]{1,0,2:T(4,128)(2,1)}), bf16[3,128,2048]{1,0,2:T(4,128)(2,1)S(1)}, u32[]{:S(2)}, u32[]{:S(2)}) async-start(bf16[3,128,2048]{1,0,2:T(4,128)(2,1)} %copy.46), calls=%async_computation | async-start | bytes 4194304 | tf_op jit(solution)/shard_map/all_to_all | solution.py:21
  93.1 10.9 %all-to-all-start.1 = ((bf16[4,4,1,128,128]{4,3,1,2,0:T(8,128)(2,1)}), bf16[4,4,1,128,128]{4,3,1,2,0:T(8,128)(2,1)S(1)}, u32[]{:S(2)}, u32[]{:S(2)}) async-start(bf16[4,4,1,128,128]{4,3,1,2,0:T(8,128)(2,1)} %bitcast.8), calls=%async_computation.1 | async-start | bytes 1048576 | tf_op jit(solution)/shard_map/all_to_all | solution.py:47
  97.2 18.4 %copy-start.1 = (bf16[1,128,2048]{2,1,0:T(8,128)(2,1)S(1)}, bf16[1,128,2048]{2,1,0:T(8,128)(2,1)}, u32[]{:S(2)}) copy-start(bf16[1,128,2048]{2,1,0:T(8,128)(2,1)} %param.15) | copy-start | bytes 1572868
  104.8 10.4 %all-to-all-start.2 = ((bf16[4,4,1,128,128]{4,3,0,2,1:T(8,128)(2,1)}), bf16[4,4,1,128,128]{4,3,0,2,1:T(8,128)(2,1)S(1)}, u32[]{:S(2)}, u32[]{:S(2)}) async-start(bf16[4,4,1,128,128]{4,3,0,2,1:T(8,128)(2,1)} %copy.51), calls=%async_computation.2 | async-start | bytes 1048576 | tf_op jit(solution)/shard_map/all_to_all | solution.py:47
  115.6 4.8 %copy-start.2 = (f32[2048]{0:T(1024)S(1)}, f32[2048]{0:T(1024)}, u32[]{:S(2)}) copy-start(f32[2048]{0:T(1024)} %param.22) | copy-start | bytes 24580
  188.6 4.6 %copy-start.4 = (f32[1,128,2]{1,2,0:T(2,128)S(1)}, f32[1,128,2]{1,2,0:T(2,128)}, u32[]{:S(2)}) copy-start(f32[1,128,2]{1,2,0:T(2,128)} %param.24) | copy-start | bytes 3076
  188.6 35.2 %all-to-all-start.4 = ((bf16[128,1,1,4,2048]{4,3,2,1,0:T(4,128)(2,1)}), bf16[128,1,1,4,2048]{4,3,2,1,0:T(4,128)(2,1)S(1)}, u32[]{:S(2)}, u32[]{:S(2)}) async-start(bf16[128,1,1,4,2048]{4,3,2,1,0:T(4,128)(2,1)} %bitcast.114), calls=%async_computation.4 | async-start | bytes 4194304 | tf_op jit(solution)/shard_map/all_to_all | solution.py:62
  223.8 1.4 copy-start
where the time goes:
time: 237 us
  waiting for transfers between devices  71.7 us (30%)
  matrix products  45.9 us (19%)
  blocking collectives  39.5 us (17%)
  local copies, waits for them, and re-layouts  34.4 us (15%)
  other arithmetic  24.3 us (10%)
  starting transfers between devices  20.2 us (9%)
    all_to_all x1, blocking collectives, exchange_both(): lax.all_to_all(blocks, axis, split_axis=0, concat_axis=0, tiled=True)  39.5 us
    all_to_all x1, waiting for transfers between devices, exchange_both(): lax.all_to_all(blocks, axis, split_axis=0, concat_axis=0, tiled=True)  30.5 us
    all_to_all x1, waiting for transfers between devices, side_by_side(): lax.all_to_all(both, axis, split_axis=split_dim, concat_axis=concat_dim,...  29 us
    sub x4, matrix products, one_block(): probabilities = jax.nn.softmax(scores, axis=-1)  19.6 us
    div x4, other arithmetic, one_block(): probabilities = jax.nn.softmax(scores, axis=-1)  17.6 us
    all_to_all x2, waiting for transfers between devices, exchange_in_order(): lax.all_to_all(blocks, axes[k], split_axis=k, concat_axis=k, tiled=True)  12.3 us
    dot_general x1, matrix products, on_device(): jnp.dot(hidden, expert_down[0], preferred_element_type=jnp.float32)  9.95 us
    all_to_all x1, starting transfers between devices, side_by_side(): lax.all_to_all(both, axis, split_axis=split_dim, concat_axis=concat_dim,...  8.72 us
  transfers between devices with their start and end apart: 4, of which 4 were waited for; matrix products, arithmetic and copies ran while one was open for 2% of the time, Pallas kernels for 0%

commit v1 on v0

--- a/solution.py
+++ b/solution.py
@@ -1,6 +1,10 @@
+import math
+
 import jax
 import jax.numpy as jnp
 from jax import lax
+from jax.experimental import pallas as pl
+from jax.experimental.pallas import tpu as pltpu
 from jax.sharding import Mesh
 from jax.sharding import PartitionSpec as P
 
@@ -15,19 +19,6 @@
 eps = 1e-06
 
 
-def side_by_side(arrays, axis, split_dim, concat_dim, along):
-    both = jnp.concatenate(arrays, axis=along)
-    whole, at, finished = (
-        lax.all_to_all(both, axis, split_axis=split_dim, concat_axis=concat_dim, tiled=True),
-        0,
-        [],
-    )
-    for a in arrays:
-        finished.append(lax.slice_in_dim(whole, at, at + a.shape[along], axis=along))
-        at += a.shape[along]
-    return tuple(finished)
-
-
 def in_blocks(value, dim, size):
     lengths = value.shape
     blocks = value.reshape(*lengths[:dim], size, lengths[dim] // size, *lengths[dim + 1 :])
@@ -38,19 +29,6 @@
     blocks = jnp.moveaxis(blocks, 0, dim)
     lengths = blocks.shape
     return blocks.reshape(*lengths[:dim], lengths[dim] * lengths[dim + 1], *lengths[dim + 2 :])
-
-
-def exchange_in_order(blocks, axes, sequence):
-    lengths = [lax.axis_size(a) for a in axes]
-    blocks = blocks.reshape(*lengths, *blocks.shape[1:])
-    for k in sequence:
-        blocks = lax.all_to_all(blocks, axes[k], split_axis=k, concat_axis=k, tiled=True)
-    return blocks.reshape(-1, *blocks.shape[len(axes) :])
-
-
-def one_axis_at_a_time(value, axes, sequence, split_dim, concat_dim):
-    blocks = in_blocks(value, split_dim, lax.axis_size(axes))
-    return laid_out(exchange_in_order(blocks, axes, sequence), concat_dim)
 
 
 def exchange_both(value, axis, axes, splits, concats):
@@ -64,25 +42,73 @@
     return laid_out(blocks, concats[1])
 
 
-def attend_head(query_head, key_head, value_head, lam_head, gain_head):
-    length = query_head.shape[0]
-    block_rows = min(512, length)
-    count_blocks = length // block_rows
-    scaling = query_head.shape[-1] ** (-0.5)
-    query_blocks = query_head.reshape(count_blocks, block_rows, 2, query_head.shape[-1])
+EXP_SCALE = HD ** (-0.5) * math.log2(math.e)
+LAST_DIMS = (((1,), (1,)), ((), ()))
+ATT_BLOCKS = 2
 
-    def one_block(query_block):
-        scores = (
-            jnp.einsum("qmd,kmd->mqk", query_block, key_head, preferred_element_type=jnp.float32)
-            * scaling
+
+def attention_kernel(lam_ref, qkv_ref, gain_ref, out_ref, values_ref, scores_ref):
+    sources, _, tokens, width = qkv_ref.shape
+    length = sources * tokens
+    rows = ATT_BLOCKS * tokens
+    steps = sources // ATT_BLOCKS
+    values_ref[:, :VD] = qkv_ref[:, 2].reshape(length, width)
+    values_ref[:, VD:] = jnp.ones((length, VD), jnp.bfloat16)
+
+    def scores(step, slot):
+        keys = qkv_ref[:, 1].reshape(length, width)
+        query = qkv_ref[pl.ds(step * ATT_BLOCKS, ATT_BLOCKS), 0].reshape(rows, width)
+        lane = lax.broadcasted_iota(jnp.int32, query.shape, 1)
+        zero = jnp.zeros_like(query)
+        both = jnp.concatenate(
+            [jnp.where(lane < HD, query, zero), jnp.where(lane < HD, zero, query)], axis=0
         )
-        probabilities = jax.nn.softmax(scores, axis=-1)
-        mixed_map = (probabilities[0] - lam_head * probabilities[1]).astype(jnp.bfloat16)
-        head_out = jnp.dot(mixed_map, value_head, preferred_element_type=jnp.float32)
+        scores_ref[slot] = lax.dot_general(
+            both, keys, LAST_DIMS, preferred_element_type=jnp.float32
+        )
+
+    def attend(step, slot):
+        score = scores_ref[slot]
+        top = jnp.max(score, axis=-1, keepdims=True)
+        weight = jnp.exp2((score - top) * EXP_SCALE).astype(jnp.bfloat16)
+        summed = jnp.dot(weight, values_ref[...], preferred_element_type=jnp.float32)
+        first, second = summed[:rows], summed[rows:]
+        head_out = first[:, :VD] / first[:, VD:] - lam_ref[0] * (second[:, :VD] / second[:, VD:])
         normed = head_out * lax.rsqrt(jnp.mean(head_out * head_out, axis=-1, keepdims=True) + eps)
-        return (normed * gain_head * 0.8).astype(jnp.bfloat16)
+        out_ref[pl.ds(step * ATT_BLOCKS, ATT_BLOCKS)] = (
+            (normed * gain_ref[...] * 0.8).astype(jnp.bfloat16).reshape(ATT_BLOCKS, tokens, VD)
+        )
 
-    return lax.map(one_block, query_blocks).reshape(length, value_head.shape[-1])
+    scores(0, 0)
+
+    def pair(index, carry):
+        scores(2 * index + 1, 1)
+        attend(2 * index, 0)
+        scores(2 * index + 2, 0)
+        attend(2 * index + 1, 1)
+        return carry
+
+    lax.fori_loop(0, steps // 2 - 1, pair, 0)
+    scores(steps - 1, 1)
+    attend(steps - 2, 0)
+    attend(steps - 1, 1)
+
+
+def attention(lam, qkv, gain):
+    sources, _, tokens, width = qkv.shape
+    length = sources * tokens
+    in_vmem = pl.BlockSpec(memory_space=pltpu.VMEM)
+    return pl.pallas_call(
+        attention_kernel,
+        in_specs=[pl.BlockSpec(memory_space=pltpu.SMEM), in_vmem, in_vmem],
+        out_specs=in_vmem,
+        out_shape=jax.ShapeDtypeStruct((sources, tokens, VD), jnp.bfloat16),
+        scratch_shapes=[
+            pltpu.VMEM((length, 2 * VD), jnp.bfloat16),
+            pltpu.VMEM((2, 2 * ATT_BLOCKS * tokens, length), jnp.float32),
+        ],
+        name="attention",
+    )(lam, qkv, gain)
 
 
 def on_device(
@@ -102,18 +128,17 @@
 ):
     count_sp = lax.axis_size(SP)
     count_dp = lax.axis_size("dp")
-    heads_here = HEADS // count_sp
-    queries, keys_all, values_all = side_by_side((query_maps, key_maps, value_rows), SP, 2, 1, 0)
-    first_head = lax.axis_index(SP) * heads_here
-    lam_here = lax.dynamic_slice_in_dim(lambdas, first_head, heads_here)
-    gain_here = lax.dynamic_slice_in_dim(head_gain, first_head * VD, heads_here * VD)
-    query_head = queries[0, :, 0 : 2 * HD].reshape(-1, 2, HD)
-    key_head = keys_all[0, :, 0 : 2 * HD].reshape(-1, 2, HD)
-    value_head = values_all[0, :, 0:VD]
-    outputs = attend_head(query_head, key_head, value_head, lam_here[0], gain_here)
-    attended = outputs[None]
-    returned_heads = one_axis_at_a_time(attended, SP, (0, 1), 1, 2)
-    projected = jnp.dot(returned_heads[0], out_weight, preferred_element_type=jnp.float32)
+    tokens = residual.shape[1]
+    packed = jnp.stack([query_maps[0], key_maps[0], value_rows[0]])
+    packed = packed.reshape(3, tokens, count_sp, VD).transpose(2, 0, 1, 3)
+    qkv = lax.all_to_all(packed, SP, split_axis=0, concat_axis=0, tiled=True)
+    head = lax.axis_index(SP)
+    lam_here = lax.dynamic_slice_in_dim(lambdas, head, 1)
+    gain_here = lax.dynamic_slice_in_dim(head_gain, head * VD, VD)[None]
+    attended = attention(lam_here, qkv, gain_here)
+    returned = lax.all_to_all(attended, SP, split_axis=0, concat_axis=0, tiled=True)
+    returned_heads = returned.transpose(1, 0, 2).reshape(tokens, HEADS * VD)
+    projected = jnp.dot(returned_heads, out_weight, preferred_element_type=jnp.float32)
     residual_mid = (residual[0].astype(jnp.float32) + projected).astype(jnp.bfloat16)
     middle = residual_mid.astype(jnp.float32)
     expert_input = (

time: 237 us -> 187 us (0.79)
  matrix products: 45.9 us -> 20.6 us
  other arithmetic: 24.3 us -> 4.93 us
  Pallas kernels: 0 us -> 14.2 us
  waiting for transfers between devices: 71.7 us -> 59.5 us
  local copies, waits for them, and re-layouts: 34.4 us -> 31.1 us
  starting transfers between devices: 20.2 us -> 17.7 us
    sub x4 -> x0, matrix products: 19.6 us -> none  [one_block(): probabilities = jax.nn.softmax(scores, axis=-1)]
    div x4 -> x0, other arithmetic: 17.6 us -> none  [one_block(): probabilities = jax.nn.softmax(scores, axis=-1)]
    pallas_call x0 -> x1, Pallas kernels: none -> 14.2 us  [attention(): pl.pallas_call(attention_kernel, in_specs=[pl.BlockSpec(memory_space=pltp...]
    all_to_all x3 -> x2, waiting for transfers between devices: 41.3 us -> 29.1 us  [the longest x1 20.5 us: on_device(): qkv = lax.all_to_all(packed, SP, split_axis=0, concat_axis=0, tiled=True)]
    dot_general x5 -> x1, matrix products: 10.5 us -> 4.76 us  [on_device(): jnp.dot(returned_heads, out_weight, preferred_element_type=jnp.float32)]
    unnamed x14 -> x23, local copies, waits for them, and re-layouts: 1.49 us -> 5.61 us
    dynamic_update_slice x8 -> x0, local copies, waits for them, and re-layouts: 3.15 us -> none  [attend_head(): lax.map(one_block, query_blocks).reshape(length, value_head.shape[-1])]
    concatenate x1 -> x0, local copies, waits for them, and re-layouts: 2.54 us -> none  [side_by_side(): both = jnp.concatenate(arrays, axis=along)]
  transfers between devices with their start and end apart: 4 -> 3, of which waited for: 4 -> 3; matrix products, arithmetic and copies ran while one was open for 2% -> 2% of each run, Pallas kernels for 0% -> 0%
where the time goes in v1:
time: 187 us; the launch traced here: 186 us
  waiting for transfers between devices  59.5 us (32%)
  blocking collectives  37.8 us (20%)
  local copies, waits for them, and re-layouts  31.1 us (17%)
  matrix products  20.6 us (11%)
  starting transfers between devices  17.7 us (9%)
  Pallas kernels  14.2 us (8%)
  other arithmetic  4.93 us (3%)
    all_to_all x1, blocking collectives, exchange_both(): lax.all_to_all(blocks, axis, split_axis=0, concat_axis=0, tiled=True)  37.8 us
    all_to_all x1, waiting for transfers between devices, exchange_both(): lax.all_to_all(blocks, axis, split_axis=0, concat_axis=0, tiled=True)  30.5 us
    all_to_all x1, waiting for transfers between devices, on_device(): qkv = lax.all_to_all(packed, SP, split_axis=0, concat_axis=0, tiled=True)  20.5 us
    pallas_call x1, Pallas kernels, attention(): pl.pallas_call(attention_kernel, in_specs=[pl.BlockSpec(memory_space=pltp...  14.2 us
    dot_general x1, matrix products, on_device(): jnp.dot(hidden, expert_down[0], preferred_element_type=jnp.float32)  10 us
    all_to_all x1, starting transfers between devices, on_device(): qkv = lax.all_to_all(packed, SP, split_axis=0, concat_axis=0, tiled=True)  8.72 us
    all_to_all x1, waiting for transfers between devices, on_device(): lax.all_to_all(attended, SP, split_axis=0, concat_axis=0, tiled=True)  8.55 us
    another operation x2, local copies, waits for them, and re-layouts, exchange_both(): blocks = blocks.reshape(-1, *inside)  6.85 us
  transfers between devices with their start and end apart: 3, of which 3 were waited for; matrix products, arithmetic and copies ran while one was open for 2% of the time, Pallas kernels for 0%

profile of v1, /device:TPU:1, one launch (start us, length us, event | category | flops | bytes accessed | tf_op | source)
XLA Modules:
  0.0 186.2 jit_solution(16085159171989586430)
XLA Ops:
  0.0 0.0 copy-start
  0.0 0.0 copy-start.4
  0.0 1.4 copy.26
  1.4 1.3 copy.27
  2.7 0.0 copy-done.4
  2.7 0.3 copy.28
  3.0 0.2 pad_maximum_fusion
  3.2 1.6 copy.29
  4.8 0.0 copy-start.6
  4.8 0.0 copy-start.8
  4.8 8.7 %all-to-all-start = ((bf16[16,3,128,128]{3,2,1,0:T(8,128)(2,1)}), bf16[16,3,128,128]{3,2,1,0:T(8,128)(2,1)S(1)}, u32[]{:S(2)}, u32[]{:S(2)}) async-start(bf16[16,3,128,128]{3,2,1,0:T(8,128)(2,1)} %bitcast.2), calls=%async_computation | async-start | bytes 3145728 | tf_op jit(solution)/shard_map/all_to_all | solution.py:134
  13.5 0.0 copy-done.6
  13.5 0.1 copy.32
  13.6 0.1 eq.29
  13.8 0.1 eq.25
  13.9 0.1 copy.34
  14.0 0.2 fusion.16
  14.3 0.1 copy.31
  14.5 0.1 mul.71
  14.6 0.0 copy-done.8
  14.6 0.6 dynamic_slice.6.lam_ref
  15.2 0.0 copy-done
  15.2 0.7 dynamic-slice_bitcast_fusion.gain_ref
  15.9 0.2 fusion.18
  16.1 0.0 copy-start.3
  16.1 20.5 %all-to-all-done.qkv_ref = bf16[16,3,128,128]{3,2,1,0:T(8,128)(2,1)S(1)} async-done(((bf16[16,3,128,128]{3,2,1,0:T(8,128)(2,1)}), bf16[16,3,128,128]{3,2,1,0:T(8,128)(2,1)S(1)}, u32[]{:S(2)}, u32[]{:S(2)}) %all-to-all-start) | async-done | bytes 1572896 | tf_op jit(solution)/shard_map/all_to_all | solution.py:134
  36.6 0.0 copy-start.2
  36.6 1.2 copy-done.2
  37.7 14.2 %attention.1 = bf16[16,128,128]{2,1,0:T(8,128)(2,1)} custom-call(f32[1]{0:T(128)} %dynamic_slice.6.lam_ref, bf16[16,3,128,128]{3,2,1,0:T(8,128)(2,1)} %copy-done.2, f32[1,128]{1,0:T(1,128)} %dynamic-slice_bitcast_fusion.gain_ref), custom_call_target="tpu_custom_call" | custom-call | tf_op jit(solution)/shard_map/attention/pallas_call | solution.py:101
  51.9 4.4 %all-to-all-start.1 = ((bf16[16,128,128]{2,1,0:T(8,128)(2,1)}), bf16[16,128,128]{2,1,0:T(8,128)(2,1)S(1)}, u32[]{:S(2)}, u32[]{:S(2)}) async-start(bf16[16,128,128]{2,1,0:T(8,128)(2,1)} %attention.1), calls=%async_computation.1 | async-start | bytes 1048576 | tf_op jit(solution)/shard_map/all_to_all | solution.py:139
  56.4 1.6 scatter_custom_fusion
  58.0 8.6 %all-to-all-done.1 = bf16[16,128,128]{2,1,0:T(8,128)(2,1)S(1)} async-done(((bf16[16,128,128]{2,1,0:T(8,128)(2,1)}), bf16[16,128,128]{2,1,0:T(8,128)(2,1)S(1)}, u32[]{:S(2)}, u32[]{:S(2)}) %all-to-all-start.1) | async-done | bytes 524320 | tf_op jit(solution)/shard_map/all_to_all | solution.py:139
  66.6 0.3 copy.30
  66.9 0.0 copy-done.3
  66.9 0.0 copy-start.5
  66.9 4.8 %multiply_reduce_fusion.1 = (f32[128]{0:T(128)S(1)}, f32[128,2048]{1,0:T(8,128)S(1)}) fusion(bf16[128,2048]{0,1:T(8,128)(2,1)S(1)} %bitcast.71, bf16[2048,2048]{1,0:T(8,128)(2,1)} %param.19, bf16[1,128,2048]{2,1,0:T(8,128)(2,1)S(1)} %copy-done.3), kind=kOutput, calls=%fused_computation.18 | convolution fusion | flops 1075314560 | bytes 10486272 | tf_op jit(solution)/shard_map/dot_general | solution.py:141
  71.7 0.0 copy-done.5
  71.7 0.2 multiply_convert_fusion.1
  71.9 3.3 %gather_fusion = bf16[512,2048]{1,0:T(8,128)(2,1)} fusion(bf16[129,2048]{1,0:T(8,128)(2,1)S(1)} %concatenate.3, s32[1024]{0:T(1024)S(1)} %pad_clamp_fusion.1), kind=kCustom, calls=%fused_computation | custom fusion | bytes 4196352 | tf_op jit(solution)/shard_map/gather | solution.py:161
  75.2 2.7 %reshape_transpose_transpose_reshape_reshape_reshape_reshape.3 = bf16[128,1,1,4,2048]{4,3,0,2,1:T(4,128)(2,1)S(1)} reshape(bf16[512,2048]{1,0:T(8,128)(2,1)} %gather_fusion) | data formatting | bytes 4194304 | tf_op jit(solution)/shard_map/reshape;transpose;transpose;reshape;reshape;reshape;reshape | solution.py:39
  78.0 37.8 %all_to_all.20 = bf16[128,1,1,4,2048]{4,3,2,1,0:T(4,128)(2,1)} all-to-all(bf16[128,1,1,4,2048]{4,3,2,1,0:T(4,128)(2,1)S(1)} %bitcast.68), channel_id=1, replica_groups=mesh['sp_0'=4,'sp_1'=4,'dp'=8] {'sp_0','sp_1','dp'}, dimensions={0} | all-to-all | bytes 4194304 | tf_op jit(solution)/shard_map/all_to_all | solution.py:40
  115.8 2.5 %reshape_reshape.6 = bf16[512,2048]{1,0:T(8,128)(2,1)S(1)} reshape(bf16[16,8,1,4,2048]{4,3,1,0,2:T(4,128)(2,1)} %bitcast.69) | data formatting | bytes 4194304 | tf_op jit(solution)/shard_map/reshape;reshape | solution.py:164
  118.3 5.9 %fusion.4 = f32[512,1024]{1,0:T(8,128)} fusion(bf16[512,2048]{1,0:T(8,128)(2,1)S(1)} %reshape_reshape.6, bf16[1,2048,1024]{2,1,0:T(8,128)(2,1)} %param.23), kind=kOutput, calls=%fused_computation.7 | convolution fusion | flops 2147483648 | bytes 8388608 | tf_op jit(solution)/shard_map/dot_general | solution.py:165
  124.2 10.0 %fusion.6 = bf16[512,2048]{1,0:T(8,128)(2,1)} fusion(bf16[1,1024,2048]{2,1,0:T(8,128)(2,1)} %param.25, f32[512,1024]{1,0:T(8,128)} %fusion.4, bf16[512,2048]{1,0:T(8,128)(2,1)S(1)} %reshape_reshape.6, bf16[1,2048,1024]{2,1,0:T(8,128)(2,1)} %param.24), kind=kOutput, calls=%fused_computation.9 | convolution fusion | flops 4299161600 | bytes 14680064 | tf_op jit(solution)/shard_map/dot_general | solution.py:168
  134.2 4.1 %reshape_transpose_transpose_reshape_reshape_reshape.3 = bf16[128,1,1,4,2048]{4,3,0,2,1:T(4,128)(2,1)} reshape(bf16[512,2048]{1,0:T(8,128)(2,1)} %fusion.6) | data formatting | bytes 4194304 | tf_op jit(solution)/shard_map/reshape;transpose;transpose;reshape;reshape;reshape | solution.py:39
  138.3 0.0 copy-start.7
  138.3 4.5 %all-to-all-start.3 = ((bf16[128,1,1,4,2048]{4,3,2,1,0:T(4,128)(2,1)}), bf16[128,1,1,4,2048]{4,3,2,1,0:T(4,128)(2,1)S(1)}, u32[]{:S(2)}, u32[]{:S(2)}) async-start(bf16[128,1,1,4,2048]{4,3,2,1,0:T(4,128)(2,1)} %bitcast.67), calls=%async_computation.3 | async-start | bytes 4194304 | tf_op jit(solution)/shard_map/all_to_all | solution.py:40
  142.8 0.0 copy-done.7
  142.8 0.1 copy.38
  143.0 30.5 %all-to-all-done.3 = bf16[128,1,1,4,2048]{4,3,2,1,0:T(4,128)(2,1)S(1)} async-done(((bf16[128,1,1,4,2048]{4,3,2,1,0:T(4,128)(2,1)}), bf16[128,1,1,4,2048]{4,3,2,1,0:T(4,128)(2,1)S(1)}, u32[]{:S(2)}, u32[]{:S(2)}) %all-to-all-start.3) | async-done | bytes 2097184 | tf_op jit(solution)/shard_map/all_to_all | solution.py:40
  173.4 0.0 copy-start.1
  173.4 1.3 copy-done.1
  174.8 2.5 %reshape_reshape.7 = bf16[512,2048]{1,0:T(8,128)(2,1)S(1)} reshape(bf16[16,8,1,4,2048]{4,3,1,0,2:T(4,128)(2,1)} %bitcast.66) | data formatting | bytes 4194304 | tf_op jit(solution)/shard_map/reshape;reshape | solution.py:172
  177.3 2.3 %gather_fusion.1 = bf16[256,2048]{1,0:T(8,128)(2,1)} fusion(bf16[512,2048]{1,0:T(8,128)(2,1)S(1)} %reshape_reshape.7, s32[1024]{0:T(1024)S(1)} %pad_clamp_fusion), kind=kCustom, calls=%fused_computation.1 | custom fusion | bytes 2098176 | tf_op jit(solution)/shard_map/gather | solution.py:172
  179.7 2.4 %reshape.92 = f32[128,2,2048]{2,1,0:T(2,128)S(1)} reshape(bf16[256,2048]{1,0:T(8,128)(2,1)} %gather_fusion.1) | data formatting | bytes 3145728 | tf_op jit(solution)/shard_map/convert_element_type | solution.py:173
  182.0 3.2 %multiply_reduce_fusion = f32[128,2048]{1,0:T(8,128)S(1)} fusion(f32[128,2,2048]{2,1,0:T(2,128)S(1)} %reshape.92, f32[128,2]{1,0:T(8,128)S(1)} %copy.38), kind=kLoop, calls=%fused_computation.13 | loop fusion | flops 786432 | bytes 3146752 | tf_op jit(solution)/shard_map/reduce_sum | solution.py:176
  185.2 0.9 fusion.15
  (14 shorter events, 0.2 us)
Async XLA Ops:
  0.0 15.2 %copy-start = (f32[2048]{0:T(1024)S(1)}, f32[2048]{0:T(1024)}, u32[]{:S(2)}) copy-start(f32[2048]{0:T(1024)} %param.18) | copy-start | bytes 24580
  0.0 2.7 %copy-start.4 = (bf16[1,128,2048]{2,1,0:T(8,128)(2,1)S(1)}, bf16[1,128,2048]{2,1,0:T(8,128)(2,1)}, u32[]{:S(2)}) copy-start(bf16[1,128,2048]{2,1,0:T(8,128)(2,1)} %param.16) | copy-start | bytes 1572868
  4.8 8.7 %copy-start.6 = (s32[1,128,2]{1,2,0:T(2,128)S(1)}, s32[1,128,2]{1,2,0:T(2,128)}, u32[]{:S(2)}) copy-start(s32[1,128,2]{1,2,0:T(2,128)} %param.21) | copy-start | bytes 3076
  4.8 9.8 %copy-start.8 = (f32[16]{0:T(128)S(1)}, f32[16]{0:T(128)}, u32[]{:S(2)}) copy-start(f32[16]{0:T(128)} %param.17) | copy-start | bytes 196
  4.8 31.8 %all-to-all-start = ((bf16[16,3,128,128]{3,2,1,0:T(8,128)(2,1)}), bf16[16,3,128,128]{3,2,1,0:T(8,128)(2,1)S(1)}, u32[]{:S(2)}, u32[]{:S(2)}) async-start(bf16[16,3,128,128]{3,2,1,0:T(8,128)(2,1)} %bitcast.2), calls=%async_computation | async-start | bytes 3145728 | tf_op jit(solution)/shard_map/all_to_all | solution.py:134
  16.1 50.8 %copy-start.3 = (bf16[1,128,2048]{2,1,0:T(8,128)(2,1)S(1)}, bf16[1,128,2048]{2,1,0:T(8,128)(2,1)}, u32[]{:S(2)}) copy-start(bf16[1,128,2048]{2,1,0:T(8,128)(2,1)} %param.13) | copy-start | bytes 1572868
  36.6 1.2 copy-start.2
  51.9 14.6 %all-to-all-start.1 = ((bf16[16,128,128]{2,1,0:T(8,128)(2,1)}), bf16[16,128,128]{2,1,0:T(8,128)(2,1)S(1)}, u32[]{:S(2)}, u32[]{:S(2)}) async-start(bf16[16,128,128]{2,1,0:T(8,128)(2,1)} %attention.1), calls=%async_computation.1 | async-start | bytes 1048576 | tf_op jit(solution)/shard_map/all_to_all | solution.py:139
  66.9 4.8 %copy-start.5 = (f32[2048]{0:T(1024)S(1)}, f32[2048]{0:T(1024)}, u32[]{:S(2)}) copy-start(f32[2048]{0:T(1024)} %param.20) | copy-start | bytes 24580
  138.3 4.6 %copy-start.7 = (f32[1,128,2]{1,2,0:T(2,128)S(1)}, f32[1,128,2]{1,2,0:T(2,128)}, u32[]{:S(2)}) copy-start(f32[1,128,2]{1,2,0:T(2,128)} %param.22) | copy-start | bytes 3076
  138.3 35.1 %all-to-all-start.3 = ((bf16[128,1,1,4,2048]{4,3,2,1,0:T(4,128)(2,1)}), bf16[128,1,1,4,2048]{4,3,2,1,0:T(4,128)(2,1)S(1)}, u32[]{:S(2)}, u32[]{:S(2)}) async-start(bf16[128,1,1,4,2048]{4,3,2,1,0:T(4,128)(2,1)} %bitcast.67), calls=%async_computation.3 | async-start | bytes 4194304 | tf_op jit(solution)/shard_map/all_to_all | solution.py:40
  173.4 1.4 copy-start.1

commit v2 on v1

--- a/solution.py
+++ b/solution.py
@@ -17,29 +17,6 @@
 
 
 eps = 1e-06
-
-
-def in_blocks(value, dim, size):
-    lengths = value.shape
-    blocks = value.reshape(*lengths[:dim], size, lengths[dim] // size, *lengths[dim + 1 :])
-    return jnp.moveaxis(blocks, dim, 0)
-
-
-def laid_out(blocks, dim):
-    blocks = jnp.moveaxis(blocks, 0, dim)
-    lengths = blocks.shape
-    return blocks.reshape(*lengths[:dim], lengths[dim] * lengths[dim + 1], *lengths[dim + 2 :])
-
-
-def exchange_both(value, axis, axes, splits, concats):
-    sizes = [lax.axis_size(a) for a in axes]
-    blocks = in_blocks(value, splits[0], sizes[0])
-    blocks = jnp.moveaxis(in_blocks(blocks, splits[1] + 1, sizes[1]), 0, 1)
-    inside = blocks.shape[2:]
-    blocks = blocks.reshape(-1, *inside)
-    blocks = lax.all_to_all(blocks, axis, split_axis=0, concat_axis=0, tiled=True)
-    blocks = laid_out(blocks.reshape(*sizes, *inside), concats[0] + 1)
-    return laid_out(blocks, concats[1])
 
 
 EXP_SCALE = HD ** (-0.5) * math.log2(math.e)
@@ -109,6 +86,247 @@
         ],
         name="attention",
     )(lam, qkv, gain)
+
+
+ROW = (16, 128)
+GROUP = 16
+CAP = 4
+HALVES = 2
+CAP_HALF = CAP // HALVES
+
+
+def route_kernel(routes_ref, slot_ref, token_ref, count_ref):
+    experts = count_ref.shape[0]
+    slots = token_ref.shape[0]
+
+    def clear_count(index, carry):
+        count_ref[index] = 0
+        return carry
+
+    def clear_token(index, carry):
+        token_ref[index] = 0
+        return carry
+
+    def place(index, carry):
+        expert = routes_ref[index]
+        rank = count_ref[expert]
+        count_ref[expert] = rank + 1
+        slot = (rank // CAP_HALF) * (experts * CAP_HALF) + expert * CAP_HALF + rank % CAP_HALF
+        slot_ref[index] = slot
+        token_ref[slot] = index // 2
+        return carry
+
+    lax.fori_loop(0, experts, clear_count, 0, unroll=8)
+    lax.fori_loop(0, slots, clear_token, 0, unroll=8)
+    lax.fori_loop(0, slot_ref.shape[0], place, 0)
+
+
+def route_slots(flat_routes, experts):
+    in_smem = pl.BlockSpec(memory_space=pltpu.SMEM)
+    return pl.pallas_call(
+        route_kernel,
+        in_specs=[in_smem],
+        out_specs=[in_smem, in_smem],
+        out_shape=[
+            jax.ShapeDtypeStruct(flat_routes.shape, jnp.int32),
+            jax.ShapeDtypeStruct((experts * CAP,), jnp.int32),
+        ],
+        scratch_shapes=[pltpu.SMEM((experts,), jnp.int32)],
+        name="route_slots",
+    )(flat_routes)
+
+
+def swap_matrix():
+    size = GROUP * GROUP
+    to = lax.broadcasted_iota(jnp.int32, (size, size), 0)
+    at = lax.broadcasted_iota(jnp.int32, (size, size), 1)
+    same = (to % GROUP) * GROUP + to // GROUP == at
+    return jnp.where(same, 1.0, 0.0).astype(jnp.bfloat16)
+
+
+def rows_to_tiles(rows, swap):
+    blocks = [rows[:, 128 * j : 128 * (j + 1)] for j in range(16)]
+    stacked = jnp.concatenate(blocks, axis=0)
+    swapped = jnp.dot(swap, stacked, preferred_element_type=jnp.float32)
+    return swapped.astype(jnp.bfloat16).reshape(GROUP, *ROW)
+
+
+def tiles_to_rows(tiles, swap):
+    stacked = tiles.reshape(GROUP * GROUP, 128)
+    swapped = jnp.dot(swap, stacked, preferred_element_type=jnp.float32).astype(jnp.bfloat16)
+    return jnp.concatenate([swapped[GROUP * j : GROUP * (j + 1)] for j in range(16)], axis=1)
+
+
+def middle_kernel(
+    token_ref, heads_ref, weight_ref, residual_ref, gain_ref,
+    mid_ref, first_ref, second_ref, heads_rows, middle, tiles,
+):
+    step = pl.program_id(0)
+    width = weight_ref.shape[1]
+    tokens = middle.shape[0]
+
+    @pl.when(step == 0)
+    def _():
+        for head in range(HEADS):
+            heads_rows[:, head * VD : (head + 1) * VD] = heads_ref[head]
+
+    projected = jnp.dot(heads_rows[...], weight_ref[...], preferred_element_type=jnp.float32)
+    at = pl.multiple_of(step * width, width)
+    middle[:, pl.ds(at, width)] = (residual_ref[...].astype(jnp.float32) + projected).astype(
+        jnp.bfloat16
+    )
+
+    @pl.when(step == pl.num_programs(0) - 1)
+    def _():
+        swap = swap_matrix()
+        for group in range(tokens // GROUP):
+            rows = slice(group * GROUP, (group + 1) * GROUP)
+            mid = middle[rows, :]
+            mid_ref[rows] = rows_to_tiles(mid, swap)
+            wide = mid.astype(jnp.float32)
+            scale = lax.rsqrt(jnp.mean(wide * wide, axis=-1, keepdims=True) + eps)
+            expert_input = (wide * scale * gain_ref[...]).astype(jnp.bfloat16)
+            tiles[rows] = rows_to_tiles(expert_input, swap)
+
+        half = first_ref.shape[0]
+
+        def gather(index, carry):
+            first_ref[index] = tiles[token_ref[index]]
+            second_ref[index] = tiles[token_ref[half + index]]
+            return carry
+
+        lax.fori_loop(0, half, gather, 0, unroll=8)
+
+
+def middle_stage(slot_token, heads, out_weight, residual, gain):
+    tokens = residual.shape[0]
+    half = slot_token.shape[0] // HALVES
+    block = 512
+    whole = lambda *lengths: pl.BlockSpec(lengths, lambda i: (0,) * len(lengths))
+    return pl.pallas_call(
+        middle_kernel,
+        grid=(D // block,),
+        in_specs=[
+            pl.BlockSpec(memory_space=pltpu.SMEM),
+            whole(HEADS, tokens, VD),
+            pl.BlockSpec((HEADS * VD, block), lambda i: (0, i)),
+            pl.BlockSpec((tokens, block), lambda i: (0, i)),
+            whole(1, D),
+        ],
+        out_specs=[whole(tokens, *ROW), whole(half, *ROW), whole(half, *ROW)],
+        out_shape=[
+            jax.ShapeDtypeStruct((tokens, *ROW), jnp.bfloat16),
+            jax.ShapeDtypeStruct((half, *ROW), jnp.bfloat16),
+            jax.ShapeDtypeStruct((half, *ROW), jnp.bfloat16),
+        ],
+        scratch_shapes=[
+            pltpu.VMEM((tokens, D), jnp.bfloat16),
+            pltpu.VMEM((tokens, D), jnp.bfloat16),
+            pltpu.VMEM((tokens, *ROW), jnp.bfloat16),
+        ],
+        cost_estimate=pl.CostEstimate(
+            flops=2 * tokens * D * D, bytes_accessed=2 * D * D, transcendentals=0
+        ),
+        name="middle",
+    )(slot_token, heads, out_weight, residual, gain)
+
+
+def expert_kernel(tile_ref, gate_ref, up_ref, down_ref, out_ref, rows, total):
+    step = pl.program_id(0)
+    groups = tile_ref.shape[0] // GROUP
+
+    @pl.when(step == 0)
+    def _():
+        swap = swap_matrix()
+        for group in range(groups):
+            at = slice(group * GROUP, (group + 1) * GROUP)
+            rows[at, :] = tiles_to_rows(tile_ref[at], swap)
+
+    inputs = rows[...]
+    gate = jnp.dot(inputs, gate_ref[0], preferred_element_type=jnp.float32)
+    up = jnp.dot(inputs, up_ref[0], preferred_element_type=jnp.float32)
+    hidden = (gate / (1.0 + jnp.exp(-gate)) * up).astype(jnp.bfloat16)
+    part = jnp.dot(hidden, down_ref[0], preferred_element_type=jnp.float32)
+
+    @pl.when(step == 0)
+    def _():
+        total[...] = part
+
+    @pl.when(step > 0)
+    def _():
+        total[...] += part
+
+    @pl.when(step == pl.num_programs(0) - 1)
+    def _():
+        swap = swap_matrix()
+        for group in range(groups):
+            at = slice(group * GROUP, (group + 1) * GROUP)
+            out_ref[at] = rows_to_tiles(total[at, :].astype(jnp.bfloat16), swap)
+
+
+def expert_stage(tiles, gate, up, down):
+    count = tiles.shape[0]
+    hidden = gate.shape[2]
+    block = 256
+    whole = pl.BlockSpec((count, *ROW), lambda i: (0, 0, 0))
+    columns = pl.BlockSpec((1, D, block), lambda i: (0, 0, i))
+    return pl.pallas_call(
+        expert_kernel,
+        grid=(hidden // block,),
+        in_specs=[whole, columns, columns, pl.BlockSpec((1, block, D), lambda i: (0, i, 0))],
+        out_specs=whole,
+        out_shape=jax.ShapeDtypeStruct((count, *ROW), jnp.bfloat16),
+        scratch_shapes=[pltpu.VMEM((count, D), jnp.bfloat16), pltpu.VMEM((count, D), jnp.float32)],
+        cost_estimate=pl.CostEstimate(
+            flops=6 * count * D * hidden, bytes_accessed=6 * D * hidden, transcendentals=0
+        ),
+        name="experts",
+    )(tiles, gate, up, down)
+
+
+def combine_kernel(slot_ref, share_ref, mid_ref, first_hbm, second_hbm, out_ref, back, tiles, sems):
+    half = first_hbm.shape[0]
+    tokens = mid_ref.shape[0]
+    copies = [
+        pltpu.make_async_copy(source, back.at[pl.ds(n * half, half)], sems.at[n])
+        for n, source in enumerate((first_hbm, second_hbm))
+    ]
+    for copy in copies:
+        copy.start()
+    for copy in copies:
+        copy.wait()
+
+    def token(index, carry):
+        one = back[slot_ref[2 * index]].astype(jnp.float32) * share_ref[2 * index]
+        two = back[slot_ref[2 * index + 1]].astype(jnp.float32) * share_ref[2 * index + 1]
+        tiles[index] = (mid_ref[index].astype(jnp.float32) + (one + two)).astype(jnp.bfloat16)
+        return carry
+
+    lax.fori_loop(0, tokens, token, 0, unroll=8)
+    swap = swap_matrix()
+    for group in range(tokens // GROUP):
+        at = slice(group * GROUP, (group + 1) * GROUP)
+        out_ref[at, :] = tiles_to_rows(tiles[at], swap)
+
+
+def combine_stage(slot, shares, mid, first, second):
+    tokens = mid.shape[0]
+    half = first.shape[0]
+    in_smem = pl.BlockSpec(memory_space=pltpu.SMEM)
+    in_vmem = pl.BlockSpec(memory_space=pltpu.VMEM)
+    in_place = pl.BlockSpec(memory_space=pl.ANY)
+    return pl.pallas_call(
+        combine_kernel,
+        in_specs=[in_smem, in_smem, in_vmem, in_place, in_place],
+        out_specs=in_vmem,
+        out_shape=jax.ShapeDtypeStruct((tokens, D), jnp.bfloat16),
+        scratch_shapes=[
+            pltpu.VMEM((HALVES * half, *ROW), jnp.bfloat16),
+            pltpu.VMEM((tokens, *ROW), jnp.bfloat16),
+            pltpu.SemaphoreType.DMA((HALVES,)),
+        ],
+        name="combine",
+    )(slot, shares, mid, first, second)
 
 
 def on_device(
@@ -137,44 +355,15 @@
     gain_here = lax.dynamic_slice_in_dim(head_gain, head * VD, VD)[None]
     attended = attention(lam_here, qkv, gain_here)
     returned = lax.all_to_all(attended, SP, split_axis=0, concat_axis=0, tiled=True)
-    returned_heads = returned.transpose(1, 0, 2).reshape(tokens, HEADS * VD)
-    projected = jnp.dot(returned_heads, out_weight, preferred_element_type=jnp.float32)
-    residual_mid = (residual[0].astype(jnp.float32) + projected).astype(jnp.bfloat16)
-    middle = residual_mid.astype(jnp.float32)
-    expert_input = (
-        middle * lax.rsqrt(jnp.mean(middle * middle, axis=-1, keepdims=True) + eps) * ffn_gain
-    ).astype(jnp.bfloat16)
-    tok_rows = residual.shape[1]
     experts_all = count_sp * count_dp
-    capacity = max(2, 4 * tok_rows // experts_all)
-    flat_routes = routes[0].reshape(-1)
-    flat_weights = route_weights[0].reshape(-1)
-    onehot = (flat_routes[:, None] == jnp.arange(experts_all, dtype=jnp.int32)[None, :]).astype(
-        jnp.int32
-    )
-    before = jnp.cumsum(onehot, axis=0) - onehot
-    rank_of = jnp.sum(before * onehot, axis=1)
-    slot = flat_routes * capacity + rank_of
-    token_of = jnp.arange(flat_routes.shape[0], dtype=jnp.int32) // routes.shape[2]
-    slot_token = jnp.full((experts_all * capacity,), tok_rows, jnp.int32).at[slot].set(token_of)
-    padded_input = jnp.concatenate([expert_input, jnp.zeros((1, D), jnp.bfloat16)], axis=0)
-    buffer = padded_input[slot_token].reshape(experts_all, capacity, D)
-    shaped = buffer.reshape(count_sp, count_dp, capacity, D)
-    received = exchange_both(shaped, SP_DP, (SP, "dp"), (0, 1), (0, 1))
-    row_block = received.reshape(-1, D)
-    gate_part = jnp.dot(row_block, expert_gate[0], preferred_element_type=jnp.float32)
-    up_part = jnp.dot(row_block, expert_up[0], preferred_element_type=jnp.float32)
-    hidden = (jax.nn.silu(gate_part) * up_part).astype(jnp.bfloat16)
-    expert_out = jnp.dot(hidden, expert_down[0], preferred_element_type=jnp.float32).astype(
-        jnp.bfloat16
-    )
-    returned = exchange_both(expert_out.reshape(received.shape), SP_DP, (SP, "dp"), (0, 1), (0, 1))
-    picked = returned.reshape(experts_all * capacity, D)[slot]
-    weighted = (picked.astype(jnp.float32) * flat_weights[:, None]).reshape(
-        tok_rows, routes.shape[2], D
-    )
-    layer_out = (middle + jnp.sum(weighted, axis=1)).astype(jnp.bfloat16)
-    return layer_out[None]
+    slot, slot_token = route_slots(routes[0].reshape(-1), experts_all)
+    mid, *sent = middle_stage(slot_token, returned, out_weight, residual[0], ffn_gain[None])
+    back = []
+    for part in sent:
+        arrived = lax.all_to_all(part, SP_DP, split_axis=0, concat_axis=0, tiled=True)
+        done = expert_stage(arrived, expert_gate, expert_up, expert_down)
+        back.append(lax.all_to_all(done, SP_DP, split_axis=0, concat_axis=0, tiled=True))
+    return combine_stage(slot, route_weights[0].reshape(-1), mid, *back)[None]
 
 
 def solution(mesh):

time: 187 us -> 180 us (0.963)
  Pallas kernels: 14.2 us -> 54.4 us
  local copies, waits for them, and re-layouts: 31.1 us -> 10.4 us
  matrix products: 20.6 us -> 0 us
  blocking collectives: 37.8 us -> 26.7 us
  starting transfers between devices: 17.7 us -> 26.5 us
  other arithmetic: 4.93 us -> 0.17 us
    pallas_call x0 -> x5, Pallas kernels: none -> 40.2 us  [the longest x2 21.6 us: expert_stage(): pl.pallas_call(expert_kernel, grid=(hidden // block,), in_specs=[whole, c...]
    dot_general x3 -> x0, matrix products: 20.6 us -> none  [the longest x1 10 us: on_device(): jnp.dot(hidden, expert_down[0], preferred_element_type=jnp.float32)]
    all_to_all x1, blocking collectives: 37.8 us -> 26.7 us  [on_device(): lax.all_to_all(part, SP_DP, split_axis=0, concat_axis=0, tiled=True)]
    another operation x7 -> x2, local copies, waits for them, and re-layouts: 11.9 us -> 1.43 us  [the longest x1 0.72 us: on_device(): return combine_stage(slot, route_weights[0].reshape(-1), mid, *back)[None]]
    all_to_all x1 -> x3, starting transfers between devices: 4.54 us -> 13.3 us  [the longest x2 8.85 us: on_device(): lax.all_to_all(done, SP_DP, split_axis=0, concat_axis=0, tiled=True)]
    gather x2 -> x0, local copies, waits for them, and re-layouts: 5.7 us -> none  [the longest x1 3.35 us: on_device(): buffer = padded_input[slot_token].reshape(experts_all, capacity, D)]
    all_to_all x1, waiting for transfers between devices: 8.55 us -> 3.23 us  [on_device(): lax.all_to_all(attended, SP, split_axis=0, concat_axis=0, tiled=True)]
    all_to_all x1 -> x3, waiting for transfers between devices: 30.5 us -> 35.5 us  [the longest x2 27 us: on_device(): lax.all_to_all(done, SP_DP, split_axis=0, concat_axis=0, tiled=True)]
  transfers between devices with their start and end apart: 3 -> 5, of which waited for: 3 -> 5; matrix products, arithmetic and copies ran while one was open for 2% -> 2% of each run, Pallas kernels for 0% -> 15%
where the time goes in v2:
time: 180 us; the launch traced here: 179 us
  waiting for transfers between devices  60.6 us (34%)
  Pallas kernels  54.4 us (30%)
  blocking collectives  26.7 us (15%)
  starting transfers between devices  26.5 us (15%)
  local copies, waits for them, and re-layouts  10.4 us (6%)
    all_to_all x2, waiting for transfers between devices, on_device(): lax.all_to_all(done, SP_DP, split_axis=0, concat_axis=0, tiled=True)  27 us
    all_to_all x1, blocking collectives, on_device(): lax.all_to_all(part, SP_DP, split_axis=0, concat_axis=0, tiled=True)  26.7 us
    all_to_all x1, waiting for transfers between devices, on_device(): qkv = lax.all_to_all(packed, SP, split_axis=0, concat_axis=0, tiled=True)  21.8 us
    pallas_call x2, Pallas kernels, expert_stage(): pl.pallas_call(expert_kernel, grid=(hidden // block,), in_specs=[whole, c...  21.6 us
    pallas_call x1, Pallas kernels, attention(): pl.pallas_call(attention_kernel, in_specs=[pl.BlockSpec(memory_space=pltp...  14.2 us
    all_to_all x2, starting transfers between devices, on_device(): lax.all_to_all(done, SP_DP, split_axis=0, concat_axis=0, tiled=True)  8.85 us
    all_to_all x1, starting transfers between devices, on_device(): qkv = lax.all_to_all(packed, SP, split_axis=0, concat_axis=0, tiled=True)  8.72 us
    all_to_all x1, waiting for transfers between devices, on_device(): lax.all_to_all(part, SP_DP, split_axis=0, concat_axis=0, tiled=True)  8.52 us
  transfers between devices with their start and end apart: 5, of which 5 were waited for; matrix products, arithmetic and copies ran while one was open for 2% of the time, Pallas kernels for 15%

profile of v2, /device:TPU:1, one launch (start us, length us, event | category | flops | bytes accessed | tf_op | source)
XLA Modules:
  0.0 179.1 jit_solution(7207991145504355366)
XLA Ops:
  0.0 0.0 copy-start
  0.0 0.0 copy-start.6
  0.0 1.4 copy.16
  1.4 1.3 copy.17
  2.7 0.0 copy-done.6
  2.7 0.3 copy.18
  3.0 0.2 pad_maximum_fusion
  3.2 1.6 copy.19
  4.8 0.0 copy-start.9
  4.8 8.7 %all-to-all-start = ((bf16[16,3,128,128]{3,2,1,0:T(8,128)(2,1)}), bf16[16,3,128,128]{3,2,1,0:T(8,128)(2,1)S(1)}, u32[]{:S(2)}, u32[]{:S(2)}) async-start(bf16[16,3,128,128]{3,2,1,0:T(8,128)(2,1)} %bitcast.1), calls=%async_computation | async-start | bytes 3145728 | tf_op jit(solution)/shard_map/all_to_all | solution.py:352
  13.5 0.0 copy-done.9
  13.5 0.6 dynamic_slice.6.lam_ref
  14.1 0.0 copy-done
  14.1 0.7 dynamic-slice_bitcast_fusion.gain_ref
  14.8 0.0 copy-start.7
  14.8 21.8 %all-to-all-done.qkv_ref = bf16[16,3,128,128]{3,2,1,0:T(8,128)(2,1)S(1)} async-done(((bf16[16,3,128,128]{3,2,1,0:T(8,128)(2,1)}), bf16[16,3,128,128]{3,2,1,0:T(8,128)(2,1)S(1)}, u32[]{:S(2)}, u32[]{:S(2)}) %all-to-all-start) | async-done | bytes 1572896 | tf_op jit(solution)/shard_map/all_to_all | solution.py:352
  36.6 0.0 copy-start.1
  36.6 1.2 copy-done.1
  37.8 14.2 %attention.1 = bf16[16,128,128]{2,1,0:T(8,128)(2,1)} custom-call(f32[1]{0:T(128)} %dynamic_slice.6.lam_ref, bf16[16,3,128,128]{3,2,1,0:T(8,128)(2,1)} %copy-done.1, f32[1,128]{1,0:T(1,128)} %dynamic-slice_bitcast_fusion.gain_ref), custom_call_target="tpu_custom_call" | custom-call | tf_op jit(solution)/shard_map/attention/pallas_call | solution.py:78
  52.0 4.4 %all-to-all-start.1 = ((bf16[16,128,128]{2,1,0:T(8,128)(2,1)}), bf16[16,128,128]{2,1,0:T(8,128)(2,1)S(1)}, u32[]{:S(2)}, u32[]{:S(2)}) async-start(bf16[16,128,128]{2,1,0:T(8,128)(2,1)} %attention.1), calls=%async_computation.1 | async-start | bytes 1048576 | tf_op jit(solution)/shard_map/all_to_all | solution.py:357
  56.4 0.0 copy-done.7
  56.4 0.1 copy.14
  56.5 0.7 reshape_squeeze.6.routes_ref
  57.3 6.1 %route_slots.1 = (s32[256]{0:T(256)}, s32[512]{0:T(512)}) custom-call(s32[256]{0:T(256)} %reshape_squeeze.6.routes_ref), custom_call_target="tpu_custom_call" | custom-call | tf_op jit(solution)/shard_map/route_slots/pallas_call | solution.py:126
  63.4 3.2 %all-to-all-done.1.heads_ref = bf16[16,128,128]{2,1,0:T(8,128)(2,1)S(1)} async-done(((bf16[16,128,128]{2,1,0:T(8,128)(2,1)}), bf16[16,128,128]{2,1,0:T(8,128)(2,1)S(1)}, u32[]{:S(2)}, u32[]{:S(2)}) %all-to-all-start.1) | async-done | bytes 524320 | tf_op jit(solution)/shard_map/all_to_all | solution.py:357
  66.6 0.0 copy-start.5
  66.6 0.8 copy-done.5
  67.4 8.2 %middle.1 = (bf16[128,16,128]{2,1,0:T(8,128)(2,1)}, bf16[256,16,128]{2,1,0:T(8,128)(2,1)}, bf16[256,16,128]{2,1,0:T(8,128)(2,1)}) custom-call(s32[512]{0:T(512)} %get-tuple-element.11.token_ref, bf16[16,128,128]{2,1,0:T(8,128)(2,1)} %copy-done.5, bf16[2048,2048]{1,0:T(8,128)(2,1)} %weight_ref.1, bf16[128,2048]{1,0:T(8,128)(2,1)} %bitcast.8, f32[1,2048]{1,0:T(1,128)} %bitcast.9), custom_call_target="tpu_custom_call" | custom-call | flops 1073741824 | bytes 8388608 | tf_op jit(solution)/shard_map/middle/pallas_call | solution.py:206
  75.6 26.7 %all_to_all.30.tile_ref = bf16[256,16,128]{2,1,0:T(8,128)(2,1)} all-to-all(bf16[256,16,128]{2,1,0:T(8,128)(2,1)} %get-tuple-element.13), channel_id=1, replica_groups=mesh['sp_0'=4,'sp_1'=4,'dp'=8] {'sp_0','sp_1','dp'}, dimensions={0} | all-to-all | bytes 2097152 | tf_op jit(solution)/shard_map/all_to_all | solution.py:363
  102.4 4.4 %all-to-all-start.4 = ((bf16[256,16,128]{2,1,0:T(8,128)(2,1)}), bf16[256,16,128]{2,1,0:T(8,128)(2,1)S(1)}, u32[]{:S(2)}, u32[]{:S(2)}) async-start(bf16[256,16,128]{2,1,0:T(8,128)(2,1)} %get-tuple-element.14), calls=%async_computation.4 | async-start | bytes 2097152 | tf_op jit(solution)/shard_map/all_to_all | solution.py:363
  106.8 10.8 %experts.2 = bf16[256,16,128]{2,1,0:T(8,128)(2,1)} custom-call(bf16[256,16,128]{2,1,0:T(8,128)(2,1)} %all_to_all.30.tile_ref, bf16[1,2048,1024]{2,1,0:T(8,128)(2,1)} %gate_ref.3, bf16[1,2048,1024]{2,1,0:T(8,128)(2,1)} %up_ref.3, bf16[1,1024,2048]{2,1,0:T(8,128)(2,1)} %down_ref.3), custom_call_target="tpu_custom_call" | custom-call | flops 3221225472 | bytes 12582912 | tf_op jit(solution)/shard_map/experts/pallas_call | solution.py:273
  117.6 8.5 %all-to-all-done.4.tile_ref = bf16[256,16,128]{2,1,0:T(8,128)(2,1)S(1)} async-done(((bf16[256,16,128]{2,1,0:T(8,128)(2,1)}), bf16[256,16,128]{2,1,0:T(8,128)(2,1)S(1)}, u32[]{:S(2)}, u32[]{:S(2)}) %all-to-all-start.4) | async-done | bytes 1048608 | tf_op jit(solution)/shard_map/all_to_all | solution.py:363
  126.1 0.0 copy-start.2
  126.1 4.4 %all-to-all-start.3 = ((bf16[256,16,128]{2,1,0:T(8,128)(2,1)}), bf16[256,16,128]{2,1,0:T(8,128)(2,1)S(1)}, u32[]{:S(2)}, u32[]{:S(2)}) async-start(bf16[256,16,128]{2,1,0:T(8,128)(2,1)} %experts.2), calls=%async_computation.3 | async-start | bytes 2097152 | tf_op jit(solution)/shard_map/all_to_all | solution.py:365
  130.5 0.0 copy-done.2
  130.6 10.8 %experts.3 = bf16[256,16,128]{2,1,0:T(8,128)(2,1)} custom-call(bf16[256,16,128]{2,1,0:T(8,128)(2,1)} %copy-done.2, bf16[1,2048,1024]{2,1,0:T(8,128)(2,1)} %gate_ref.3, bf16[1,2048,1024]{2,1,0:T(8,128)(2,1)} %up_ref.3, bf16[1,1024,2048]{2,1,0:T(8,128)(2,1)} %down_ref.3), custom_call_target="tpu_custom_call" | custom-call | flops 3221225472 | bytes 12582912 | tf_op jit(solution)/shard_map/experts/pallas_call | solution.py:273
  141.4 0.0 copy-start.8
  141.4 8.5 %all-to-all-done.3.first_hbm = bf16[256,16,128]{2,1,0:T(8,128)(2,1)S(1)} async-done(((bf16[256,16,128]{2,1,0:T(8,128)(2,1)}), bf16[256,16,128]{2,1,0:T(8,128)(2,1)S(1)}, u32[]{:S(2)}, u32[]{:S(2)}) %all-to-all-start.3) | async-done | bytes 1048608 | tf_op jit(solution)/shard_map/all_to_all | solution.py:365
  149.9 0.0 copy-start.3
  149.9 4.4 %all-to-all-start.5 = ((bf16[256,16,128]{2,1,0:T(8,128)(2,1)}), bf16[256,16,128]{2,1,0:T(8,128)(2,1)S(1)}, u32[]{:S(2)}, u32[]{:S(2)}) async-start(bf16[256,16,128]{2,1,0:T(8,128)(2,1)} %experts.3), calls=%async_computation.5 | async-start | bytes 2097152 | tf_op jit(solution)/shard_map/all_to_all | solution.py:365
  154.3 0.0 copy-done.8
  154.3 0.1 copy.15
  154.4 0.7 reshape_squeeze.7.share_ref
  155.2 18.5 %all-to-all-done.5.second_hbm = bf16[256,16,128]{2,1,0:T(8,128)(2,1)S(1)} async-done(((bf16[256,16,128]{2,1,0:T(8,128)(2,1)}), bf16[256,16,128]{2,1,0:T(8,128)(2,1)S(1)}, u32[]{:S(2)}, u32[]{:S(2)}) %all-to-all-start.5) | async-done | bytes 1048608 | tf_op jit(solution)/shard_map/all_to_all | solution.py:365
  173.6 0.0 copy-start.4
  173.6 0.0 copy-done.3
  173.6 1.0 copy-done.4
  174.6 4.3 %combine.1 = bf16[128,2048]{1,0:T(8,128)(2,1)} custom-call(s32[256]{0:T(256)} %get-tuple-element.10.slot_ref, f32[256]{0:T(256)} %reshape_squeeze.7.share_ref, bf16[128,16,128]{2,1,0:T(8,128)(2,1)} %get-tuple-element.12.mid_ref, bf16[256,16,128]{2,1,0:T(8,128)(2,1)} %copy-done.3, bf16[256,16,128]{2,1,0:T(8,128)(2,1)} %copy-done.4), custom_call_target="tpu_custom_call" | custom-call | tf_op jit(solution)/shard_map/combine/pallas_call | solution.py:318
Async XLA Ops:
  0.0 14.1 %copy-start = (f32[2048]{0:T(1024)S(1)}, f32[2048]{0:T(1024)}, u32[]{:S(2)}) copy-start(f32[2048]{0:T(1024)} %param.18) | copy-start | bytes 24580
  0.0 2.7 %copy-start.6 = (bf16[1,128,2048]{2,1,0:T(8,128)(2,1)S(1)}, bf16[1,128,2048]{2,1,0:T(8,128)(2,1)}, u32[]{:S(2)}) copy-start(bf16[1,128,2048]{2,1,0:T(8,128)(2,1)} %param.16) | copy-start | bytes 1572868
  4.8 8.7 %copy-start.9 = (f32[16]{0:T(128)S(1)}, f32[16]{0:T(128)}, u32[]{:S(2)}) copy-start(f32[16]{0:T(128)} %param.17) | copy-start | bytes 196
  4.8 31.8 %all-to-all-start = ((bf16[16,3,128,128]{3,2,1,0:T(8,128)(2,1)}), bf16[16,3,128,128]{3,2,1,0:T(8,128)(2,1)S(1)}, u32[]{:S(2)}, u32[]{:S(2)}) async-start(bf16[16,3,128,128]{3,2,1,0:T(8,128)(2,1)} %bitcast.1), calls=%async_computation | async-start | bytes 3145728 | tf_op jit(solution)/shard_map/all_to_all | solution.py:352
  14.8 41.7 %copy-start.7 = (s32[1,128,2]{1,2,0:T(2,128)S(1)}, s32[1,128,2]{1,2,0:T(2,128)}, u32[]{:S(2)}) copy-start(s32[1,128,2]{1,2,0:T(2,128)} %param.21) | copy-start | bytes 3076
  36.6 1.2 copy-start.1
  52.0 14.6 %all-to-all-start.1 = ((bf16[16,128,128]{2,1,0:T(8,128)(2,1)}), bf16[16,128,128]{2,1,0:T(8,128)(2,1)S(1)}, u32[]{:S(2)}, u32[]{:S(2)}) async-start(bf16[16,128,128]{2,1,0:T(8,128)(2,1)} %attention.1), calls=%async_computation.1 | async-start | bytes 1048576 | tf_op jit(solution)/shard_map/all_to_all | solution.py:357
  66.6 0.8 copy-start.5
  102.4 23.8 %all-to-all-start.4 = ((bf16[256,16,128]{2,1,0:T(8,128)(2,1)}), bf16[256,16,128]{2,1,0:T(8,128)(2,1)S(1)}, u32[]{:S(2)}, u32[]{:S(2)}) async-start(bf16[256,16,128]{2,1,0:T(8,128)(2,1)} %get-tuple-element.14), calls=%async_computation.4 | async-start | bytes 2097152 | tf_op jit(solution)/shard_map/all_to_all | solution.py:363
  126.1 4.4 %copy-start.2 = (bf16[256,16,128]{2,1,0:T(8,128)(2,1)}, bf16[256,16,128]{2,1,0:T(8,128)(2,1)S(1)}, u32[]{:S(2)}) copy-start(bf16[256,16,128]{2,1,0:T(8,128)(2,1)S(1)} %all-to-all-done.4.tile_ref) | copy-start | bytes 3145732
  126.1 23.8 %all-to-all-start.3 = ((bf16[256,16,128]{2,1,0:T(8,128)(2,1)}), bf16[256,16,128]{2,1,0:T(8,128)(2,1)S(1)}, u32[]{:S(2)}, u32[]{:S(2)}) async-start(bf16[256,16,128]{2,1,0:T(8,128)(2,1)} %experts.2), calls=%async_computation.3 | async-start | bytes 2097152 | tf_op jit(solution)/shard_map/all_to_all | solution.py:365
  141.4 13.0 %copy-start.8 = (f32[1,128,2]{1,2,0:T(2,128)S(1)}, f32[1,128,2]{1,2,0:T(2,128)}, u32[]{:S(2)}) copy-start(f32[1,128,2]{1,2,0:T(2,128)} %param.22) | copy-start | bytes 3076
  149.9 23.8 %copy-start.3 = (bf16[256,16,128]{2,1,0:T(8,128)(2,1)}, bf16[256,16,128]{2,1,0:T(8,128)(2,1)S(1)}, u32[]{:S(2)}) copy-start(bf16[256,16,128]{2,1,0:T(8,128)(2,1)S(1)} %all-to-all-done.3.first_hbm) | copy-start | bytes 3145732
  149.9 23.8 %all-to-all-start.5 = ((bf16[256,16,128]{2,1,0:T(8,128)(2,1)}), bf16[256,16,128]{2,1,0:T(8,128)(2,1)S(1)}, u32[]{:S(2)}, u32[]{:S(2)}) async-start(bf16[256,16,128]{2,1,0:T(8,128)(2,1)} %experts.3), calls=%async_computation.5 | async-start | bytes 2097152 | tf_op jit(solution)/shard_map/all_to_all | solution.py:365
  173.6 1.0 copy-start.4

commit v3 on v2

v3 whole, which is shorter than its diff:
```python
import math

import jax
import jax.numpy as jnp
from jax import lax
from jax.experimental import pallas as pl
from jax.experimental.pallas import tpu as pltpu
from jax.sharding import Mesh
from jax.sharding import PartitionSpec as P

D = 2048
HEADS = 16
HD = 64
VD = 128
SP = ("sp_0", "sp_1")
SP_DP = ("sp_0", "sp_1", "dp")


eps = 1e-06


def on_chip(value):
    return pltpu.with_memory_space_constraint(value, pltpu.VMEM)


def within(mebibytes):
    return pltpu.CompilerParams(vmem_limit_bytes=mebibytes * 2**20)


EXP_SCALE = HD ** (-0.5) * math.log2(math.e)
LAST_DIMS = (((1,), (1,)), ((), ()))
ATT_BLOCKS = 2


def attention_kernel(lam_ref, qkv_ref, gain_ref, out_ref, values_ref, scores_ref):
    sources, _, tokens, width = qkv_ref.shape
    length = sources * tokens
    rows = ATT_BLOCKS * tokens
    steps = sources // ATT_BLOCKS
    values_ref[:, :VD] = qkv_ref[:, 2].reshape(length, width)
    values_ref[:, VD:] = jnp.ones((length, VD), jnp.bfloat16)

    def scores(step, slot):
        keys = qkv_ref[:, 1].reshape(length, width)
        query = qkv_ref[pl.ds(step * ATT_BLOCKS, ATT_BLOCKS), 0].reshape(rows, width)
        lane = lax.broadcasted_iota(jnp.int32, query.shape, 1)
        zero = jnp.zeros_like(query)
        both = jnp.concatenate(
            [jnp.where(lane < HD, query, zero), jnp.where(lane < HD, zero, query)], axis=0
        )
        scores_ref[slot] = lax.dot_general(
            both, keys, LAST_DIMS, preferred_element_type=jnp.float32
        )

    def attend(step, slot):
        score = scores_ref[slot]
        top = jnp.max(score, axis=-1, keepdims=True)
        weight = jnp.exp2((score - top) * EXP_SCALE).astype(jnp.bfloat16)
        summed = jnp.dot(weight, values_ref[...], preferred_element_type=jnp.float32)
        first, second = summed[:rows], summed[rows:]
        head_out = first[:, :VD] / first[:, VD:] - lam_ref[0] * (second[:, :VD] / second[:, VD:])
        normed = head_out * lax.rsqrt(jnp.mean(head_out * head_out, axis=-1, keepdims=True) + eps)
        out_ref[pl.ds(step * ATT_BLOCKS, ATT_BLOCKS)] = (
            (normed * gain_ref[...] * 0.8).astype(jnp.bfloat16).reshape(ATT_BLOCKS, tokens, VD)
        )

    scores(0, 0)

    def pair(index, carry):
        scores(2 * index + 1, 1)
        attend(2 * index, 0)
        scores(2 * index + 2, 0)
        attend(2 * index + 1, 1)
        return carry

    lax.fori_loop(0, steps // 2 - 1, pair, 0)
    scores(steps - 1, 1)
    attend(steps - 2, 0)
    attend(steps - 1, 1)


def attention(lam, qkv, gain):
    sources, _, tokens, width = qkv.shape
    length = sources * tokens
    in_vmem = pl.BlockSpec(memory_space=pltpu.VMEM)
    return pl.pallas_call(
        attention_kernel,
        in_specs=[pl.BlockSpec(memory_space=pltpu.SMEM), in_vmem, in_vmem],
        out_specs=in_vmem,
        out_shape=jax.ShapeDtypeStruct((sources, tokens, VD), jnp.bfloat16),
        scratch_shapes=[
            pltpu.VMEM((length, 2 * VD), jnp.bfloat16),
            pltpu.VMEM((2, 2 * ATT_BLOCKS * tokens, length), jnp.float32),
        ],
        compiler_params=within(24),
        cost_estimate=pl.CostEstimate(
            flops=8 * length * length * VD,
            bytes_accessed=8 * length * VD,
            transcendentals=2 * length * length,
        ),
        name="attention",
    )(lam, on_chip(qkv), gain)


ROW = (16, 128)
GROUP = 16
PAIR = 2 * GROUP
CAP = 4


def pack_kernel(query_ref, key_ref, value_ref, out_ref):
    for at, ref in enumerate((query_ref, key_ref, value_ref)):
        for head in range(HEADS):
            out_ref[head, at] = ref[:, head * VD : (head + 1) * VD]


def pack_heads(query, key, value):
    in_vmem = pl.BlockSpec(memory_space=pltpu.VMEM)
    return pl.pallas_call(
        pack_kernel,
        in_specs=[in_vmem] * 3,
        out_specs=in_vmem,
        out_shape=jax.ShapeDtypeStruct((HEADS, 3, query.shape[0], VD), jnp.bfloat16),
        compiler_params=within(8),
        name="pack_heads",
    )(*(pltpu.with_memory_space_constraint(a, pltpu.HBM) for a in (query, key, value)))


def route_kernel(routes_ref, slot_ref, token_ref, count_ref):
    experts = count_ref.shape[0]
    slots = token_ref.shape[0]

    def clear_count(index, carry):
        count_ref[index] = 0
        return carry

    def clear_token(index, carry):
        token_ref[index] = 0
        return carry

    def place(index, carry):
        expert = routes_ref[index]
        rank = count_ref[expert]
        count_ref[expert] = rank + 1
        slot = expert * CAP + rank
        slot_ref[index] = slot
        token_ref[slot] = index // 2
        return carry

    lax.fori_loop(0, experts, clear_count, 0, unroll=8)
    lax.fori_loop(0, slots, clear_token, 0, unroll=8)
    lax.fori_loop(0, slot_ref.shape[0], place, 0)


def route_slots(flat_routes, experts):
    in_smem = pl.BlockSpec(memory_space=pltpu.SMEM)
    return pl.pallas_call(
        route_kernel,
        in_specs=[in_smem],
        out_specs=[in_smem, in_smem],
        out_shape=[
            jax.ShapeDtypeStruct(flat_routes.shape, jnp.int32),
            jax.ShapeDtypeStruct((experts * CAP,), jnp.int32),
        ],
        scratch_shapes=[pltpu.SMEM((experts,), jnp.int32)],
        compiler_params=within(1),
        name="route_slots",
    )(flat_routes)


def swap_matrix():
    size = GROUP * GROUP
    to = lax.broadcasted_iota(jnp.int32, (size, size), 0)
    at = lax.broadcasted_iota(jnp.int32, (size, size), 1)
    same = (to % GROUP) * GROUP + to // GROUP == at
    return jnp.where(same, 1.0, 0.0).astype(jnp.bfloat16)


def rows_to_tiles(rows, swap):
    halves = [
        jnp.concatenate(
            [rows[at : at + GROUP, 128 * j : 128 * (j + 1)] for j in range(16)], axis=0
        )
        for at in (0, GROUP)
    ]
    both = jnp.concatenate(halves, axis=1)
    swapped = jnp.dot(swap, both, preferred_element_type=jnp.float32).astype(jnp.bfloat16)
    return swapped[:, :128].reshape(GROUP, *ROW), swapped[:, 128:].reshape(GROUP, *ROW)


def tiles_to_rows(first, second, swap):
    size = GROUP * GROUP
    both = jnp.concatenate([first.reshape(size, 128), second.reshape(size, 128)], axis=1)
    swapped = jnp.dot(swap, both, preferred_element_type=jnp.float32).astype(jnp.bfloat16)
    return [
        jnp.concatenate(
            [swapped[GROUP * j : GROUP * (j + 1), at : at + 128] for j in range(16)], axis=1
        )
        for at in (0, 128)
    ]


def pair_slices(count):
    for at in range(0, count, PAIR):
        yield slice(at, at + GROUP), slice(at + GROUP, at + PAIR)


def middle_kernel(
    token_ref, heads_ref, weight_ref, residual_ref, gain_ref,
    mid_ref, sent_ref, heads_rows, middle, tiles,
):
    tokens = middle.shape[0]
    block = 512
    for head in range(HEADS):
        heads_rows[:, head * VD : (head + 1) * VD] = heads_ref[head]
    rows = heads_rows[...]
    squares = jnp.zeros((tokens, 128), jnp.float32)
    for at in range(0, D, block):
        columns = slice(at, at + block)
        projected = jnp.dot(rows, weight_ref[:, columns], preferred_element_type=jnp.float32)
        mid = (residual_ref[:, columns].astype(jnp.float32) + projected).astype(jnp.bfloat16)
        middle[:, columns] = mid
        wide = mid.astype(jnp.float32)
        wide = wide * wide
        for lane in range(0, block, 128):
            squares = squares + wide[:, lane : lane + 128]
    scale = lax.rsqrt(jnp.sum(squares, axis=-1, keepdims=True) / D + eps)
    swap = swap_matrix()
    for one, two in pair_slices(tokens):
        both = slice(one.start, two.stop)
        mid = middle[both, :]
        mid_ref[one], mid_ref[two] = rows_to_tiles(mid, swap)
        normed = mid.astype(jnp.float32) * scale[both] * gain_ref[...]
        tiles[one], tiles[two] = rows_to_tiles(normed.astype(jnp.bfloat16), swap)

    def gather(index, carry):
        sent_ref[index] = tiles[token_ref[index]]
        return carry

    lax.fori_loop(0, sent_ref.shape[0], gather, 0, unroll=16)


def middle_stage(slot_token, heads, out_weight, residual, gain):
    tokens = residual.shape[0]
    slots = slot_token.shape[0]
    in_vmem = pl.BlockSpec(memory_space=pltpu.VMEM)
    return pl.pallas_call(
        middle_kernel,
        in_specs=[pl.BlockSpec(memory_space=pltpu.SMEM)] + [in_vmem] * 4,
        out_specs=[in_vmem] * 2,
        out_shape=[
            jax.ShapeDtypeStruct((tokens, *ROW), jnp.bfloat16),
            jax.ShapeDtypeStruct((slots, *ROW), jnp.bfloat16),
        ],
        scratch_shapes=[
            pltpu.VMEM((tokens, D), jnp.bfloat16),
            pltpu.VMEM((tokens, D), jnp.bfloat16),
            pltpu.VMEM((tokens, *ROW), jnp.bfloat16),
        ],
        compiler_params=within(16),
        cost_estimate=pl.CostEstimate(
            flops=2 * tokens * D * D, bytes_accessed=2 * D * D, transcendentals=0
        ),
        name="middle",
    )(slot_token, on_chip(heads), on_chip(out_weight), on_chip(residual), gain)


def expert_kernel(tile_ref, gate_ref, up_ref, down_ref, out_ref, rows, hidden, result):
    count = tile_ref.shape[0]
    block = 512
    swap = swap_matrix()
    for one, two in pair_slices(count):
        rows[one, :], rows[two, :] = tiles_to_rows(tile_ref[one], tile_ref[two], swap)
    inputs = rows[...]
    for at in range(0, hidden.shape[1], block):
        columns = slice(at, at + block)
        gate = jnp.dot(inputs, gate_ref[:, columns], preferred_element_type=jnp.float32)
        up = jnp.dot(inputs, up_ref[:, columns], preferred_element_type=jnp.float32)
        hidden[:, columns] = (gate / (1.0 + jnp.exp(-gate)) * up).astype(jnp.bfloat16)
    acts = hidden[...]
    for at in range(0, D, block):
        columns = slice(at, at + block)
        result[:, columns] = jnp.dot(
            acts, down_ref[:, columns], preferred_element_type=jnp.float32
        ).astype(jnp.bfloat16)
    for one, two in pair_slices(count):
        out_ref[one], out_ref[two] = rows_to_tiles(result[one.start : two.stop, :], swap)


def expert_stage(tiles, gate, up, down):
    count = tiles.shape[0]
    width = gate.shape[1]
    in_vmem = pl.BlockSpec(memory_space=pltpu.VMEM)
    return pl.pallas_call(
        expert_kernel,
        in_specs=[in_vmem] * 4,
        out_specs=in_vmem,
        out_shape=jax.ShapeDtypeStruct((count, *ROW), jnp.bfloat16),
        scratch_shapes=[
            pltpu.VMEM((count, D), jnp.bfloat16),
            pltpu.VMEM((count, width), jnp.bfloat16),
            pltpu.VMEM((count, D), jnp.bfloat16),
        ],
        compiler_params=within(24),
        cost_estimate=pl.CostEstimate(
            flops=6 * count * D * width, bytes_accessed=6 * D * width, transcendentals=0
        ),
        name="experts",
    )(on_chip(tiles), on_chip(gate), on_chip(up), on_chip(down))


def combine_kernel(slot_ref, share_ref, mid_ref, back_ref, out_ref, tiles):
    tokens = mid_ref.shape[0]

    def token(index, carry):
        one = back_ref[slot_ref[2 * index]].astype(jnp.float32) * share_ref[2 * index]
        two = back_ref[slot_ref[2 * index + 1]].astype(jnp.float32) * share_ref[2 * index + 1]
        tiles[index] = (mid_ref[index].astype(jnp.float32) + (one + two)).astype(jnp.bfloat16)
        return carry

    lax.fori_loop(0, tokens, token, 0, unroll=16)
    swap = swap_matrix()
    for one, two in pair_slices(tokens):
        out_ref[one, :], out_ref[two, :] = tiles_to_rows(tiles[one], tiles[two], swap)


def combine_stage(slot, shares, mid, back):
    tokens = mid.shape[0]
    in_smem = pl.BlockSpec(memory_space=pltpu.SMEM)
    in_vmem = pl.BlockSpec(memory_space=pltpu.VMEM)
    return pl.pallas_call(
        combine_kernel,
        in_specs=[in_smem, in_smem, in_vmem, in_vmem],
        out_specs=in_vmem,
        out_shape=jax.ShapeDtypeStruct((tokens, D), jnp.bfloat16),
        scratch_shapes=[pltpu.VMEM((tokens, *ROW), jnp.bfloat16)],
        compiler_params=within(8),
        name="combine",
    )(slot, shares, on_chip(mid), on_chip(back))


def on_device(
    residual,
    query_maps,
    key_maps,
    value_rows,
    lambdas,
    head_gain,
    out_weight,
    ffn_gain,
    routes,
    route_weights,
    expert_gate,
    expert_up,
    expert_down,
):
    count_sp = lax.axis_size(SP)
    count_dp = lax.axis_size("dp")
    packed = pack_heads(query_maps[0], key_maps[0], value_rows[0])
    qkv = lax.all_to_all(packed, SP, split_axis=0, concat_axis=0, tiled=True)
    head = lax.axis_index(SP)
    lam_here = lax.dynamic_slice_in_dim(lambdas, head, 1)
    gain_here = lax.dynamic_slice_in_dim(head_gain, head * VD, VD)[None]
    attended = attention(lam_here, qkv, gain_here)
    returned = lax.all_to_all(attended, SP, split_axis=0, concat_axis=0, tiled=True)
    experts_all = count_sp * count_dp
    slot, slot_token = route_slots(routes[0].reshape(-1), experts_all)
    mid, sent = middle_stage(slot_token, returned, out_weight, residual[0], ffn_gain[None])
    arrived = lax.all_to_all(sent, SP_DP, split_axis=0, concat_axis=0, tiled=True)
    done = expert_stage(arrived, expert_gate[0], expert_up[0], expert_down[0])
    back = lax.all_to_all(done, SP_DP, split_axis=0, concat_axis=0, tiled=True)
    return combine_stage(slot, route_weights[0].reshape(-1), mid, back)[None]


def solution(mesh):
    finer = Mesh(mesh.devices.reshape(4, 4, mesh.shape["dp"]), ("sp_0", "sp_1", "dp"))
    placed = (
        P("dp", SP, None),
        P("dp", SP, None),
        P("dp", SP, None),
        P("dp", SP, None),
        P(),
        P(),
        P(),
        P(),
        P("dp", SP, None),
        P("dp", SP, None),
        P(SP_DP, None, None),
        P(SP_DP, None, None),
        P(SP_DP, None, None),
    )
    return jax.shard_map(
        on_device, mesh=finer, in_specs=placed, out_specs=P("dp", SP, None), check_vma=False
    )
```

time: 180 us -> 153 us (0.85)
  Pallas kernels: 54.4 us -> 33.9 us
  blocking collectives: 26.7 us -> 37.7 us
  starting transfers between devices: 26.5 us -> 17.7 us
  local copies, waits for them, and re-layouts: 10.4 us -> 5.97 us
  waiting for transfers between devices: 60.6 us -> 57.5 us
    pallas_call x4, Pallas kernels: 34.1 us -> 16 us  [the longest x1 8.02 us: expert_stage(): pl.pallas_call(expert_kernel, in_specs=[in_vmem] * 4, out_specs=in_vmem,...]
    all_to_all x1, blocking collectives: 26.7 us -> 37.7 us  [on_device(): lax.all_to_all(sent, SP_DP, split_axis=0, concat_axis=0, tiled=True)]
    all_to_all x3 -> x1, starting transfers between devices: 13.3 us -> 4.54 us  [on_device(): back = lax.all_to_all(done, SP_DP, split_axis=0, concat_axis=0, tiled=True)]
    all_to_all x3 -> x1, waiting for transfers between devices: 35.5 us -> 30.3 us  [on_device(): back = lax.all_to_all(done, SP_DP, split_axis=0, concat_axis=0, tiled=True)]
    unnamed x25 -> x24, local copies, waits for them, and re-layouts: 6.14 us -> 4.98 us
  transfers between devices with their start and end apart: 5 -> 3, of which waited for: 5 -> 3; matrix products, arithmetic and copies ran while one was open for 2% -> 1% of each run, Pallas kernels for 15% -> 3%
where the time goes in v3:
time: 153 us
  waiting for transfers between devices  57.5 us (38%)
  blocking collectives  37.7 us (25%)
  Pallas kernels  33.9 us (22%)
  starting transfers between devices  17.7 us (12%)
  local copies, waits for them, and re-layouts  5.97 us (4%)
    all_to_all x1, blocking collectives, on_device(): lax.all_to_all(sent, SP_DP, split_axis=0, concat_axis=0, tiled=True)  37.7 us
    all_to_all x1, waiting for transfers between devices, on_device(): back = lax.all_to_all(done, SP_DP, split_axis=0, concat_axis=0, tiled=True)  30.3 us
    all_to_all x1, waiting for transfers between devices, on_device(): qkv = lax.all_to_all(packed, SP, split_axis=0, concat_axis=0, tiled=True)  22.3 us
    pallas_call x1, Pallas kernels, attention(): pl.pallas_call(attention_kernel, in_specs=[pl.BlockSpec(memory_space=pltp...  12.8 us
    all_to_all x1, starting transfers between devices, on_device(): qkv = lax.all_to_all(packed, SP, split_axis=0, concat_axis=0, tiled=True)  8.72 us
    pallas_call x1, Pallas kernels, expert_stage(): pl.pallas_call(expert_kernel, in_specs=[in_vmem] * 4, out_specs=in_vmem,...  8.02 us
    pallas_call x1, Pallas kernels, route_slots(): pl.pallas_call(route_kernel, in_specs=[in_smem], out_specs=[in_smem, in_s...  5.08 us
    unnamed x24, local copies, waits for them, and re-layouts  4.98 us
  transfers between devices with their start and end apart: 3, of which 3 were waited for; matrix products, arithmetic and copies ran while one was open for 1% of the time, Pallas kernels for 3%

profile of v3, /device:TPU:1, one launch (start us, length us, event | category | flops | bytes accessed | tf_op | source)
XLA Modules:
  0.0 152.9 jit_solution(995871937247066383)
XLA Ops:
  0.0 0.0 copy-start
  0.0 2.8 %pack_heads.1 = bf16[16,3,128,128]{3,2,1,0:T(8,128)(2,1)} custom-call(bf16[128,2048]{1,0:T(8,128)(2,1)} %bitcast.16, bf16[128,2048]{1,0:T(8,128)(2,1)} %bitcast.17, bf16[128,2048]{1,0:T(8,128)(2,1)} %bitcast.18), custom_call_target="tpu_custom_call" | custom-call | tf_op jit(solution)/shard_map/pack_heads/pallas_call | solution.py:119
  2.8 0.0 copy-start.10
  2.8 8.7 %all-to-all-start = ((bf16[16,3,128,128]{3,2,1,0:T(8,128)(2,1)}), bf16[16,3,128,128]{3,2,1,0:T(8,128)(2,1)S(1)}, u32[]{:S(2)}, u32[]{:S(2)}) async-start(bf16[16,3,128,128]{3,2,1,0:T(8,128)(2,1)} %pack_heads.1), calls=%async_computation | async-start | bytes 3145728 | tf_op jit(solution)/shard_map/all_to_all | solution.py:360
  11.6 0.0 copy-done.10
  11.6 0.6 dynamic_slice.6.lam_ref
  12.2 0.0 copy-done
  12.2 0.1 dynamic-slice_bitcast_fusion.gain_ref
  12.3 0.0 copy-start.8
  12.3 0.0 copy-start.3
  12.3 0.0 copy-start.4
  12.3 22.3 %all-to-all-done.qkv_ref = bf16[16,3,128,128]{3,2,1,0:T(8,128)(2,1)S(1)} async-done(((bf16[16,3,128,128]{3,2,1,0:T(8,128)(2,1)}), bf16[16,3,128,128]{3,2,1,0:T(8,128)(2,1)S(1)}, u32[]{:S(2)}, u32[]{:S(2)}) %all-to-all-start) | async-done | bytes 1572896 | tf_op jit(solution)/shard_map/all_to_all | solution.py:360
  34.6 12.8 %attention.1 = bf16[16,128,128]{2,1,0:T(8,128)(2,1)} custom-call(f32[1]{0:T(128)} %dynamic_slice.6.lam_ref, bf16[16,3,128,128]{3,2,1,0:T(8,128)(2,1)S(1)} %all-to-all-done.qkv_ref, f32[1,128]{1,0:T(1,128)S(1)} %dynamic-slice_bitcast_fusion.gain_ref), custom_call_target="tpu_custom_call" | custom-call | flops 4294967296 | bytes 2097152 | tf_op jit(solution)/shard_map/attention/pallas_call | solution.py:86
  47.4 4.4 %all-to-all-start.1 = ((bf16[16,128,128]{2,1,0:T(8,128)(2,1)}), bf16[16,128,128]{2,1,0:T(8,128)(2,1)S(1)}, u32[]{:S(2)}, u32[]{:S(2)}) async-start(bf16[16,128,128]{2,1,0:T(8,128)(2,1)} %attention.1), calls=%async_computation.1 | async-start | bytes 1048576 | tf_op jit(solution)/shard_map/all_to_all | solution.py:365
  51.9 0.0 copy-done.8
  51.9 0.1 copy.14
  52.0 0.1 reshape_squeeze.6.routes_ref
  52.2 5.1 %route_slots.1 = (s32[256]{0:T(256)S(1)}, s32[512]{0:T(512)S(1)}) custom-call(s32[256]{0:T(256)S(1)} %reshape_squeeze.6.routes_ref), custom_call_target="tpu_custom_call" | custom-call | tf_op jit(solution)/shard_map/route_slots/pallas_call | solution.py:157
  57.2 4.8 %all-to-all-done.1.heads_ref = bf16[16,128,128]{2,1,0:T(8,128)(2,1)S(1)} async-done(((bf16[16,128,128]{2,1,0:T(8,128)(2,1)}), bf16[16,128,128]{2,1,0:T(8,128)(2,1)S(1)}, u32[]{:S(2)}, u32[]{:S(2)}) %all-to-all-start.1) | async-done | bytes 524320 | tf_op jit(solution)/shard_map/all_to_all | solution.py:365
  62.1 0.0 copy-done.3
  62.1 0.0 copy-done.4
  62.1 0.0 copy-start.1
  62.1 3.4 %copy-done.1 = bf16[2048,2048]{1,0:T(8,128)(2,1)S(1)} copy-done((bf16[2048,2048]{1,0:T(8,128)(2,1)S(1)}, bf16[2048,2048]{1,0:T(8,128)(2,1)}, u32[]{:S(2)}) %copy-start.1) | copy-done | bytes 8388632
  65.5 0.0 copy-start.6
  65.5 0.0 copy-start.7
  65.5 3.1 %middle.1 = (bf16[128,16,128]{2,1,0:T(8,128)(2,1)S(1)}, bf16[512,16,128]{2,1,0:T(8,128)(2,1)S(1)}) custom-call(s32[512]{0:T(512)S(1)} %get-tuple-element.10.token_ref, bf16[16,128,128]{2,1,0:T(8,128)(2,1)S(1)} %all-to-all-done.1.heads_ref, bf16[2048,2048]{1,0:T(8,128)(2,1)S(1)} %copy-done.1, bf16[128,2048]{1,0:T(8,128)(2,1)S(1)} %bitcast.11, ...), custom_call_target="tpu_custom_call" | custom-call | flops 1073741824 | bytes 8388608 | tf_op jit(solution)/shard_map/middle/pallas_call | solution.py:247
  68.6 0.0 copy-start.5
  68.6 37.7 %all_to_all.20.tile_ref = bf16[512,16,128]{2,1,0:T(8,128)(2,1)S(1)} all-to-all(bf16[512,16,128]{2,1,0:T(8,128)(2,1)S(1)} %get-tuple-element.12), channel_id=1, replica_groups=mesh['sp_0'=4,'sp_1'=4,'dp'=8] {'sp_0','sp_1','dp'}, dimensions={0} | all-to-all | bytes 4194304 | tf_op jit(solution)/shard_map/all_to_all | solution.py:369
  106.3 0.0 copy-done.6
  106.3 0.0 copy-done.7
  106.3 0.0 copy-done.5
  106.3 8.0 %experts.1 = bf16[512,16,128]{2,1,0:T(8,128)(2,1)S(1)} custom-call(bf16[512,16,128]{2,1,0:T(8,128)(2,1)S(1)} %all_to_all.20.tile_ref, bf16[2048,1024]{1,0:T(8,128)(2,1)S(1)} %bitcast.13, bf16[2048,1024]{1,0:T(8,128)(2,1)S(1)} %bitcast.14, bf16[1024,2048]{1,0:T(8,128)(2,1)S(1)} %bitcast.15), custom_call_target="tpu_custom_call" | custom-call | flops 6442450944 | bytes 12582912 | tf_op jit(solution)/shard_map/experts/pallas_call | solution.py:294
  114.3 0.0 copy-start.2
  114.3 1.3 copy-done.2
  115.7 0.0 copy-start.9
  115.7 4.5 %all-to-all-start.3 = ((bf16[512,16,128]{2,1,0:T(8,128)(2,1)}), bf16[512,16,128]{2,1,0:T(8,128)(2,1)S(1)}, u32[]{:S(2)}, u32[]{:S(2)}) async-start(bf16[512,16,128]{2,1,0:T(8,128)(2,1)} %copy-done.2), calls=%async_computation.3 | async-start | bytes 4194304 | tf_op jit(solution)/shard_map/all_to_all | solution.py:371
  120.2 0.0 copy-done.9
  120.2 0.1 copy.15
  120.4 0.1 reshape_squeeze.7.share_ref
  120.5 30.3 %all-to-all-done.3.back_ref = bf16[512,16,128]{2,1,0:T(8,128)(2,1)S(1)} async-done(((bf16[512,16,128]{2,1,0:T(8,128)(2,1)}), bf16[512,16,128]{2,1,0:T(8,128)(2,1)S(1)}, u32[]{:S(2)}, u32[]{:S(2)}) %all-to-all-start.3) | async-done | bytes 2097184 | tf_op jit(solution)/shard_map/all_to_all | solution.py:371
  150.8 2.1 %combine.1 = bf16[128,2048]{1,0:T(8,128)(2,1)} custom-call(s32[256]{0:T(256)S(1)} %get-tuple-element.9.slot_ref, f32[256]{0:T(256)S(1)} %reshape_squeeze.7.share_ref, bf16[128,16,128]{2,1,0:T(8,128)(2,1)S(1)} %get-tuple-element.11.mid_ref, bf16[512,16,128]{2,1,0:T(8,128)(2,1)S(1)} %all-to-all-done.3.back_ref), custom_call_target="tpu_custom_call" | custom-call | tf_op jit(solution)/shard_map/combine/pallas_call | solution.py:331
Async XLA Ops:
  0.0 12.2 %copy-start = (f32[2048]{0:T(1024)S(1)}, f32[2048]{0:T(1024)}, u32[]{:S(2)}) copy-start(f32[2048]{0:T(1024)} %param.18) | copy-start | bytes 24580
  2.8 8.7 %copy-start.10 = (f32[16]{0:T(128)S(1)}, f32[16]{0:T(128)}, u32[]{:S(2)}) copy-start(f32[16]{0:T(128)} %param.17) | copy-start | bytes 196
  2.8 31.8 %all-to-all-start = ((bf16[16,3,128,128]{3,2,1,0:T(8,128)(2,1)}), bf16[16,3,128,128]{3,2,1,0:T(8,128)(2,1)S(1)}, u32[]{:S(2)}, u32[]{:S(2)}) async-start(bf16[16,3,128,128]{3,2,1,0:T(8,128)(2,1)} %pack_heads.1), calls=%async_computation | async-start | bytes 3145728 | tf_op jit(solution)/shard_map/all_to_all | solution.py:360
  12.3 39.6 %copy-start.8 = (s32[1,128,2]{1,2,0:T(2,128)S(1)}, s32[1,128,2]{1,2,0:T(2,128)}, u32[]{:S(2)}) copy-start(s32[1,128,2]{1,2,0:T(2,128)} %param.21) | copy-start | bytes 3076
  12.3 49.8 %copy-start.3 = (bf16[1,128,2048]{2,1,0:T(8,128)(2,1)S(1)}, bf16[1,128,2048]{2,1,0:T(8,128)(2,1)}, u32[]{:S(2)}) copy-start(bf16[1,128,2048]{2,1,0:T(8,128)(2,1)} %param.13) | copy-start | bytes 1572868
  12.3 49.8 %copy-start.4 = (f32[2048]{0:T(1024)S(1)}, f32[2048]{0:T(1024)}, u32[]{:S(2)}) copy-start(f32[2048]{0:T(1024)} %param.20) | copy-start | bytes 24580
  47.4 14.6 %all-to-all-start.1 = ((bf16[16,128,128]{2,1,0:T(8,128)(2,1)}), bf16[16,128,128]{2,1,0:T(8,128)(2,1)S(1)}, u32[]{:S(2)}, u32[]{:S(2)}) async-start(bf16[16,128,128]{2,1,0:T(8,128)(2,1)} %attention.1), calls=%async_computation.1 | async-start | bytes 1048576 | tf_op jit(solution)/shard_map/all_to_all | solution.py:365
  62.1 3.4 %copy-start.1 = (bf16[2048,2048]{1,0:T(8,128)(2,1)S(1)}, bf16[2048,2048]{1,0:T(8,128)(2,1)}, u32[]{:S(2)}) copy-start(bf16[2048,2048]{1,0:T(8,128)(2,1)} %weight_ref.1) | copy-start | bytes 25165828
  65.5 40.8 %copy-start.6 = (bf16[1,2048,1024]{2,1,0:T(8,128)(2,1)S(1)}, bf16[1,2048,1024]{2,1,0:T(8,128)(2,1)}, u32[]{:S(2)}) copy-start(bf16[1,2048,1024]{2,1,0:T(8,128)(2,1)} %param.24) | copy-start | bytes 12582916
  65.5 40.8 %copy-start.7 = (bf16[1,1024,2048]{2,1,0:T(8,128)(2,1)S(1)}, bf16[1,1024,2048]{2,1,0:T(8,128)(2,1)}, u32[]{:S(2)}) copy-start(bf16[1,1024,2048]{2,1,0:T(8,128)(2,1)} %param.25) | copy-start | bytes 12582916
  68.6 37.7 %copy-start.5 = (bf16[1,2048,1024]{2,1,0:T(8,128)(2,1)S(1)}, bf16[1,2048,1024]{2,1,0:T(8,128)(2,1)}, u32[]{:S(2)}) copy-start(bf16[1,2048,1024]{2,1,0:T(8,128)(2,1)} %param.23) | copy-start | bytes 12582916
  114.3 1.3 copy-start.2
  115.7 4.6 %copy-start.9 = (f32[1,128,2]{1,2,0:T(2,128)S(1)}, f32[1,128,2]{1,2,0:T(2,128)}, u32[]{:S(2)}) copy-start(f32[1,128,2]{1,2,0:T(2,128)} %param.22) | copy-start | bytes 3076
  115.7 35.1 %all-to-all-start.3 = ((bf16[512,16,128]{2,1,0:T(8,128)(2,1)}), bf16[512,16,128]{2,1,0:T(8,128)(2,1)S(1)}, u32[]{:S(2)}, u32[]{:S(2)}) async-start(bf16[512,16,128]{2,1,0:T(8,128)(2,1)} %copy-done.2), calls=%async_computation.3 | async-start | bytes 4194304 | tf_op jit(solution)/shard_map/all_to_all | solution.py:371

commit v4 on v3

--- a/solution.py
+++ b/solution.py
@@ -23,6 +23,10 @@
     return pltpu.with_memory_space_constraint(value, pltpu.VMEM)
 
 
+def off_chip(value):
+    return pltpu.with_memory_space_constraint(value, pltpu.HBM)
+
+
 def within(mebibytes):
     return pltpu.CompilerParams(vmem_limit_bytes=mebibytes * 2**20)
 
@@ -32,11 +36,17 @@
 ATT_BLOCKS = 2
 
 
-def attention_kernel(lam_ref, qkv_ref, gain_ref, out_ref, values_ref, scores_ref):
+def attention_kernel(
+    lam_ref, qkv_ref, gain_ref, weight_hbm, routed_ref,
+    out_ref, weight_ref, values_ref, scores_ref, sems,
+):
+    del routed_ref
     sources, _, tokens, width = qkv_ref.shape
     length = sources * tokens
     rows = ATT_BLOCKS * tokens
     steps = sources // ATT_BLOCKS
+    fetch = pltpu.make_async_copy(weight_hbm, weight_ref, sems.at[0])
+    fetch.start()
     values_ref[:, :VD] = qkv_ref[:, 2].reshape(length, width)
     values_ref[:, VD:] = jnp.ones((length, VD), jnp.bfloat16)
 
@@ -60,37 +70,38 @@
         first, second = summed[:rows], summed[rows:]
         head_out = first[:, :VD] / first[:, VD:] - lam_ref[0] * (second[:, :VD] / second[:, VD:])
         normed = head_out * lax.rsqrt(jnp.mean(head_out * head_out, axis=-1, keepdims=True) + eps)
-        out_ref[pl.ds(step * ATT_BLOCKS, ATT_BLOCKS)] = (
+        at = pl.ds(step * ATT_BLOCKS, ATT_BLOCKS)
+        out_ref[at] = (
             (normed * gain_ref[...] * 0.8).astype(jnp.bfloat16).reshape(ATT_BLOCKS, tokens, VD)
         )
 
     scores(0, 0)
-
-    def pair(index, carry):
-        scores(2 * index + 1, 1)
-        attend(2 * index, 0)
-        scores(2 * index + 2, 0)
-        attend(2 * index + 1, 1)
-        return carry
-
-    lax.fori_loop(0, steps // 2 - 1, pair, 0)
-    scores(steps - 1, 1)
-    attend(steps - 2, 0)
-    attend(steps - 1, 1)
-
-
-def attention(lam, qkv, gain):
+    for step in range(1, steps):
+        scores(step, step % 2)
+        attend(step - 1, (step - 1) % 2)
+    attend(steps - 1, (steps - 1) % 2)
+    fetch.wait()
+
+
+def attention(lam, qkv, gain, out_weight, routed):
     sources, _, tokens, width = qkv.shape
     length = sources * tokens
     in_vmem = pl.BlockSpec(memory_space=pltpu.VMEM)
+    in_hbm = pl.BlockSpec(memory_space=pltpu.HBM)
+    heads = (sources, tokens, VD)
     return pl.pallas_call(
         attention_kernel,
-        in_specs=[pl.BlockSpec(memory_space=pltpu.SMEM), in_vmem, in_vmem],
-        out_specs=in_vmem,
-        out_shape=jax.ShapeDtypeStruct((sources, tokens, VD), jnp.bfloat16),
+        in_specs=[pl.BlockSpec(memory_space=pltpu.SMEM), in_vmem, in_vmem, in_hbm]
+        + [pl.BlockSpec(memory_space=pl.ANY)],
+        out_specs=[in_vmem] * 2,
+        out_shape=[
+            jax.ShapeDtypeStruct(heads, jnp.bfloat16),
+            pltpu.VMEM(out_weight.shape, jnp.bfloat16),
+        ],
         scratch_shapes=[
             pltpu.VMEM((length, 2 * VD), jnp.bfloat16),
             pltpu.VMEM((2, 2 * ATT_BLOCKS * tokens, length), jnp.float32),
+            pltpu.SemaphoreType.DMA((1,)),
         ],
         compiler_params=within(24),
         cost_estimate=pl.CostEstimate(
@@ -99,7 +110,7 @@
             transcendentals=2 * length * length,
         ),
         name="attention",
-    )(lam, on_chip(qkv), gain)
+    )(lam, on_chip(qkv), gain, off_chip(out_weight), routed)
 
 
 ROW = (16, 128)
@@ -108,25 +119,47 @@
 CAP = 4
 
 
-def pack_kernel(query_ref, key_ref, value_ref, out_ref):
-    for at, ref in enumerate((query_ref, key_ref, value_ref)):
+def pack_kernel(query_ref, key_ref, value_ref, out_ref, rows, blocks, in_sems, out_sems):
+    copies_in = [
+        pltpu.make_async_copy(ref, rows.at[at], in_sems.at[at])
+        for at, ref in enumerate((query_ref, key_ref, value_ref))
+    ]
+    copies_out = [
+        pltpu.make_async_copy(blocks.at[:, at], out_ref.at[:, at], out_sems.at[at])
+        for at in range(3)
+    ]
+    for copy in copies_in:
+        copy.start()
+    for at in range(3):
+        copies_in[at].wait()
         for head in range(HEADS):
-            out_ref[head, at] = ref[:, head * VD : (head + 1) * VD]
+            blocks[head, at] = rows[at, :, head * VD : (head + 1) * VD]
+        copies_out[at].start()
+    for copy in copies_out:
+        copy.wait()
 
 
 def pack_heads(query, key, value):
-    in_vmem = pl.BlockSpec(memory_space=pltpu.VMEM)
+    tokens = query.shape[0]
+    packed = (HEADS, 3, tokens, VD)
+    in_hbm = pl.BlockSpec(memory_space=pltpu.HBM)
     return pl.pallas_call(
         pack_kernel,
-        in_specs=[in_vmem] * 3,
-        out_specs=in_vmem,
-        out_shape=jax.ShapeDtypeStruct((HEADS, 3, query.shape[0], VD), jnp.bfloat16),
+        in_specs=[in_hbm] * 3,
+        out_specs=in_hbm,
+        out_shape=pltpu.HBM(packed, jnp.bfloat16),
+        scratch_shapes=[
+            pltpu.VMEM((3, tokens, HEADS * VD), jnp.bfloat16),
+            pltpu.VMEM(packed, jnp.bfloat16),
+            pltpu.SemaphoreType.DMA((3,)),
+            pltpu.SemaphoreType.DMA((3,)),
+        ],
         compiler_params=within(8),
         name="pack_heads",
-    )(*(pltpu.with_memory_space_constraint(a, pltpu.HBM) for a in (query, key, value)))
-
-
-def route_kernel(routes_ref, slot_ref, token_ref, count_ref):
+    )(*(off_chip(a) for a in (query, key, value)))
+
+
+def route_kernel(routes_ref, shares_ref, slot_ref, token_ref, kept_ref, count_ref):
     experts = count_ref.shape[0]
     slots = token_ref.shape[0]
 
@@ -145,6 +178,7 @@
         slot = expert * CAP + rank
         slot_ref[index] = slot
         token_ref[slot] = index // 2
+        kept_ref[index] = shares_ref[index]
         return carry
 
     lax.fori_loop(0, experts, clear_count, 0, unroll=8)
@@ -152,20 +186,21 @@
     lax.fori_loop(0, slot_ref.shape[0], place, 0)
 
 
-def route_slots(flat_routes, experts):
+def route_slots(flat_routes, flat_shares, experts):
     in_smem = pl.BlockSpec(memory_space=pltpu.SMEM)
     return pl.pallas_call(
         route_kernel,
-        in_specs=[in_smem],
-        out_specs=[in_smem, in_smem],
+        in_specs=[in_smem] * 2,
+        out_specs=[in_smem] * 3,
         out_shape=[
             jax.ShapeDtypeStruct(flat_routes.shape, jnp.int32),
             jax.ShapeDtypeStruct((experts * CAP,), jnp.int32),
+            jax.ShapeDtypeStruct(flat_shares.shape, jnp.float32),
         ],
         scratch_shapes=[pltpu.SMEM((experts,), jnp.int32)],
         compiler_params=within(1),
         name="route_slots",
-    )(flat_routes)
+    )(flat_routes, flat_shares)
 
 
 def swap_matrix():
@@ -267,7 +302,7 @@
 
 def expert_kernel(tile_ref, gate_ref, up_ref, down_ref, out_ref, rows, hidden, result):
     count = tile_ref.shape[0]
-    block = 512
+    block = 256
     swap = swap_matrix()
     for one, two in pair_slices(count):
         rows[one, :], rows[two, :] = tiles_to_rows(tile_ref[one], tile_ref[two], swap)
@@ -278,8 +313,8 @@
         up = jnp.dot(inputs, up_ref[:, columns], preferred_element_type=jnp.float32)
         hidden[:, columns] = (gate / (1.0 + jnp.exp(-gate)) * up).astype(jnp.bfloat16)
     acts = hidden[...]
-    for at in range(0, D, block):
-        columns = slice(at, at + block)
+    for at in range(0, D, 1024):
+        columns = slice(at, at + 1024)
         result[:, columns] = jnp.dot(
             acts, down_ref[:, columns], preferred_element_type=jnp.float32
         ).astype(jnp.bfloat16)
@@ -309,7 +344,7 @@
     )(on_chip(tiles), on_chip(gate), on_chip(up), on_chip(down))
 
 
-def combine_kernel(slot_ref, share_ref, mid_ref, back_ref, out_ref, tiles):
+def combine_kernel(slot_ref, share_ref, mid_ref, back_ref, out_hbm, tiles, out_ref, sems):
     tokens = mid_ref.shape[0]
 
     def token(index, carry):
@@ -318,10 +353,17 @@
         tiles[index] = (mid_ref[index].astype(jnp.float32) + (one + two)).astype(jnp.bfloat16)
         return carry
 
-    lax.fori_loop(0, tokens, token, 0, unroll=16)
     swap = swap_matrix()
+    copies = []
     for one, two in pair_slices(tokens):
+        lax.fori_loop(one.start, two.stop, token, 0, unroll=PAIR)
         out_ref[one, :], out_ref[two, :] = tiles_to_rows(tiles[one], tiles[two], swap)
+        at = pl.ds(one.start, PAIR)
+        copy = pltpu.make_async_copy(out_ref.at[at], out_hbm.at[at], sems.at[len(copies)])
+        copy.start()
+        copies.append(copy)
+    for copy in copies:
+        copy.wait()
 
 
 def combine_stage(slot, shares, mid, back):
@@ -331,9 +373,13 @@
     return pl.pallas_call(
         combine_kernel,
         in_specs=[in_smem, in_smem, in_vmem, in_vmem],
-        out_specs=in_vmem,
-        out_shape=jax.ShapeDtypeStruct((tokens, D), jnp.bfloat16),
-        scratch_shapes=[pltpu.VMEM((tokens, *ROW), jnp.bfloat16)],
+        out_specs=pl.BlockSpec(memory_space=pltpu.HBM),
+        out_shape=pltpu.HBM((tokens, D), jnp.bfloat16),
+        scratch_shapes=[
+            pltpu.VMEM((tokens, *ROW), jnp.bfloat16),
+            pltpu.VMEM((tokens, D), jnp.bfloat16),
+            pltpu.SemaphoreType.DMA((tokens // PAIR,)),
+        ],
         compiler_params=within(8),
         name="combine",
     )(slot, shares, on_chip(mid), on_chip(back))
@@ -361,15 +407,17 @@
     head = lax.axis_index(SP)
     lam_here = lax.dynamic_slice_in_dim(lambdas, head, 1)
     gain_here = lax.dynamic_slice_in_dim(head_gain, head * VD, VD)[None]
-    attended = attention(lam_here, qkv, gain_here)
+    experts_all = count_sp * count_dp
+    slot, slot_token, shares = route_slots(
+        routes[0].reshape(-1), route_weights[0].reshape(-1), experts_all
+    )
+    attended, weight_here = attention(lam_here, qkv, gain_here, out_weight, slot_token)
     returned = lax.all_to_all(attended, SP, split_axis=0, concat_axis=0, tiled=True)
-    experts_all = count_sp * count_dp
-    slot, slot_token = route_slots(routes[0].reshape(-1), experts_all)
-    mid, sent = middle_stage(slot_token, returned, out_weight, residual[0], ffn_gain[None])
+    mid, sent = middle_stage(slot_token, returned, weight_here, residual[0], ffn_gain[None])
     arrived = lax.all_to_all(sent, SP_DP, split_axis=0, concat_axis=0, tiled=True)
     done = expert_stage(arrived, expert_gate[0], expert_up[0], expert_down[0])
     back = lax.all_to_all(done, SP_DP, split_axis=0, concat_axis=0, tiled=True)
-    return combine_stage(slot, route_weights[0].reshape(-1), mid, back)[None]
+    return combine_stage(slot, shares, mid, back)[None]
 
 
 def solution(mesh):

time: 153 us -> 145 us (0.948)
  blocking collectives: 37.7 us -> 86.5 us
  waiting for transfers between devices: 57.5 us -> 16.5 us
  starting transfers between devices: 17.7 us -> 8.73 us
  local copies, waits for them, and re-layouts: 5.97 us -> 1.22 us
  Pallas kernels: 33.9 us -> 31.7 us
    all_to_all x0 -> x2, blocking collectives: none -> 49.2 us  [the longest x1 34.4 us: on_device(): back = lax.all_to_all(done, SP_DP, split_axis=0, concat_axis=0, tiled=True)]
    all_to_all x2 -> x0, waiting for transfers between devices: 35.2 us -> none  [the longest x1 30.3 us: on_device(): back = lax.all_to_all(done, SP_DP, split_axis=0, concat_axis=0, tiled=True)]
    all_to_all x2 -> x0, starting transfers between devices: 8.99 us -> none  [the longest x1 4.54 us: on_device(): back = lax.all_to_all(done, SP_DP, split_axis=0, concat_axis=0, tiled=True)]
    all_to_all x1, waiting for transfers between devices: 22.3 us -> 16.5 us  [on_device(): qkv = lax.all_to_all(packed, SP, split_axis=0, concat_axis=0, tiled=True)]
    unnamed x24 -> x20, local copies, waits for them, and re-layouts: 4.98 us -> 0.27 us
    pallas_call x1, Pallas kernels: 12.8 us -> 11.1 us  [attention(): pl.pallas_call(attention_kernel, in_specs=[pl.BlockSpec(memory_space=pltp...]
  transfers between devices with their start and end apart: 3 -> 1, of which waited for: 3 -> 1; matrix products, arithmetic and copies ran while one was open for 1% -> 1% of each run, Pallas kernels for 3% -> 4%
where the time goes in v4:
time: 145 us
  blocking collectives  86.5 us (60%)
  Pallas kernels  31.7 us (22%)
  waiting for transfers between devices  16.5 us (11%)
  starting transfers between devices  8.73 us (6%)
    all_to_all x1, blocking collectives, on_device(): lax.all_to_all(sent, SP_DP, split_axis=0, concat_axis=0, tiled=True)  37.3 us
    all_to_all x1, blocking collectives, on_device(): back = lax.all_to_all(done, SP_DP, split_axis=0, concat_axis=0, tiled=True)  34.4 us
    all_to_all x1, waiting for transfers between devices, on_device(): qkv = lax.all_to_all(packed, SP, split_axis=0, concat_axis=0, tiled=True)  16.5 us
    all_to_all x1, blocking collectives, on_device(): lax.all_to_all(attended, SP, split_axis=0, concat_axis=0, tiled=True)  14.8 us
    pallas_call x1, Pallas kernels, attention(): pl.pallas_call(attention_kernel, in_specs=[pl.BlockSpec(memory_space=pltp...  11.1 us
    all_to_all x1, starting transfers between devices, on_device(): qkv = lax.all_to_all(packed, SP, split_axis=0, concat_axis=0, tiled=True)  8.73 us
    pallas_call x1, Pallas kernels, expert_stage(): pl.pallas_call(expert_kernel, in_specs=[in_vmem] * 4, out_specs=in_vmem,...  7.83 us
    pallas_call x1, Pallas kernels, route_slots(): pl.pallas_call(route_kernel, in_specs=[in_smem] * 2, out_specs=[in_smem]...  5.37 us
  transfers between devices with their start and end apart: 1, of which 1 were waited for; matrix products, arithmetic and copies ran while one was open for 1% of the time, Pallas kernels for 4%

profile of v4, /device:TPU:1, one launch (start us, length us, event | category | flops | bytes accessed | tf_op | source)
XLA Modules:
  0.0 144.9 jit_solution(11146975959664361709)
XLA Ops:
  0.0 0.0 copy-start
  0.0 2.3 %pack_heads.1 = bf16[16,3,128,128]{3,2,1,0:T(8,128)(2,1)} custom-call(bf16[128,2048]{1,0:T(8,128)(2,1)} %bitcast.16, bf16[128,2048]{1,0:T(8,128)(2,1)} %bitcast.17, bf16[128,2048]{1,0:T(8,128)(2,1)} %bitcast.18), custom_call_target="tpu_custom_call" | custom-call | tf_op jit(solution)/shard_map/pack_heads/pallas_call | solution.py:146
  2.4 0.0 copy-start.6
  2.4 0.0 copy-start.7
  2.4 0.0 copy-start.8
  2.4 8.7 %all-to-all-start = ((bf16[16,3,128,128]{3,2,1,0:T(8,128)(2,1)}), bf16[16,3,128,128]{3,2,1,0:T(8,128)(2,1)S(1)}, u32[]{:S(2)}, u32[]{:S(2)}) async-start(bf16[16,3,128,128]{3,2,1,0:T(8,128)(2,1)} %pack_heads.1), calls=%async_computation | async-start | bytes 3145728 | tf_op jit(solution)/shard_map/all_to_all | solution.py:406
  11.1 0.0 copy-done.6
  11.2 0.1 copy.14
  11.3 0.1 reshape_squeeze.6.routes_ref
  11.4 0.0 copy-done.7
  11.4 0.1 copy.15
  11.5 0.1 reshape_squeeze.7.shares_ref
  11.7 0.0 copy-done.8
  11.7 0.6 dynamic_slice.6.lam_ref
  12.3 5.4 %route_slots.1 = (s32[256]{0:T(256)S(1)}, s32[512]{0:T(512)S(1)}, f32[256]{0:T(256)S(1)}) custom-call(s32[256]{0:T(256)S(1)} %reshape_squeeze.6.routes_ref, f32[256]{0:T(256)S(1)} %reshape_squeeze.7.shares_ref), custom_call_target="tpu_custom_call" | custom-call | tf_op jit(solution)/shard_map/route_slots/pallas_call | solution.py:191
  17.6 0.0 copy-done
  17.7 0.1 dynamic-slice_bitcast_fusion.gain_ref
  17.7 16.5 %all-to-all-done.qkv_ref = bf16[16,3,128,128]{3,2,1,0:T(8,128)(2,1)S(1)} async-done(((bf16[16,3,128,128]{3,2,1,0:T(8,128)(2,1)}), bf16[16,3,128,128]{3,2,1,0:T(8,128)(2,1)S(1)}, u32[]{:S(2)}, u32[]{:S(2)}) %all-to-all-start) | async-done | bytes 1572896 | tf_op jit(solution)/shard_map/all_to_all | solution.py:406
  34.2 0.0 copy-start.1
  34.2 0.0 copy-start.2
  34.2 11.1 %attention.1 = (bf16[16,128,128]{2,1,0:T(8,128)(2,1)S(1)}, bf16[2048,2048]{1,0:T(8,128)(2,1)S(1)}) custom-call(f32[1]{0:T(128)} %dynamic_slice.6.lam_ref, bf16[16,3,128,128]{3,2,1,0:T(8,128)(2,1)S(1)} %all-to-all-done.qkv_ref, f32[1,128]{1,0:T(1,128)S(1)} %dynamic-slice_bitcast_fusion.gain_ref, bf16[2048,2048]{1,0:T(8,128)(2,1)} %weight_hbm.1, ...), custom_call_target="tpu_custom_call" | custom-call | flops 4294967296 | bytes 2097152 | tf_op jit(solution)/shard_map/attention/pallas_call | solution.py:92
  45.3 14.8 %all_to_all.20.heads_ref = bf16[16,128,128]{2,1,0:T(8,128)(2,1)S(1)} all-to-all(bf16[16,128,128]{2,1,0:T(8,128)(2,1)S(1)} %get-tuple-element.15), channel_id=1, replica_groups=mesh['sp_0'=4,'sp_1'=4,'dp'=8] {'sp_0','sp_1'}, dimensions={0} | all-to-all | bytes 1048576 | tf_op jit(solution)/shard_map/all_to_all | solution.py:415
  60.2 0.0 copy-done.1
  60.2 0.0 copy-done.2
  60.2 0.0 copy-start.4
  60.2 0.0 copy-start.5
  60.2 3.1 %middle.1 = (bf16[128,16,128]{2,1,0:T(8,128)(2,1)S(1)}, bf16[512,16,128]{2,1,0:T(8,128)(2,1)S(1)}) custom-call(s32[512]{0:T(512)S(1)} %get-tuple-element.14.routed_ref.token_ref, bf16[16,128,128]{2,1,0:T(8,128)(2,1)S(1)} %all_to_all.20.heads_ref, bf16[2048,2048]{1,0:T(8,128)(2,1)S(1)} %get-tuple-element.16.weight_ref, bf16[128,2048]{1,0:T(8,128)(2,1)S(1)} %bitcast.11, ...), custom_call_target="tpu_custom_call" | custom-call | flops 1073741824 | bytes 8388608 | tf_op jit(solution)/shard_map/middle/pallas_call | solution.py:282
  63.3 0.0 copy-start.3
  63.3 37.3 %all_to_all.21.tile_ref = bf16[512,16,128]{2,1,0:T(8,128)(2,1)S(1)} all-to-all(bf16[512,16,128]{2,1,0:T(8,128)(2,1)S(1)} %get-tuple-element.18), channel_id=1, replica_groups=mesh['sp_0'=4,'sp_1'=4,'dp'=8] {'sp_0','sp_1','dp'}, dimensions={0} | all-to-all | bytes 4194304 | tf_op jit(solution)/shard_map/all_to_all | solution.py:417
  100.6 0.0 copy-done.4
  100.6 0.0 copy-done.5
  100.6 0.0 copy-done.3
  100.6 7.8 %experts.1 = bf16[512,16,128]{2,1,0:T(8,128)(2,1)S(1)} custom-call(bf16[512,16,128]{2,1,0:T(8,128)(2,1)S(1)} %all_to_all.21.tile_ref, bf16[2048,1024]{1,0:T(8,128)(2,1)S(1)} %bitcast.13, bf16[2048,1024]{1,0:T(8,128)(2,1)S(1)} %bitcast.14, bf16[1024,2048]{1,0:T(8,128)(2,1)S(1)} %bitcast.15), custom_call_target="tpu_custom_call" | custom-call | flops 6442450944 | bytes 12582912 | tf_op jit(solution)/shard_map/experts/pallas_call | solution.py:329
  108.4 34.4 %all_to_all.22.back_ref = bf16[512,16,128]{2,1,0:T(8,128)(2,1)S(1)} all-to-all(bf16[512,16,128]{2,1,0:T(8,128)(2,1)S(1)} %experts.1), channel_id=1, replica_groups=mesh['sp_0'=4,'sp_1'=4,'dp'=8] {'sp_0','sp_1','dp'}, dimensions={0} | all-to-all | bytes 4194304 | tf_op jit(solution)/shard_map/all_to_all | solution.py:419
  142.8 1.9 %combine.1 = bf16[128,2048]{1,0:T(8,128)(2,1)} custom-call(s32[256]{0:T(256)S(1)} %get-tuple-element.12.slot_ref, f32[256]{0:T(256)S(1)} %get-tuple-element.13.share_ref, bf16[128,16,128]{2,1,0:T(8,128)(2,1)S(1)} %get-tuple-element.17.mid_ref, bf16[512,16,128]{2,1,0:T(8,128)(2,1)S(1)} %all_to_all.22.back_ref), custom_call_target="tpu_custom_call" | custom-call | tf_op jit(solution)/shard_map/combine/pallas_call | solution.py:373
Async XLA Ops:
  0.0 17.6 %copy-start = (f32[2048]{0:T(1024)S(1)}, f32[2048]{0:T(1024)}, u32[]{:S(2)}) copy-start(f32[2048]{0:T(1024)} %param.18) | copy-start | bytes 24580
  2.4 8.8 %copy-start.6 = (s32[1,128,2]{1,2,0:T(2,128)S(1)}, s32[1,128,2]{1,2,0:T(2,128)}, u32[]{:S(2)}) copy-start(s32[1,128,2]{1,2,0:T(2,128)} %param.21) | copy-start | bytes 3076
  2.4 9.0 %copy-start.7 = (f32[1,128,2]{1,2,0:T(2,128)S(1)}, f32[1,128,2]{1,2,0:T(2,128)}, u32[]{:S(2)}) copy-start(f32[1,128,2]{1,2,0:T(2,128)} %param.22) | copy-start | bytes 3076
  2.4 9.3 %copy-start.8 = (f32[16]{0:T(128)S(1)}, f32[16]{0:T(128)}, u32[]{:S(2)}) copy-start(f32[16]{0:T(128)} %param.17) | copy-start | bytes 196
  2.4 31.8 %all-to-all-start = ((bf16[16,3,128,128]{3,2,1,0:T(8,128)(2,1)}), bf16[16,3,128,128]{3,2,1,0:T(8,128)(2,1)S(1)}, u32[]{:S(2)}, u32[]{:S(2)}) async-start(bf16[16,3,128,128]{3,2,1,0:T(8,128)(2,1)} %pack_heads.1), calls=%async_computation | async-start | bytes 3145728 | tf_op jit(solution)/shard_map/all_to_all | solution.py:406
  34.2 25.9 %copy-start.1 = (bf16[1,128,2048]{2,1,0:T(8,128)(2,1)S(1)}, bf16[1,128,2048]{2,1,0:T(8,128)(2,1)}, u32[]{:S(2)}) copy-start(bf16[1,128,2048]{2,1,0:T(8,128)(2,1)} %param.13) | copy-start | bytes 1572868
  34.2 25.9 %copy-start.2 = (f32[2048]{0:T(1024)S(1)}, f32[2048]{0:T(1024)}, u32[]{:S(2)}) copy-start(f32[2048]{0:T(1024)} %param.20) | copy-start | bytes 24580
  60.2 40.4 %copy-start.4 = (bf16[1,2048,1024]{2,1,0:T(8,128)(2,1)S(1)}, bf16[1,2048,1024]{2,1,0:T(8,128)(2,1)}, u32[]{:S(2)}) copy-start(bf16[1,2048,1024]{2,1,0:T(8,128)(2,1)} %param.24) | copy-start | bytes 12582916
  60.2 40.4 %copy-start.5 = (bf16[1,1024,2048]{2,1,0:T(8,128)(2,1)S(1)}, bf16[1,1024,2048]{2,1,0:T(8,128)(2,1)}, u32[]{:S(2)}) copy-start(bf16[1,1024,2048]{2,1,0:T(8,128)(2,1)} %param.25) | copy-start | bytes 12582916
  63.3 37.3 %copy-start.3 = (bf16[1,2048,1024]{2,1,0:T(8,128)(2,1)S(1)}, bf16[1,2048,1024]{2,1,0:T(8,128)(2,1)}, u32[]{:S(2)}) copy-start(bf16[1,2048,1024]{2,1,0:T(8,128)(2,1)} %param.23) | copy-start | bytes 12582916

commit v5 on v4

--- a/solution.py
+++ b/solution.py
@@ -37,16 +37,41 @@
 
 
 def attention_kernel(
-    lam_ref, qkv_ref, gain_ref, weight_hbm, routed_ref,
-    out_ref, weight_ref, values_ref, scores_ref, sems,
+    lam_ref, qkv_ref, gain_ref, weight_hbm, routes_ref,
+    out_ref, weight_ref, slot_ref, token_ref, values_ref, scores_ref, count_ref, sems,
 ):
-    del routed_ref
+    head = lax.axis_index(SP)
+    lam = lam_ref[head]
+    gain = gain_ref[pl.ds(head, 1), :]
+    experts = count_ref.shape[0]
+    topk, tokens_here = routes_ref.shape
+    routed = [(k, t) for k in range(topk) for t in range(tokens_here)]
+
+    def clear_count(index, carry):
+        count_ref[index] = 0
+        return carry
+
+    def clear_token(index, carry):
+        token_ref[index] = 0
+        return carry
+
+    def route(places):
+        for k, t in places:
+            expert = routes_ref[k, t]
+            rank = count_ref[expert]
+            count_ref[expert] = rank + 1
+            slot = expert * CAP + rank
+            slot_ref[k, t] = slot
+            token_ref[slot] = t
+
     sources, _, tokens, width = qkv_ref.shape
     length = sources * tokens
     rows = ATT_BLOCKS * tokens
     steps = sources // ATT_BLOCKS
     fetch = pltpu.make_async_copy(weight_hbm, weight_ref, sems.at[0])
     fetch.start()
+    lax.fori_loop(0, experts, clear_count, 0, unroll=16)
+    lax.fori_loop(0, token_ref.shape[0], clear_token, 0, unroll=16)
     values_ref[:, :VD] = qkv_ref[:, 2].reshape(length, width)
     values_ref[:, VD:] = jnp.ones((length, VD), jnp.bfloat16)
 
@@ -68,39 +93,45 @@
         weight = jnp.exp2((score - top) * EXP_SCALE).astype(jnp.bfloat16)
         summed = jnp.dot(weight, values_ref[...], preferred_element_type=jnp.float32)
         first, second = summed[:rows], summed[rows:]
-        head_out = first[:, :VD] / first[:, VD:] - lam_ref[0] * (second[:, :VD] / second[:, VD:])
+        head_out = first[:, :VD] / first[:, VD:] - lam * (second[:, :VD] / second[:, VD:])
         normed = head_out * lax.rsqrt(jnp.mean(head_out * head_out, axis=-1, keepdims=True) + eps)
         at = pl.ds(step * ATT_BLOCKS, ATT_BLOCKS)
         out_ref[at] = (
-            (normed * gain_ref[...] * 0.8).astype(jnp.bfloat16).reshape(ATT_BLOCKS, tokens, VD)
+            (normed * gain * 0.8).astype(jnp.bfloat16).reshape(ATT_BLOCKS, tokens, VD)
         )
 
     scores(0, 0)
+    share = len(routed) // steps
     for step in range(1, steps):
+        route(routed[(step - 1) * share : step * share])
         scores(step, step % 2)
         attend(step - 1, (step - 1) % 2)
+    route(routed[(steps - 1) * share :])
     attend(steps - 1, (steps - 1) % 2)
     fetch.wait()
 
 
-def attention(lam, qkv, gain, out_weight, routed):
+def attention(lam, qkv, gain, out_weight, routes, experts):
     sources, _, tokens, width = qkv.shape
     length = sources * tokens
     in_vmem = pl.BlockSpec(memory_space=pltpu.VMEM)
     in_hbm = pl.BlockSpec(memory_space=pltpu.HBM)
+    in_smem = pl.BlockSpec(memory_space=pltpu.SMEM)
     heads = (sources, tokens, VD)
     return pl.pallas_call(
         attention_kernel,
-        in_specs=[pl.BlockSpec(memory_space=pltpu.SMEM), in_vmem, in_vmem, in_hbm]
-        + [pl.BlockSpec(memory_space=pl.ANY)],
-        out_specs=[in_vmem] * 2,
+        in_specs=[in_smem, in_vmem, in_vmem, in_hbm, in_smem],
+        out_specs=[in_vmem, in_vmem, in_smem, in_smem],
         out_shape=[
             jax.ShapeDtypeStruct(heads, jnp.bfloat16),
             pltpu.VMEM(out_weight.shape, jnp.bfloat16),
+            jax.ShapeDtypeStruct(routes.shape, jnp.int32),
+            jax.ShapeDtypeStruct((experts * CAP,), jnp.int32),
         ],
         scratch_shapes=[
             pltpu.VMEM((length, 2 * VD), jnp.bfloat16),
             pltpu.VMEM((2, 2 * ATT_BLOCKS * tokens, length), jnp.float32),
+            pltpu.SMEM((experts,), jnp.int32),
             pltpu.SemaphoreType.DMA((1,)),
         ],
         compiler_params=within(24),
@@ -110,7 +141,7 @@
             transcendentals=2 * length * length,
         ),
         name="attention",
-    )(lam, on_chip(qkv), gain, off_chip(out_weight), routed)
+    )(lam, on_chip(qkv), gain, off_chip(out_weight), routes)
 
 
 ROW = (16, 128)
@@ -119,88 +150,34 @@
 CAP = 4
 
 
-def pack_kernel(query_ref, key_ref, value_ref, out_ref, rows, blocks, in_sems, out_sems):
-    copies_in = [
-        pltpu.make_async_copy(ref, rows.at[at], in_sems.at[at])
+def pack_kernel(query_ref, key_ref, value_ref, out_ref, rows, sems):
+    copies = [
+        pltpu.make_async_copy(ref, rows.at[at], sems.at[at])
         for at, ref in enumerate((query_ref, key_ref, value_ref))
     ]
-    copies_out = [
-        pltpu.make_async_copy(blocks.at[:, at], out_ref.at[:, at], out_sems.at[at])
-        for at in range(3)
-    ]
-    for copy in copies_in:
+    for copy in copies:
         copy.start()
     for at in range(3):
-        copies_in[at].wait()
+        copies[at].wait()
         for head in range(HEADS):
-            blocks[head, at] = rows[at, :, head * VD : (head + 1) * VD]
-        copies_out[at].start()
-    for copy in copies_out:
-        copy.wait()
+            out_ref[head, at] = rows[at, :, head * VD : (head + 1) * VD]
 
 
 def pack_heads(query, key, value):
     tokens = query.shape[0]
-    packed = (HEADS, 3, tokens, VD)
     in_hbm = pl.BlockSpec(memory_space=pltpu.HBM)
     return pl.pallas_call(
         pack_kernel,
         in_specs=[in_hbm] * 3,
-        out_specs=in_hbm,
-        out_shape=pltpu.HBM(packed, jnp.bfloat16),
+        out_specs=pl.BlockSpec(memory_space=pltpu.VMEM),
+        out_shape=jax.ShapeDtypeStruct((HEADS, 3, tokens, VD), jnp.bfloat16),
         scratch_shapes=[
             pltpu.VMEM((3, tokens, HEADS * VD), jnp.bfloat16),
-            pltpu.VMEM(packed, jnp.bfloat16),
-            pltpu.SemaphoreType.DMA((3,)),
             pltpu.SemaphoreType.DMA((3,)),
         ],
         compiler_params=within(8),
         name="pack_heads",
     )(*(off_chip(a) for a in (query, key, value)))
-
-
-def route_kernel(routes_ref, shares_ref, slot_ref, token_ref, kept_ref, count_ref):
-    experts = count_ref.shape[0]
-    slots = token_ref.shape[0]
-
-    def clear_count(index, carry):
-        count_ref[index] = 0
-        return carry
-
-    def clear_token(index, carry):
-        token_ref[index] = 0
-        return carry
-
-    def place(index, carry):
-        expert = routes_ref[index]
-        rank = count_ref[expert]
-        count_ref[expert] = rank + 1
-        slot = expert * CAP + rank
-        slot_ref[index] = slot
-        token_ref[slot] = index // 2
-        kept_ref[index] = shares_ref[index]
-        return carry
-
-    lax.fori_loop(0, experts, clear_count, 0, unroll=8)
-    lax.fori_loop(0, slots, clear_token, 0, unroll=8)
-    lax.fori_loop(0, slot_ref.shape[0], place, 0)
-
-
-def route_slots(flat_routes, flat_shares, experts):
-    in_smem = pl.BlockSpec(memory_space=pltpu.SMEM)
-    return pl.pallas_call(
-        route_kernel,
-        in_specs=[in_smem] * 2,
-        out_specs=[in_smem] * 3,
-        out_shape=[
-            jax.ShapeDtypeStruct(flat_routes.shape, jnp.int32),
-            jax.ShapeDtypeStruct((experts * CAP,), jnp.int32),
-            jax.ShapeDtypeStruct(flat_shares.shape, jnp.float32),
-        ],
-        scratch_shapes=[pltpu.SMEM((experts,), jnp.int32)],
-        compiler_params=within(1),
-        name="route_slots",
-    )(flat_routes, flat_shares)
 
 
 def swap_matrix():
@@ -348,8 +325,8 @@
     tokens = mid_ref.shape[0]
 
     def token(index, carry):
-        one = back_ref[slot_ref[2 * index]].astype(jnp.float32) * share_ref[2 * index]
-        two = back_ref[slot_ref[2 * index + 1]].astype(jnp.float32) * share_ref[2 * index + 1]
+        one = back_ref[slot_ref[0, index]].astype(jnp.float32) * share_ref[0, index]
+        two = back_ref[slot_ref[1, index]].astype(jnp.float32) * share_ref[1, index]
         tiles[index] = (mid_ref[index].astype(jnp.float32) + (one + two)).astype(jnp.bfloat16)
         return carry
 
@@ -404,20 +381,16 @@
     count_dp = lax.axis_size("dp")
     packed = pack_heads(query_maps[0], key_maps[0], value_rows[0])
     qkv = lax.all_to_all(packed, SP, split_axis=0, concat_axis=0, tiled=True)
-    head = lax.axis_index(SP)
-    lam_here = lax.dynamic_slice_in_dim(lambdas, head, 1)
-    gain_here = lax.dynamic_slice_in_dim(head_gain, head * VD, VD)[None]
     experts_all = count_sp * count_dp
-    slot, slot_token, shares = route_slots(
-        routes[0].reshape(-1), route_weights[0].reshape(-1), experts_all
+    attended, weight_here, slot, slot_token = attention(
+        lambdas, qkv, head_gain.reshape(HEADS, VD), out_weight, routes[0].T, experts_all
     )
-    attended, weight_here = attention(lam_here, qkv, gain_here, out_weight, slot_token)
     returned = lax.all_to_all(attended, SP, split_axis=0, concat_axis=0, tiled=True)
     mid, sent = middle_stage(slot_token, returned, weight_here, residual[0], ffn_gain[None])
     arrived = lax.all_to_all(sent, SP_DP, split_axis=0, concat_axis=0, tiled=True)
     done = expert_stage(arrived, expert_gate[0], expert_up[0], expert_down[0])
     back = lax.all_to_all(done, SP_DP, split_axis=0, concat_axis=0, tiled=True)
-    return combine_stage(slot, shares, mid, back)[None]
+    return combine_stage(slot, route_weights[0].T, mid, back)[None]
 
 
 def solution(mesh):

time: 145 us -> 143 us (0.986)
  blocking collectives: 86.5 us -> 116 us
  waiting for transfers between devices: 16.5 us -> 0 us
  starting transfers between devices: 8.73 us -> 0 us
  Pallas kernels: 31.7 us -> 26.5 us
    all_to_all x0 -> x1, blocking collectives: none -> 30.2 us  [on_device(): qkv = lax.all_to_all(packed, SP, split_axis=0, concat_axis=0, tiled=True)]
    all_to_all x1 -> x0, waiting for transfers between devices: 16.5 us -> none  [on_device(): qkv = lax.all_to_all(packed, SP, split_axis=0, concat_axis=0, tiled=True)]
    all_to_all x1 -> x0, starting transfers between devices: 8.73 us -> none  [on_device(): qkv = lax.all_to_all(packed, SP, split_axis=0, concat_axis=0, tiled=True)]
    pallas_call x3 -> x2, Pallas kernels: 18.8 us -> 13.6 us  [the longest x1 12.1 us: attention(): pl.pallas_call(attention_kernel, in_specs=[in_smem, in_vmem, in_vmem, in_...]
    all_to_all x1, blocking collectives: 14.8 us -> 13.3 us  [on_device(): lax.all_to_all(attended, SP, split_axis=0, concat_axis=0, tiled=True)]
  transfers between devices with their start and end apart: 1 -> 0, of which waited for: 1 -> 0; matrix products, arithmetic and copies ran while one was open for 1% -> 0% of each run, Pallas kernels for 4% -> 0%
where the time goes in v5:
time: 143 us; the launch traced here: 142 us
  blocking collectives  116 us (81%)
  Pallas kernels  26.5 us (19%)
    all_to_all x1, blocking collectives, on_device(): lax.all_to_all(sent, SP_DP, split_axis=0, concat_axis=0, tiled=True)  37.8 us
    all_to_all x1, blocking collectives, on_device(): back = lax.all_to_all(done, SP_DP, split_axis=0, concat_axis=0, tiled=True)  34.4 us
    all_to_all x1, blocking collectives, on_device(): qkv = lax.all_to_all(packed, SP, split_axis=0, concat_axis=0, tiled=True)  30.2 us
    all_to_all x1, blocking collectives, on_device(): lax.all_to_all(attended, SP, split_axis=0, concat_axis=0, tiled=True)  13.3 us
    pallas_call x1, Pallas kernels, attention(): pl.pallas_call(attention_kernel, in_specs=[in_smem, in_vmem, in_vmem, in_...  12.1 us
    pallas_call x1, Pallas kernels, expert_stage(): pl.pallas_call(expert_kernel, in_specs=[in_vmem] * 4, out_specs=in_vmem,...  7.78 us
    pallas_call x1, Pallas kernels, middle_stage(): pl.pallas_call(middle_kernel, in_specs=[pl.BlockSpec(memory_space=pltpu.S...  3.17 us

profile of v5, /device:TPU:1, one launch (start us, length us, event | category | flops | bytes accessed | tf_op | source)
XLA Modules:
  0.0 142.5 jit_solution(1795869361508128557)
XLA Ops:
  0.0 1.5 %pack_heads.1 = bf16[16,3,128,128]{3,2,1,0:T(8,128)(2,1)S(1)} custom-call(bf16[128,2048]{1,0:T(8,128)(2,1)} %bitcast.24, bf16[128,2048]{1,0:T(8,128)(2,1)} %bitcast.25, bf16[128,2048]{1,0:T(8,128)(2,1)} %bitcast.26), custom_call_target="tpu_custom_call" | custom-call | tf_op jit(solution)/shard_map/pack_heads/pallas_call | solution.py:169
  1.5 0.0 copy-start.6
  1.5 0.0 copy-start.7
  1.5 0.0 copy-start.8
  1.5 30.2 %all_to_all.20.qkv_ref = bf16[16,3,128,128]{3,2,1,0:T(8,128)(2,1)S(1)} all-to-all(bf16[16,3,128,128]{3,2,1,0:T(8,128)(2,1)S(1)} %pack_heads.1), channel_id=1, replica_groups=mesh['sp_0'=4,'sp_1'=4,'dp'=8] {'sp_0','sp_1'}, dimensions={0} | all-to-all | bytes 3145728 | tf_op jit(solution)/shard_map/all_to_all | solution.py:383
  31.7 0.0 copy-done.6
  31.7 0.0 copy-done.7
  31.7 0.0 copy-done.8
  31.7 0.0 copy-start
  31.7 0.0 copy-start.1
  31.7 12.1 %attention.1 = (bf16[16,128,128]{2,1,0:T(8,128)(2,1)S(1)}, bf16[2048,2048]{1,0:T(8,128)(2,1)S(1)}, s32[2,128]{1,0:T(2,128)S(1)}, s32[512]{0:T(512)S(1)}) custom-call(f32[16]{0:T(128)S(1)} %copy-done.8, bf16[16,3,128,128]{3,2,1,0:T(8,128)(2,1)S(1)} %all_to_all.20.qkv_ref, f32[16,128]{1,0:T(8,128)S(1)} %bitcast.22, bf16[2048,2048]{1,0:T(8,128)(2,1)} %weight_hbm.1, ...), custom_call_target="tpu_custom_call" | custom-call | flops 4294967296 | bytes 2097152 | tf_op jit(solution)/shard_map/attention/pallas_call | solution.py:121
  43.9 13.3 %all_to_all.21.heads_ref = bf16[16,128,128]{2,1,0:T(8,128)(2,1)S(1)} all-to-all(bf16[16,128,128]{2,1,0:T(8,128)(2,1)S(1)} %get-tuple-element.13), channel_id=1, replica_groups=mesh['sp_0'=4,'sp_1'=4,'dp'=8] {'sp_0','sp_1'}, dimensions={0} | all-to-all | bytes 1048576 | tf_op jit(solution)/shard_map/all_to_all | solution.py:388
  57.2 0.0 copy-done
  57.2 0.0 copy-done.1
  57.2 0.0 copy-start.4
  57.2 0.0 copy-start.5
  57.2 3.2 %middle.1 = (bf16[128,16,128]{2,1,0:T(8,128)(2,1)S(1)}, bf16[512,16,128]{2,1,0:T(8,128)(2,1)S(1)}) custom-call(s32[512]{0:T(512)S(1)} %get-tuple-element.12.token_ref, bf16[16,128,128]{2,1,0:T(8,128)(2,1)S(1)} %all_to_all.21.heads_ref, bf16[2048,2048]{1,0:T(8,128)(2,1)S(1)} %get-tuple-element.14.weight_ref, bf16[128,2048]{1,0:T(8,128)(2,1)S(1)} %bitcast.16, ...), custom_call_target="tpu_custom_call" | custom-call | flops 1073741824 | bytes 8388608 | tf_op jit(solution)/shard_map/middle/pallas_call | solution.py:259
  60.4 0.0 copy-start.3
  60.4 37.8 %all_to_all.22.tile_ref = bf16[512,16,128]{2,1,0:T(8,128)(2,1)S(1)} all-to-all(bf16[512,16,128]{2,1,0:T(8,128)(2,1)S(1)} %get-tuple-element.16), channel_id=1, replica_groups=mesh['sp_0'=4,'sp_1'=4,'dp'=8] {'sp_0','sp_1','dp'}, dimensions={0} | all-to-all | bytes 4194304 | tf_op jit(solution)/shard_map/all_to_all | solution.py:390
  98.2 0.0 copy-done.4
  98.2 0.0 copy-done.5
  98.2 0.0 copy-done.3
  98.2 7.8 %experts.1 = bf16[512,16,128]{2,1,0:T(8,128)(2,1)S(1)} custom-call(bf16[512,16,128]{2,1,0:T(8,128)(2,1)S(1)} %all_to_all.22.tile_ref, bf16[2048,1024]{1,0:T(8,128)(2,1)S(1)} %bitcast.19, bf16[2048,1024]{1,0:T(8,128)(2,1)S(1)} %bitcast.20, bf16[1024,2048]{1,0:T(8,128)(2,1)S(1)} %bitcast.21), custom_call_target="tpu_custom_call" | custom-call | flops 6442450944 | bytes 12582912 | tf_op jit(solution)/shard_map/experts/pallas_call | solution.py:306
  106.0 0.0 copy-start.2
  106.0 34.4 %all_to_all.23.back_ref = bf16[512,16,128]{2,1,0:T(8,128)(2,1)S(1)} all-to-all(bf16[512,16,128]{2,1,0:T(8,128)(2,1)S(1)} %experts.1), channel_id=1, replica_groups=mesh['sp_0'=4,'sp_1'=4,'dp'=8] {'sp_0','sp_1','dp'}, dimensions={0} | all-to-all | bytes 4194304 | tf_op jit(solution)/shard_map/all_to_all | solution.py:392
  140.4 0.0 copy-done.2
  140.4 1.9 %combine.1 = bf16[128,2048]{1,0:T(8,128)(2,1)} custom-call(s32[2,128]{1,0:T(2,128)S(1)} %get-tuple-element.11.slot_ref, f32[2,128]{1,0:T(2,128)S(1)} %bitcast.18, bf16[128,16,128]{2,1,0:T(8,128)(2,1)S(1)} %get-tuple-element.15.mid_ref, bf16[512,16,128]{2,1,0:T(8,128)(2,1)S(1)} %all_to_all.23.back_ref), custom_call_target="tpu_custom_call" | custom-call | tf_op jit(solution)/shard_map/combine/pallas_call | solution.py:350
Async XLA Ops:
  1.5 30.2 %copy-start.6 = (f32[2048]{0:T(1024)S(1)}, f32[2048]{0:T(1024)}, u32[]{:S(2)}) copy-start(f32[2048]{0:T(1024)} %param.18) | copy-start | bytes 24580
  1.5 30.2 %copy-start.7 = (s32[1,128,2]{1,2,0:T(2,128)S(1)}, s32[1,128,2]{1,2,0:T(2,128)}, u32[]{:S(2)}) copy-start(s32[1,128,2]{1,2,0:T(2,128)} %param.21) | copy-start | bytes 3076
  1.5 30.2 %copy-start.8 = (f32[16]{0:T(128)S(1)}, f32[16]{0:T(128)}, u32[]{:S(2)}) copy-start(f32[16]{0:T(128)} %lam_ref.1) | copy-start | bytes 196
  31.7 25.5 %copy-start = (bf16[1,128,2048]{2,1,0:T(8,128)(2,1)S(1)}, bf16[1,128,2048]{2,1,0:T(8,128)(2,1)}, u32[]{:S(2)}) copy-start(bf16[1,128,2048]{2,1,0:T(8,128)(2,1)} %param.13) | copy-start | bytes 1572868
  31.7 25.5 %copy-start.1 = (f32[2048]{0:T(1024)S(1)}, f32[2048]{0:T(1024)}, u32[]{:S(2)}) copy-start(f32[2048]{0:T(1024)} %param.20) | copy-start | bytes 24580
  57.2 41.0 %copy-start.4 = (bf16[1,2048,1024]{2,1,0:T(8,128)(2,1)S(1)}, bf16[1,2048,1024]{2,1,0:T(8,128)(2,1)}, u32[]{:S(2)}) copy-start(bf16[1,2048,1024]{2,1,0:T(8,128)(2,1)} %param.24) | copy-start | bytes 12582916
  57.2 41.0 %copy-start.5 = (bf16[1,1024,2048]{2,1,0:T(8,128)(2,1)S(1)}, bf16[1,1024,2048]{2,1,0:T(8,128)(2,1)}, u32[]{:S(2)}) copy-start(bf16[1,1024,2048]{2,1,0:T(8,128)(2,1)} %param.25) | copy-start | bytes 12582916
  60.4 37.8 %copy-start.3 = (bf16[1,2048,1024]{2,1,0:T(8,128)(2,1)S(1)}, bf16[1,2048,1024]{2,1,0:T(8,128)(2,1)}, u32[]{:S(2)}) copy-start(bf16[1,2048,1024]{2,1,0:T(8,128)(2,1)} %param.23) | copy-start | bytes 12582916
  106.0 34.4 %copy-start.2 = (f32[1,128,2]{1,2,0:T(2,128)S(1)}, f32[1,128,2]{1,2,0:T(2,128)}, u32[]{:S(2)}) copy-start(f32[1,128,2]{1,2,0:T(2,128)} %param.22) | copy-start | bytes 3076

commit v6 on v5

--- a/solution.py
+++ b/solution.py
@@ -47,14 +47,6 @@
     topk, tokens_here = routes_ref.shape
     routed = [(k, t) for k in range(topk) for t in range(tokens_here)]
 
-    def clear_count(index, carry):
-        count_ref[index] = 0
-        return carry
-
-    def clear_token(index, carry):
-        token_ref[index] = 0
-        return carry
-
     def route(places):
         for k, t in places:
             expert = routes_ref[k, t]
@@ -70,8 +62,10 @@
     steps = sources // ATT_BLOCKS
     fetch = pltpu.make_async_copy(weight_hbm, weight_ref, sems.at[0])
     fetch.start()
-    lax.fori_loop(0, experts, clear_count, 0, unroll=16)
-    lax.fori_loop(0, token_ref.shape[0], clear_token, 0, unroll=16)
+    for index in range(experts):
+        count_ref[index] = 0
+    for index in range(token_ref.shape[0]):
+        token_ref[index] = 0
     values_ref[:, :VD] = qkv_ref[:, 2].reshape(length, width)
     values_ref[:, VD:] = jnp.ones((length, VD), jnp.bfloat16)
 
@@ -240,16 +234,13 @@
     swap = swap_matrix()
     for one, two in pair_slices(tokens):
         both = slice(one.start, two.stop)
-        mid = middle[both, :]
-        mid_ref[one], mid_ref[two] = rows_to_tiles(mid, swap)
-        normed = mid.astype(jnp.float32) * scale[both] * gain_ref[...]
+        normed = middle[both, :].astype(jnp.float32) * scale[both] * gain_ref[...]
         tiles[one], tiles[two] = rows_to_tiles(normed.astype(jnp.bfloat16), swap)
 
-    def gather(index, carry):
+    for index in range(sent_ref.shape[0]):
         sent_ref[index] = tiles[token_ref[index]]
-        return carry
-
-    lax.fori_loop(0, sent_ref.shape[0], gather, 0, unroll=16)
+    for one, two in pair_slices(tokens):
+        mid_ref[one], mid_ref[two] = rows_to_tiles(middle[one.start : two.stop, :], swap)
 
 
 def middle_stage(slot_token, heads, out_weight, residual, gain):

time: 143 us -> 144 us (level)
  no operation moved by 1% of the time
where the time goes in v6:
time: 144 us; the launch traced here: 143 us
  blocking collectives  116 us (81%)
  Pallas kernels  27.3 us (19%)
    all_to_all x1, blocking collectives, on_device(): lax.all_to_all(sent, SP_DP, split_axis=0, concat_axis=0, tiled=True)  37.8 us
    all_to_all x1, blocking collectives, on_device(): back = lax.all_to_all(done, SP_DP, split_axis=0, concat_axis=0, tiled=True)  34.4 us
    all_to_all x1, blocking collectives, on_device(): qkv = lax.all_to_all(packed, SP, split_axis=0, concat_axis=0, tiled=True)  30.2 us
    all_to_all x1, blocking collectives, on_device(): lax.all_to_all(attended, SP, split_axis=0, concat_axis=0, tiled=True)  13.3 us
    pallas_call x1, Pallas kernels, attention(): pl.pallas_call(attention_kernel, in_specs=[in_smem, in_vmem, in_vmem, in_...  13.2 us
    pallas_call x1, Pallas kernels, expert_stage(): pl.pallas_call(expert_kernel, in_specs=[in_vmem] * 4, out_specs=in_vmem,...  7.78 us

profile of v6, /device:TPU:1, one launch (start us, length us, event | category | flops | bytes accessed | tf_op | source)
XLA Modules:
  0.0 143.3 jit_solution(17237252358538398942)
XLA Ops:
  0.0 1.5 %pack_heads.1 = bf16[16,3,128,128]{3,2,1,0:T(8,128)(2,1)S(1)} custom-call(bf16[128,2048]{1,0:T(8,128)(2,1)} %bitcast.24, bf16[128,2048]{1,0:T(8,128)(2,1)} %bitcast.25, bf16[128,2048]{1,0:T(8,128)(2,1)} %bitcast.26), custom_call_target="tpu_custom_call" | custom-call | tf_op jit(solution)/shard_map/pack_heads/pallas_call | solution.py:163
  1.5 0.0 copy-start.6
  1.5 0.0 copy-start.7
  1.5 0.0 copy-start.8
  1.5 30.2 %all_to_all.20.qkv_ref = bf16[16,3,128,128]{3,2,1,0:T(8,128)(2,1)S(1)} all-to-all(bf16[16,3,128,128]{3,2,1,0:T(8,128)(2,1)S(1)} %pack_heads.1), channel_id=1, replica_groups=mesh['sp_0'=4,'sp_1'=4,'dp'=8] {'sp_0','sp_1'}, dimensions={0} | all-to-all | bytes 3145728 | tf_op jit(solution)/shard_map/all_to_all | solution.py:374
  31.7 0.0 copy-done.6
  31.7 0.0 copy-done.7
  31.7 0.0 copy-done.8
  31.7 0.0 copy-start
  31.7 0.0 copy-start.1
  31.7 13.2 %attention.1 = (bf16[16,128,128]{2,1,0:T(8,128)(2,1)S(1)}, bf16[2048,2048]{1,0:T(8,128)(2,1)S(1)}, s32[2,128]{1,0:T(2,128)S(1)}, s32[512]{0:T(512)S(1)}) custom-call(f32[16]{0:T(128)S(1)} %copy-done.8, bf16[16,3,128,128]{3,2,1,0:T(8,128)(2,1)S(1)} %all_to_all.20.qkv_ref, f32[16,128]{1,0:T(8,128)S(1)} %bitcast.22, bf16[2048,2048]{1,0:T(8,128)(2,1)} %weight_hbm.1, ...), custom_call_target="tpu_custom_call" | custom-call | flops 4294967296 | bytes 2097152 | tf_op jit(solution)/shard_map/attention/pallas_call | solution.py:115
  45.0 13.3 %all_to_all.21.heads_ref = bf16[16,128,128]{2,1,0:T(8,128)(2,1)S(1)} all-to-all(bf16[16,128,128]{2,1,0:T(8,128)(2,1)S(1)} %get-tuple-element.13), channel_id=1, replica_groups=mesh['sp_0'=4,'sp_1'=4,'dp'=8] {'sp_0','sp_1'}, dimensions={0} | all-to-all | bytes 1048576 | tf_op jit(solution)/shard_map/all_to_all | solution.py:379
  58.3 0.0 copy-done
  58.3 0.0 copy-done.1
  58.3 0.0 copy-start.4
  58.3 0.0 copy-start.5
  58.3 2.9 %middle.1 = (bf16[128,16,128]{2,1,0:T(8,128)(2,1)S(1)}, bf16[512,16,128]{2,1,0:T(8,128)(2,1)S(1)}) custom-call(s32[512]{0:T(512)S(1)} %get-tuple-element.12.token_ref, bf16[16,128,128]{2,1,0:T(8,128)(2,1)S(1)} %all_to_all.21.heads_ref, bf16[2048,2048]{1,0:T(8,128)(2,1)S(1)} %get-tuple-element.14.weight_ref, bf16[128,2048]{1,0:T(8,128)(2,1)S(1)} %bitcast.16, ...), custom_call_target="tpu_custom_call" | custom-call | flops 1073741824 | bytes 8388608 | tf_op jit(solution)/shard_map/middle/pallas_call | solution.py:250
  61.2 0.0 copy-start.3
  61.2 37.8 %all_to_all.22.tile_ref = bf16[512,16,128]{2,1,0:T(8,128)(2,1)S(1)} all-to-all(bf16[512,16,128]{2,1,0:T(8,128)(2,1)S(1)} %get-tuple-element.16), channel_id=1, replica_groups=mesh['sp_0'=4,'sp_1'=4,'dp'=8] {'sp_0','sp_1','dp'}, dimensions={0} | all-to-all | bytes 4194304 | tf_op jit(solution)/shard_map/all_to_all | solution.py:381
  99.0 0.0 copy-done.4
  99.0 0.0 copy-done.5
  99.0 0.0 copy-done.3
  99.0 7.8 %experts.1 = bf16[512,16,128]{2,1,0:T(8,128)(2,1)S(1)} custom-call(bf16[512,16,128]{2,1,0:T(8,128)(2,1)S(1)} %all_to_all.22.tile_ref, bf16[2048,1024]{1,0:T(8,128)(2,1)S(1)} %bitcast.19, bf16[2048,1024]{1,0:T(8,128)(2,1)S(1)} %bitcast.20, bf16[1024,2048]{1,0:T(8,128)(2,1)S(1)} %bitcast.21), custom_call_target="tpu_custom_call" | custom-call | flops 6442450944 | bytes 12582912 | tf_op jit(solution)/shard_map/experts/pallas_call | solution.py:297
  106.8 0.0 copy-start.2
  106.8 34.4 %all_to_all.23.back_ref = bf16[512,16,128]{2,1,0:T(8,128)(2,1)S(1)} all-to-all(bf16[512,16,128]{2,1,0:T(8,128)(2,1)S(1)} %experts.1), channel_id=1, replica_groups=mesh['sp_0'=4,'sp_1'=4,'dp'=8] {'sp_0','sp_1','dp'}, dimensions={0} | all-to-all | bytes 4194304 | tf_op jit(solution)/shard_map/all_to_all | solution.py:383
  141.2 0.0 copy-done.2
  141.2 1.9 %combine.1 = bf16[128,2048]{1,0:T(8,128)(2,1)} custom-call(s32[2,128]{1,0:T(2,128)S(1)} %get-tuple-element.11.slot_ref, f32[2,128]{1,0:T(2,128)S(1)} %bitcast.18, bf16[128,16,128]{2,1,0:T(8,128)(2,1)S(1)} %get-tuple-element.15.mid_ref, bf16[512,16,128]{2,1,0:T(8,128)(2,1)S(1)} %all_to_all.23.back_ref), custom_call_target="tpu_custom_call" | custom-call | tf_op jit(solution)/shard_map/combine/pallas_call | solution.py:341
Async XLA Ops:
  1.5 30.2 %copy-start.6 = (f32[2048]{0:T(1024)S(1)}, f32[2048]{0:T(1024)}, u32[]{:S(2)}) copy-start(f32[2048]{0:T(1024)} %param.18) | copy-start | bytes 24580
  1.5 30.2 %copy-start.7 = (s32[1,128,2]{1,2,0:T(2,128)S(1)}, s32[1,128,2]{1,2,0:T(2,128)}, u32[]{:S(2)}) copy-start(s32[1,128,2]{1,2,0:T(2,128)} %param.21) | copy-start | bytes 3076
  1.5 30.2 %copy-start.8 = (f32[16]{0:T(128)S(1)}, f32[16]{0:T(128)}, u32[]{:S(2)}) copy-start(f32[16]{0:T(128)} %lam_ref.1) | copy-start | bytes 196
  31.7 26.6 %copy-start = (bf16[1,128,2048]{2,1,0:T(8,128)(2,1)S(1)}, bf16[1,128,2048]{2,1,0:T(8,128)(2,1)}, u32[]{:S(2)}) copy-start(bf16[1,128,2048]{2,1,0:T(8,128)(2,1)} %param.13) | copy-start | bytes 1572868
  31.7 26.6 %copy-start.1 = (f32[2048]{0:T(1024)S(1)}, f32[2048]{0:T(1024)}, u32[]{:S(2)}) copy-start(f32[2048]{0:T(1024)} %param.20) | copy-start | bytes 24580
  58.3 40.7 %copy-start.4 = (bf16[1,2048,1024]{2,1,0:T(8,128)(2,1)S(1)}, bf16[1,2048,1024]{2,1,0:T(8,128)(2,1)}, u32[]{:S(2)}) copy-start(bf16[1,2048,1024]{2,1,0:T(8,128)(2,1)} %param.24) | copy-start | bytes 12582916
  58.3 40.7 %copy-start.5 = (bf16[1,1024,2048]{2,1,0:T(8,128)(2,1)S(1)}, bf16[1,1024,2048]{2,1,0:T(8,128)(2,1)}, u32[]{:S(2)}) copy-start(bf16[1,1024,2048]{2,1,0:T(8,128)(2,1)} %param.25) | copy-start | bytes 12582916
  61.2 37.8 %copy-start.3 = (bf16[1,2048,1024]{2,1,0:T(8,128)(2,1)S(1)}, bf16[1,2048,1024]{2,1,0:T(8,128)(2,1)}, u32[]{:S(2)}) copy-start(bf16[1,2048,1024]{2,1,0:T(8,128)(2,1)} %param.23) | copy-start | bytes 12582916
  106.8 34.4 %copy-start.2 = (f32[1,128,2]{1,2,0:T(2,128)S(1)}, f32[1,128,2]{1,2,0:T(2,128)}, u32[]{:S(2)}) copy-start(f32[1,128,2]{1,2,0:T(2,128)} %param.22) | copy-start | bytes 3076

commit v7 on v6

--- a/solution.py
+++ b/solution.py
@@ -36,36 +36,52 @@
 ATT_BLOCKS = 2
 
 
+def route_rows(routes_ref, slot_ref, token_ref):
+    experts = token_ref.shape[1]
+    topk, tokens = routes_ref.shape
+    expert_at = lax.broadcasted_iota(jnp.int32, (experts, tokens), 0)
+    square = (tokens, tokens)
+    earlier = lax.broadcasted_iota(jnp.int32, square, 0) < lax.broadcasted_iota(
+        jnp.int32, square, 1
+    )
+    earlier = jnp.where(earlier, 1.0, 0.0).astype(jnp.bfloat16)
+    taken = jnp.zeros((experts, 1), jnp.float32)
+    ranked = [jnp.zeros((experts, tokens), jnp.float32) for _ in range(CAP)]
+    for k in range(topk):
+        here = jnp.where(expert_at == routes_ref[k : k + 1, :], 1.0, 0.0)
+        before = taken + jnp.dot(
+            here.astype(jnp.bfloat16), earlier, preferred_element_type=jnp.float32
+        )
+        slot = here * (CAP * expert_at.astype(jnp.float32) + before)
+        slot_ref[k : k + 1, :] = jnp.sum(slot, axis=0, keepdims=True).astype(jnp.int32)
+        taken = taken + jnp.sum(here, axis=1, keepdims=True)
+        for rank in range(CAP):
+            ranked[rank] = ranked[rank] + jnp.where(before == rank, here, 0.0)
+    token_at = lax.broadcasted_iota(jnp.int32, (16, tokens), 1).astype(jnp.float32)
+    for rank in range(CAP):
+        of_slot = lax.dot_general(
+            token_at.astype(jnp.bfloat16),
+            ranked[rank].astype(jnp.bfloat16),
+            LAST_DIMS,
+            preferred_element_type=jnp.float32,
+        )
+        token_ref[rank : rank + 1, :] = of_slot[:1].astype(jnp.int32)
+
+
 def attention_kernel(
     lam_ref, qkv_ref, gain_ref, weight_hbm, routes_ref,
-    out_ref, weight_ref, slot_ref, token_ref, values_ref, scores_ref, count_ref, sems,
+    out_ref, weight_ref, slot_ref, token_ref, values_ref, scores_ref, sems,
 ):
     head = lax.axis_index(SP)
     lam = lam_ref[head]
     gain = gain_ref[pl.ds(head, 1), :]
-    experts = count_ref.shape[0]
-    topk, tokens_here = routes_ref.shape
-    routed = [(k, t) for k in range(topk) for t in range(tokens_here)]
-
-    def route(places):
-        for k, t in places:
-            expert = routes_ref[k, t]
-            rank = count_ref[expert]
-            count_ref[expert] = rank + 1
-            slot = expert * CAP + rank
-            slot_ref[k, t] = slot
-            token_ref[slot] = t
-
     sources, _, tokens, width = qkv_ref.shape
     length = sources * tokens
     rows = ATT_BLOCKS * tokens
     steps = sources // ATT_BLOCKS
     fetch = pltpu.make_async_copy(weight_hbm, weight_ref, sems.at[0])
     fetch.start()
-    for index in range(experts):
-        count_ref[index] = 0
-    for index in range(token_ref.shape[0]):
-        token_ref[index] = 0
+    route_rows(routes_ref, slot_ref, token_ref)
     values_ref[:, :VD] = qkv_ref[:, 2].reshape(length, width)
     values_ref[:, VD:] = jnp.ones((length, VD), jnp.bfloat16)
 
@@ -95,12 +111,9 @@
         )
 
     scores(0, 0)
-    share = len(routed) // steps
     for step in range(1, steps):
-        route(routed[(step - 1) * share : step * share])
         scores(step, step % 2)
         attend(step - 1, (step - 1) % 2)
-    route(routed[(steps - 1) * share :])
     attend(steps - 1, (steps - 1) % 2)
     fetch.wait()
 
@@ -114,18 +127,17 @@
     heads = (sources, tokens, VD)
     return pl.pallas_call(
         attention_kernel,
-        in_specs=[in_smem, in_vmem, in_vmem, in_hbm, in_smem],
-        out_specs=[in_vmem, in_vmem, in_smem, in_smem],
+        in_specs=[in_smem, in_vmem, in_vmem, in_hbm, in_vmem],
+        out_specs=[in_vmem] * 4,
         out_shape=[
             jax.ShapeDtypeStruct(heads, jnp.bfloat16),
             pltpu.VMEM(out_weight.shape, jnp.bfloat16),
             jax.ShapeDtypeStruct(routes.shape, jnp.int32),
-            jax.ShapeDtypeStruct((experts * CAP,), jnp.int32),
+            jax.ShapeDtypeStruct((CAP, experts), jnp.int32),
         ],
         scratch_shapes=[
             pltpu.VMEM((length, 2 * VD), jnp.bfloat16),
             pltpu.VMEM((2, 2 * ATT_BLOCKS * tokens, length), jnp.float32),
-            pltpu.SMEM((experts,), jnp.int32),
             pltpu.SemaphoreType.DMA((1,)),
         ],
         compiler_params=within(24),
@@ -238,14 +250,14 @@
         tiles[one], tiles[two] = rows_to_tiles(normed.astype(jnp.bfloat16), swap)
 
     for index in range(sent_ref.shape[0]):
-        sent_ref[index] = tiles[token_ref[index]]
+        sent_ref[index] = tiles[token_ref[index % CAP, index // CAP]]
     for one, two in pair_slices(tokens):
         mid_ref[one], mid_ref[two] = rows_to_tiles(middle[one.start : two.stop, :], swap)
 
 
 def middle_stage(slot_token, heads, out_weight, residual, gain):
     tokens = residual.shape[0]
-    slots = slot_token.shape[0]
+    slots = slot_token.size
     in_vmem = pl.BlockSpec(memory_space=pltpu.VMEM)
     return pl.pallas_call(
         middle_kernel,

time: 144 us -> 143 us (level)
  no operation moved by 1% of the time
where the time goes in v7:
time: 143 us
  blocking collectives  116 us (81%)
  Pallas kernels  26.7 us (19%)
    all_to_all x1, blocking collectives, on_device(): lax.all_to_all(sent, SP_DP, split_axis=0, concat_axis=0, tiled=True)  37.8 us
    all_to_all x1, blocking collectives, on_device(): back = lax.all_to_all(done, SP_DP, split_axis=0, concat_axis=0, tiled=True)  34.4 us
    all_to_all x1, blocking collectives, on_device(): qkv = lax.all_to_all(packed, SP, split_axis=0, concat_axis=0, tiled=True)  30.2 us
    all_to_all x1, blocking collectives, on_device(): lax.all_to_all(attended, SP, split_axis=0, concat_axis=0, tiled=True)  13.3 us
    pallas_call x1, Pallas kernels, attention(): pl.pallas_call(attention_kernel, in_specs=[in_smem, in_vmem, in_vmem, in_...  12.6 us
    pallas_call x1, Pallas kernels, expert_stage(): pl.pallas_call(expert_kernel, in_specs=[in_vmem] * 4, out_specs=in_vmem,...  7.78 us

profile of v7, /device:TPU:1, one launch (start us, length us, event | category | flops | bytes accessed | tf_op | source)
XLA Modules:
  0.0 142.6 jit_solution(6812030277878261638)
XLA Ops:
  0.0 1.5 %pack_heads.1 = bf16[16,3,128,128]{3,2,1,0:T(8,128)(2,1)S(1)} custom-call(bf16[128,2048]{1,0:T(8,128)(2,1)} %bitcast.24, bf16[128,2048]{1,0:T(8,128)(2,1)} %bitcast.25, bf16[128,2048]{1,0:T(8,128)(2,1)} %bitcast.26), custom_call_target="tpu_custom_call" | custom-call | tf_op jit(solution)/shard_map/pack_heads/pallas_call | solution.py:175
  1.5 0.0 copy-start.6
  1.5 0.0 copy-start.7
  1.5 0.0 copy-start.8
  1.5 30.2 %all_to_all.20.qkv_ref = bf16[16,3,128,128]{3,2,1,0:T(8,128)(2,1)S(1)} all-to-all(bf16[16,3,128,128]{3,2,1,0:T(8,128)(2,1)S(1)} %pack_heads.1), channel_id=1, replica_groups=mesh['sp_0'=4,'sp_1'=4,'dp'=8] {'sp_0','sp_1'}, dimensions={0} | all-to-all | bytes 3145728 | tf_op jit(solution)/shard_map/all_to_all | solution.py:386
  31.7 0.0 copy-done.6
  31.7 0.0 copy-done.7
  31.7 0.0 copy-done.8
  31.7 0.0 copy-start
  31.7 0.0 copy-start.1
  31.7 12.6 %attention.1 = (bf16[16,128,128]{2,1,0:T(8,128)(2,1)S(1)}, bf16[2048,2048]{1,0:T(8,128)(2,1)S(1)}, s32[2,128]{1,0:T(2,128)S(1)}, s32[4,128]{1,0:T(4,128)S(1)}) custom-call(f32[16]{0:T(128)S(1)} %copy-done.8, bf16[16,3,128,128]{3,2,1,0:T(8,128)(2,1)S(1)} %all_to_all.20.qkv_ref, f32[16,128]{1,0:T(8,128)S(1)} %bitcast.22, bf16[2048,2048]{1,0:T(8,128)(2,1)} %weight_hbm.1, ...), custom_call_target="tpu_custom_call" | custom-call | flops 4294967296 | bytes 2097152 | tf_op jit(solution)/shard_map/attention/pallas_call | solution.py:128
  44.4 13.3 %all_to_all.21.heads_ref = bf16[16,128,128]{2,1,0:T(8,128)(2,1)S(1)} all-to-all(bf16[16,128,128]{2,1,0:T(8,128)(2,1)S(1)} %get-tuple-element.13), channel_id=1, replica_groups=mesh['sp_0'=4,'sp_1'=4,'dp'=8] {'sp_0','sp_1'}, dimensions={0} | all-to-all | bytes 1048576 | tf_op jit(solution)/shard_map/all_to_all | solution.py:391
  57.7 0.0 copy-done
  57.7 0.0 copy-done.1
  57.7 0.0 copy-start.4
  57.7 0.0 copy-start.5
  57.7 2.8 %middle.1 = (bf16[128,16,128]{2,1,0:T(8,128)(2,1)S(1)}, bf16[512,16,128]{2,1,0:T(8,128)(2,1)S(1)}) custom-call(s32[4,128]{1,0:T(4,128)S(1)} %get-tuple-element.12.token_ref, bf16[16,128,128]{2,1,0:T(8,128)(2,1)S(1)} %all_to_all.21.heads_ref, bf16[2048,2048]{1,0:T(8,128)(2,1)S(1)} %get-tuple-element.14.weight_ref, bf16[128,2048]{1,0:T(8,128)(2,1)S(1)} %bitcast.16, ...), custom_call_target="tpu_custom_call" | custom-call | flops 1073741824 | bytes 8388608 | tf_op jit(solution)/shard_map/middle/pallas_call | solution.py:262
  60.6 0.0 copy-start.3
  60.6 37.8 %all_to_all.22.tile_ref = bf16[512,16,128]{2,1,0:T(8,128)(2,1)S(1)} all-to-all(bf16[512,16,128]{2,1,0:T(8,128)(2,1)S(1)} %get-tuple-element.16), channel_id=1, replica_groups=mesh['sp_0'=4,'sp_1'=4,'dp'=8] {'sp_0','sp_1','dp'}, dimensions={0} | all-to-all | bytes 4194304 | tf_op jit(solution)/shard_map/all_to_all | solution.py:393
  98.4 0.0 copy-done.4
  98.4 0.0 copy-done.5
  98.4 0.0 copy-done.3
  98.4 7.8 %experts.1 = bf16[512,16,128]{2,1,0:T(8,128)(2,1)S(1)} custom-call(bf16[512,16,128]{2,1,0:T(8,128)(2,1)S(1)} %all_to_all.22.tile_ref, bf16[2048,1024]{1,0:T(8,128)(2,1)S(1)} %bitcast.19, bf16[2048,1024]{1,0:T(8,128)(2,1)S(1)} %bitcast.20, bf16[1024,2048]{1,0:T(8,128)(2,1)S(1)} %bitcast.21), custom_call_target="tpu_custom_call" | custom-call | flops 6442450944 | bytes 12582912 | tf_op jit(solution)/shard_map/experts/pallas_call | solution.py:309
  106.2 0.0 copy-start.2
  106.2 34.4 %all_to_all.23.back_ref = bf16[512,16,128]{2,1,0:T(8,128)(2,1)S(1)} all-to-all(bf16[512,16,128]{2,1,0:T(8,128)(2,1)S(1)} %experts.1), channel_id=1, replica_groups=mesh['sp_0'=4,'sp_1'=4,'dp'=8] {'sp_0','sp_1','dp'}, dimensions={0} | all-to-all | bytes 4194304 | tf_op jit(solution)/shard_map/all_to_all | solution.py:395
  140.5 0.0 copy-done.2
  140.5 1.9 %combine.1 = bf16[128,2048]{1,0:T(8,128)(2,1)} custom-call(s32[2,128]{1,0:T(2,128)S(1)} %get-tuple-element.11.slot_ref, f32[2,128]{1,0:T(2,128)S(1)} %bitcast.18, bf16[128,16,128]{2,1,0:T(8,128)(2,1)S(1)} %get-tuple-element.15.mid_ref, bf16[512,16,128]{2,1,0:T(8,128)(2,1)S(1)} %all_to_all.23.back_ref), custom_call_target="tpu_custom_call" | custom-call | tf_op jit(solution)/shard_map/combine/pallas_call | solution.py:353
Async XLA Ops:
  1.5 30.2 %copy-start.6 = (f32[2048]{0:T(1024)S(1)}, f32[2048]{0:T(1024)}, u32[]{:S(2)}) copy-start(f32[2048]{0:T(1024)} %param.18) | copy-start | bytes 24580
  1.5 30.2 %copy-start.7 = (s32[1,128,2]{1,2,0:T(2,128)S(1)}, s32[1,128,2]{1,2,0:T(2,128)}, u32[]{:S(2)}) copy-start(s32[1,128,2]{1,2,0:T(2,128)} %param.21) | copy-start | bytes 3076
  1.5 30.2 %copy-start.8 = (f32[16]{0:T(128)S(1)}, f32[16]{0:T(128)}, u32[]{:S(2)}) copy-start(f32[16]{0:T(128)} %lam_ref.1) | copy-start | bytes 196
  31.7 26.0 %copy-start = (bf16[1,128,2048]{2,1,0:T(8,128)(2,1)S(1)}, bf16[1,128,2048]{2,1,0:T(8,128)(2,1)}, u32[]{:S(2)}) copy-start(bf16[1,128,2048]{2,1,0:T(8,128)(2,1)} %param.13) | copy-start | bytes 1572868
  31.7 26.0 %copy-start.1 = (f32[2048]{0:T(1024)S(1)}, f32[2048]{0:T(1024)}, u32[]{:S(2)}) copy-start(f32[2048]{0:T(1024)} %param.20) | copy-start | bytes 24580
  57.7 40.7 %copy-start.4 = (bf16[1,2048,1024]{2,1,0:T(8,128)(2,1)S(1)}, bf16[1,2048,1024]{2,1,0:T(8,128)(2,1)}, u32[]{:S(2)}) copy-start(bf16[1,2048,1024]{2,1,0:T(8,128)(2,1)} %param.24) | copy-start | bytes 12582916
  57.7 40.7 %copy-start.5 = (bf16[1,1024,2048]{2,1,0:T(8,128)(2,1)S(1)}, bf16[1,1024,2048]{2,1,0:T(8,128)(2,1)}, u32[]{:S(2)}) copy-start(bf16[1,1024,2048]{2,1,0:T(8,128)(2,1)} %param.25) | copy-start | bytes 12582916
  60.6 37.8 %copy-start.3 = (bf16[1,2048,1024]{2,1,0:T(8,128)(2,1)S(1)}, bf16[1,2048,1024]{2,1,0:T(8,128)(2,1)}, u32[]{:S(2)}) copy-start(bf16[1,2048,1024]{2,1,0:T(8,128)(2,1)} %param.23) | copy-start | bytes 12582916
  106.2 34.4 %copy-start.2 = (f32[1,128,2]{1,2,0:T(2,128)S(1)}, f32[1,128,2]{1,2,0:T(2,128)}, u32[]{:S(2)}) copy-start(f32[1,128,2]{1,2,0:T(2,128)} %param.22) | copy-start | bytes 3076

commit v8 on v7

--- a/solution.py
+++ b/solution.py
@@ -69,8 +69,8 @@
 
 
 def attention_kernel(
-    lam_ref, qkv_ref, gain_ref, weight_hbm, routes_ref,
-    out_ref, weight_ref, slot_ref, token_ref, values_ref, scores_ref, sems,
+    lam_ref, qkv_ref, gain_ref, weight_hbm,
+    out_ref, weight_ref, values_ref, scores_ref, sems,
 ):
     head = lax.axis_index(SP)
     lam = lam_ref[head]
@@ -81,7 +81,6 @@
     steps = sources // ATT_BLOCKS
     fetch = pltpu.make_async_copy(weight_hbm, weight_ref, sems.at[0])
     fetch.start()
-    route_rows(routes_ref, slot_ref, token_ref)
     values_ref[:, :VD] = qkv_ref[:, 2].reshape(length, width)
     values_ref[:, VD:] = jnp.ones((length, VD), jnp.bfloat16)
 
@@ -118,7 +117,7 @@
     fetch.wait()
 
 
-def attention(lam, qkv, gain, out_weight, routes, experts):
+def attention(lam, qkv, gain, out_weight):
     sources, _, tokens, width = qkv.shape
     length = sources * tokens
     in_vmem = pl.BlockSpec(memory_space=pltpu.VMEM)
@@ -127,13 +126,11 @@
     heads = (sources, tokens, VD)
     return pl.pallas_call(
         attention_kernel,
-        in_specs=[in_smem, in_vmem, in_vmem, in_hbm, in_vmem],
-        out_specs=[in_vmem] * 4,
+        in_specs=[in_smem, in_vmem, in_vmem, in_hbm],
+        out_specs=[in_vmem] * 2,
         out_shape=[
             jax.ShapeDtypeStruct(heads, jnp.bfloat16),
             pltpu.VMEM(out_weight.shape, jnp.bfloat16),
-            jax.ShapeDtypeStruct(routes.shape, jnp.int32),
-            jax.ShapeDtypeStruct((CAP, experts), jnp.int32),
         ],
         scratch_shapes=[
             pltpu.VMEM((length, 2 * VD), jnp.bfloat16),
@@ -147,7 +144,7 @@
             transcendentals=2 * length * length,
         ),
         name="attention",
-    )(lam, on_chip(qkv), gain, off_chip(out_weight), routes)
+    )(lam, on_chip(qkv), gain, off_chip(out_weight))
 
 
 ROW = (16, 128)
@@ -156,34 +153,47 @@
 CAP = 4
 
 
-def pack_kernel(query_ref, key_ref, value_ref, out_ref, rows, sems):
+def pack_kernel(
+    routes_hbm, query_ref, key_ref, value_ref,
+    out_ref, slot_ref, token_ref, routes_ref, rows, sems,
+):
+    route_copy = pltpu.make_async_copy(routes_hbm, routes_ref, sems.at[3])
     copies = [
         pltpu.make_async_copy(ref, rows.at[at], sems.at[at])
         for at, ref in enumerate((query_ref, key_ref, value_ref))
     ]
+    route_copy.start()
     for copy in copies:
         copy.start()
+    route_copy.wait()
+    route_rows(routes_ref, slot_ref, token_ref)
     for at in range(3):
         copies[at].wait()
         for head in range(HEADS):
             out_ref[head, at] = rows[at, :, head * VD : (head + 1) * VD]
 
 
-def pack_heads(query, key, value):
+def pack_heads(routes, query, key, value, experts):
     tokens = query.shape[0]
     in_hbm = pl.BlockSpec(memory_space=pltpu.HBM)
+    in_vmem = pl.BlockSpec(memory_space=pltpu.VMEM)
     return pl.pallas_call(
         pack_kernel,
-        in_specs=[in_hbm] * 3,
-        out_specs=pl.BlockSpec(memory_space=pltpu.VMEM),
-        out_shape=jax.ShapeDtypeStruct((HEADS, 3, tokens, VD), jnp.bfloat16),
+        in_specs=[in_hbm] * 4,
+        out_specs=[in_vmem] * 3,
+        out_shape=[
+            jax.ShapeDtypeStruct((HEADS, 3, tokens, VD), jnp.bfloat16),
+            jax.ShapeDtypeStruct(routes.shape, jnp.int32),
+            jax.ShapeDtypeStruct((CAP, experts), jnp.int32),
+        ],
         scratch_shapes=[
+            pltpu.VMEM(routes.shape, jnp.int32),
             pltpu.VMEM((3, tokens, HEADS * VD), jnp.bfloat16),
-            pltpu.SemaphoreType.DMA((3,)),
+            pltpu.SemaphoreType.DMA((4,)),
         ],
         compiler_params=within(8),
         name="pack_heads",
-    )(*(off_chip(a) for a in (query, key, value)))
+    )(*(off_chip(a) for a in (routes, query, key, value)))
 
 
 def swap_matrix():
@@ -382,12 +392,11 @@
 ):
     count_sp = lax.axis_size(SP)
     count_dp = lax.axis_size("dp")
-    packed = pack_heads(query_maps[0], key_maps[0], value_rows[0])
+    packed, slot, slot_token = pack_heads(
+        routes[0].T, query_maps[0], key_maps[0], value_rows[0], count_sp * count_dp
+    )
     qkv = lax.all_to_all(packed, SP, split_axis=0, concat_axis=0, tiled=True)
-    experts_all = count_sp * count_dp
-    attended, weight_here, slot, slot_token = attention(
-        lambdas, qkv, head_gain.reshape(HEADS, VD), out_weight, routes[0].T, experts_all
-    )
+    attended, weight_here = attention(lambdas, qkv, head_gain.reshape(HEADS, VD), out_weight)
     returned = lax.all_to_all(attended, SP, split_axis=0, concat_axis=0, tiled=True)
     mid, sent = middle_stage(slot_token, returned, weight_here, residual[0], ffn_gain[None])
     arrived = lax.all_to_all(sent, SP_DP, split_axis=0, concat_axis=0, tiled=True)

time: 143 us -> 143 us (level)
  no operation moved by 1% of the time
where the time goes in v8:
time: 143 us; the launch traced here: 142 us
  blocking collectives  116 us (81%)
  Pallas kernels  26.5 us (19%)
    all_to_all x1, blocking collectives, on_device(): lax.all_to_all(sent, SP_DP, split_axis=0, concat_axis=0, tiled=True)  37.8 us
    all_to_all x1, blocking collectives, on_device(): back = lax.all_to_all(done, SP_DP, split_axis=0, concat_axis=0, tiled=True)  34.4 us
    all_to_all x1, blocking collectives, on_device(): qkv = lax.all_to_all(packed, SP, split_axis=0, concat_axis=0, tiled=True)  30 us
    all_to_all x1, blocking collectives, on_device(): lax.all_to_all(attended, SP, split_axis=0, concat_axis=0, tiled=True)  13.3 us
    pallas_call x1, Pallas kernels, attention(): pl.pallas_call(attention_kernel, in_specs=[in_smem, in_vmem, in_vmem, in_...  12.4 us
    pallas_call x1, Pallas kernels, expert_stage(): pl.pallas_call(expert_kernel, in_specs=[in_vmem] * 4, out_specs=in_vmem,...  7.76 us

profile of v8, /device:TPU:1, one launch (start us, length us, event | category | flops | bytes accessed | tf_op | source)
XLA Modules:
  0.0 142.3 jit_solution(8118256780631573920)
XLA Ops:
  0.0 0.0 copy-start.6
  0.0 0.0 copy-start.7
  0.0 1.5 %pack_heads.1 = (bf16[16,3,128,128]{3,2,1,0:T(8,128)(2,1)S(1)}, s32[2,128]{1,0:T(2,128)S(1)}, s32[4,128]{1,0:T(4,128)S(1)}) custom-call(s32[2,128]{1,0:T(2,128)} %bitcast.26, bf16[128,2048]{1,0:T(8,128)(2,1)} %bitcast.23, bf16[128,2048]{1,0:T(8,128)(2,1)} %bitcast.24, bf16[128,2048]{1,0:T(8,128)(2,1)} %bitcast.25), custom_call_target="tpu_custom_call" | custom-call | tf_op jit(solution)/shard_map/pack_heads/pallas_call | solution.py:180
  1.5 30.0 %all_to_all.20.qkv_ref = bf16[16,3,128,128]{3,2,1,0:T(8,128)(2,1)S(1)} all-to-all(bf16[16,3,128,128]{3,2,1,0:T(8,128)(2,1)S(1)} %get-tuple-element.14), channel_id=1, replica_groups=mesh['sp_0'=4,'sp_1'=4,'dp'=8] {'sp_0','sp_1'}, dimensions={0} | all-to-all | bytes 3145728 | tf_op jit(solution)/shard_map/all_to_all | solution.py:398
  31.6 0.0 copy-done.6
  31.6 0.0 copy-done.7
  31.6 0.0 copy-start
  31.6 0.0 copy-start.1
  31.6 12.4 %attention.1 = (bf16[16,128,128]{2,1,0:T(8,128)(2,1)S(1)}, bf16[2048,2048]{1,0:T(8,128)(2,1)S(1)}) custom-call(f32[16]{0:T(128)S(1)} %copy-done.7, bf16[16,3,128,128]{3,2,1,0:T(8,128)(2,1)S(1)} %all_to_all.20.qkv_ref, f32[16,128]{1,0:T(8,128)S(1)} %bitcast.22, bf16[2048,2048]{1,0:T(8,128)(2,1)} %weight_hbm.1), custom_call_target="tpu_custom_call" | custom-call | flops 4294967296 | bytes 2097152 | tf_op jit(solution)/shard_map/attention/pallas_call | solution.py:127
  44.1 13.3 %all_to_all.21.heads_ref = bf16[16,128,128]{2,1,0:T(8,128)(2,1)S(1)} all-to-all(bf16[16,128,128]{2,1,0:T(8,128)(2,1)S(1)} %get-tuple-element.15), channel_id=1, replica_groups=mesh['sp_0'=4,'sp_1'=4,'dp'=8] {'sp_0','sp_1'}, dimensions={0} | all-to-all | bytes 1048576 | tf_op jit(solution)/shard_map/all_to_all | solution.py:400
  57.4 0.0 copy-done
  57.4 0.0 copy-done.1
  57.4 0.0 copy-start.4
  57.4 0.0 copy-start.5
  57.4 2.8 %middle.1 = (bf16[128,16,128]{2,1,0:T(8,128)(2,1)S(1)}, bf16[512,16,128]{2,1,0:T(8,128)(2,1)S(1)}) custom-call(s32[4,128]{1,0:T(4,128)S(1)} %get-tuple-element.13.token_ref, bf16[16,128,128]{2,1,0:T(8,128)(2,1)S(1)} %all_to_all.21.heads_ref, bf16[2048,2048]{1,0:T(8,128)(2,1)S(1)} %get-tuple-element.16.weight_ref, bf16[128,2048]{1,0:T(8,128)(2,1)S(1)} %bitcast.16, ...), custom_call_target="tpu_custom_call" | custom-call | flops 1073741824 | bytes 8388608 | tf_op jit(solution)/shard_map/middle/pallas_call | solution.py:272
  60.2 0.0 copy-start.3
  60.2 37.8 %all_to_all.22.tile_ref = bf16[512,16,128]{2,1,0:T(8,128)(2,1)S(1)} all-to-all(bf16[512,16,128]{2,1,0:T(8,128)(2,1)S(1)} %get-tuple-element.18), channel_id=1, replica_groups=mesh['sp_0'=4,'sp_1'=4,'dp'=8] {'sp_0','sp_1','dp'}, dimensions={0} | all-to-all | bytes 4194304 | tf_op jit(solution)/shard_map/all_to_all | solution.py:402
  98.0 0.0 copy-done.4
  98.0 0.0 copy-done.5
  98.0 0.0 copy-done.3
  98.0 7.8 %experts.1 = bf16[512,16,128]{2,1,0:T(8,128)(2,1)S(1)} custom-call(bf16[512,16,128]{2,1,0:T(8,128)(2,1)S(1)} %all_to_all.22.tile_ref, bf16[2048,1024]{1,0:T(8,128)(2,1)S(1)} %bitcast.19, bf16[2048,1024]{1,0:T(8,128)(2,1)S(1)} %bitcast.20, bf16[1024,2048]{1,0:T(8,128)(2,1)S(1)} %bitcast.21), custom_call_target="tpu_custom_call" | custom-call | flops 6442450944 | bytes 12582912 | tf_op jit(solution)/shard_map/experts/pallas_call | solution.py:319
  105.8 0.0 copy-start.2
  105.8 34.4 %all_to_all.23.back_ref = bf16[512,16,128]{2,1,0:T(8,128)(2,1)S(1)} all-to-all(bf16[512,16,128]{2,1,0:T(8,128)(2,1)S(1)} %experts.1), channel_id=1, replica_groups=mesh['sp_0'=4,'sp_1'=4,'dp'=8] {'sp_0','sp_1','dp'}, dimensions={0} | all-to-all | bytes 4194304 | tf_op jit(solution)/shard_map/all_to_all | solution.py:404
  140.2 0.0 copy-done.2
  140.2 1.9 %combine.1 = bf16[128,2048]{1,0:T(8,128)(2,1)} custom-call(s32[2,128]{1,0:T(2,128)S(1)} %get-tuple-element.12.slot_ref, f32[2,128]{1,0:T(2,128)S(1)} %bitcast.18, bf16[128,16,128]{2,1,0:T(8,128)(2,1)S(1)} %get-tuple-element.17.mid_ref, bf16[512,16,128]{2,1,0:T(8,128)(2,1)S(1)} %all_to_all.23.back_ref), custom_call_target="tpu_custom_call" | custom-call | tf_op jit(solution)/shard_map/combine/pallas_call | solution.py:363
Async XLA Ops:
  0.0 31.6 %copy-start.6 = (f32[2048]{0:T(1024)S(1)}, f32[2048]{0:T(1024)}, u32[]{:S(2)}) copy-start(f32[2048]{0:T(1024)} %param.18) | copy-start | bytes 24580
  0.0 31.6 %copy-start.7 = (f32[16]{0:T(128)S(1)}, f32[16]{0:T(128)}, u32[]{:S(2)}) copy-start(f32[16]{0:T(128)} %lam_ref.1) | copy-start | bytes 196
  31.6 25.8 %copy-start = (bf16[1,128,2048]{2,1,0:T(8,128)(2,1)S(1)}, bf16[1,128,2048]{2,1,0:T(8,128)(2,1)}, u32[]{:S(2)}) copy-start(bf16[1,128,2048]{2,1,0:T(8,128)(2,1)} %param.13) | copy-start | bytes 1572868
  31.6 25.8 %copy-start.1 = (f32[2048]{0:T(1024)S(1)}, f32[2048]{0:T(1024)}, u32[]{:S(2)}) copy-start(f32[2048]{0:T(1024)} %param.20) | copy-start | bytes 24580
  57.4 40.7 %copy-start.4 = (bf16[1,2048,1024]{2,1,0:T(8,128)(2,1)S(1)}, bf16[1,2048,1024]{2,1,0:T(8,128)(2,1)}, u32[]{:S(2)}) copy-start(bf16[1,2048,1024]{2,1,0:T(8,128)(2,1)} %param.24) | copy-start | bytes 12582916
  57.4 40.7 %copy-start.5 = (bf16[1,1024,2048]{2,1,0:T(8,128)(2,1)S(1)}, bf16[1,1024,2048]{2,1,0:T(8,128)(2,1)}, u32[]{:S(2)}) copy-start(bf16[1,1024,2048]{2,1,0:T(8,128)(2,1)} %param.25) | copy-start | bytes 12582916
  60.2 37.8 %copy-start.3 = (bf16[1,2048,1024]{2,1,0:T(8,128)(2,1)S(1)}, bf16[1,2048,1024]{2,1,0:T(8,128)(2,1)}, u32[]{:S(2)}) copy-start(bf16[1,2048,1024]{2,1,0:T(8,128)(2,1)} %param.23) | copy-start | bytes 12582916
  105.8 34.4 %copy-start.2 = (f32[1,128,2]{1,2,0:T(2,128)S(1)}, f32[1,128,2]{1,2,0:T(2,128)}, u32[]{:S(2)}) copy-start(f32[1,128,2]{1,2,0:T(2,128)} %param.22) | copy-start | bytes 3076
